TPU v7x, 32 devices: a whole 2x2x4 slice. The times are simulated.
32 devices in a mesh: ep: 4 (over y, x), tp: 8 (over z, core).
Axes of the slice: x: 2, y: 2, z: 4, core: 2. Of those that a mesh axis runs over, the one named last changes fastest.
Arguments:
- query_latent: bfloat16 [2048, 1024], P('ep'), may hold values from -6 to 6
- joint_latent: bfloat16 [2048, 512], P('ep'), may hold values from -6 to 6
- rotary_key: bfloat16 [2048, 32], P('ep'), may hold values from -60 to 60
- query_gain: float32 [1024], replicated, may hold values from 0.1 to 1.9
- joint_gain: float32 [512], replicated, may hold values from 0.1 to 1.9
- query_weight: bfloat16 [1024, 2048], P(None, 'tp'), may hold values from -0.1875 to 0.1875
- query_rotary: bfloat16 [1024, 1024], P(None, 'tp'), may hold values from -0.1875 to 0.1875
- key_weight: bfloat16 [512, 2048], P(None, 'tp'), may hold values from -0.25 to 0.25
- value_weight: bfloat16 [512, 2048], P(None, 'tp'), may hold values from -0.25 to 0.25
- output_weight: bfloat16 [2048, 2048], P('tp'), may hold values from -6 to 6
- expert_input: bfloat16 [2048, 2048], P('ep'), may hold values from -6 to 6
- expert_gain: float32 [2048], replicated, may hold values from 0.1 to 1.9
- routes: int32 [2048, 2], P('ep'), may hold values from 0 to 7, all different within a row; in each aligned block of 512 rows (0 to 511, 512 to 1023, ...) at most 192 rows name the same one
- route_weight: float32 [2048, 2], P('ep'), may hold values from 0.2 to 1
- gate_weight: bfloat16 [8, 2048, 4096], P('ep', None, 'tp'), may hold values from -0.125 to 0.125
- up_weight: bfloat16 [8, 2048, 4096], P('ep', None, 'tp'), may hold values from -0.125 to 0.125
- down_weight: bfloat16 [8, 4096, 2048], P('ep', 'tp'), may hold values from -0.09375 to 0.09375
Outputs:
- mixer_out: bfloat16 [2048, 2048], P(('ep', 'tp'))
- expert_out: bfloat16 [2048, 2048], P('ep', 'tp')
Inputs may be any that keep to these rules, and one draw needn't show every extreme that they name: `routes`: A row names 2 different experts. Among the rows of one device (aligned blocks of 512 rows) no expert is named by more than 192 rows, a bound that some block reaches.
All inputs are finite; a program needn't handle non-finite values.
Results may differ from a plain program's by a relative error of at most 0.019.
The roundings to bfloat16 on the way count: a program that leaves them out, or rounds other values in their place, can miss the bound.
Values may be sent and summed in bfloat16 or wider, within the bound.
No kernel may reach another device: no remote copies, remote signals or barrier semaphores. Data moves between devices by JAX's collectives and lax.ppermute only.
A program may use at most 128 MiB of HBM per device.

v0:
```python
import functools

import jax
import jax.numpy as jnp
from jax import lax
from jax.experimental import pallas as pl
from jax.experimental.pallas import tpu as pltpu
from jax.sharding import PartitionSpec as P


NOPE = 64
VDIM = 64
NORM_EPSILON = 1e-06
ROTARY_BASE = 10000.0
LOG2E = 1.4426950408889634

F32 = jnp.float32
BF16 = jnp.bfloat16

SMEM_SPEC = pl.BlockSpec(memory_space=pltpu.SMEM)
VMEM_SPEC = pl.BlockSpec(memory_space=pltpu.VMEM)
HBM_SPEC = pl.BlockSpec(memory_space=pltpu.HBM)


def params(mebibytes):
    return pltpu.CompilerParams(vmem_limit_bytes=mebibytes * 1024 * 1024)


def cost(flops, bytes_accessed):
    return pl.CostEstimate(
        flops=int(flops), bytes_accessed=int(bytes_accessed), transcendentals=0
    )


def swap_over(value, axis, mask):
    size = lax.axis_size(axis)
    return lax.ppermute(value, axis, [(i, i ^ mask) for i in range(size)])


def bits_of(size):
    return max(size - 1, 0).bit_length()


def spread(index, bits):
    return sum(((index >> (bits - 1 - b)) & 1) << b for b in range(bits))


def norm_value(source, gain):
    wide = source.astype(F32)
    factor = lax.rsqrt(jnp.mean(wide * wide, axis=-1, keepdims=True) + NORM_EPSILON)
    return (wide * factor * gain).astype(BF16)


def rotate_lanes(source, cosine, sine, half):
    width = source.shape[-1]
    lane = lax.broadcasted_iota(jnp.int32, source.shape, 1)
    first = (lane & (2 * half - 1)) < half
    partner = jnp.where(
        first, pltpu.roll(source, width - half, 1), pltpu.roll(source, half, 1)
    )
    return source * cosine + partner * sine


def prepare_kernel(
    ids, joint_hbm, joint_gain_hbm, rotary_hbm, routes_hbm, weights_hbm, rows_hbm, rows_gain_hbm,
    mine_hbm, other_hbm, meta_hbm, row_mine_hbm, row_other_hbm,
    joint, joint_gain, rotary, routes, weights, rows, rows_gain,
    mine, other, meta, row_mine, row_other, sems,
):
    inputs = (
        (joint_hbm, joint), (joint_gain_hbm, joint_gain), (rotary_hbm, rotary),
        (routes_hbm, routes), (weights_hbm, weights), (rows_gain_hbm, rows_gain), (rows_hbm, rows),
    )
    loads = [
        pltpu.make_async_copy(source, target, sems.at[i])
        for i, (source, target) in enumerate(inputs)
    ]
    outputs = (
        (mine, mine_hbm), (other, other_hbm), (meta, meta_hbm), (row_mine, row_mine_hbm),
        (row_other, row_other_hbm),
    )
    stores = [
        pltpu.make_async_copy(source, target, sems.at[len(loads) + i])
        for i, (source, target) in enumerate(outputs)
    ]
    for load in loads:
        load.start()
    for load in loads[:5]:
        load.wait()
    half, full = mine.shape
    count, width = joint.shape
    turn, top = rotary.shape[0], routes.shape[0]
    weight = weights[...]
    high = weight.astype(BF16).astype(F32)
    middle = (weight - high).astype(BF16).astype(F32)
    low = weight - high - middle
    rest = jnp.zeros((full - width - turn - 4 * top, count), F32)
    named = routes[...].astype(F32)
    meta[...] = jnp.concatenate([named, weight, rest[: 8 - 2 * top]], axis=0)
    side = jnp.concatenate(
        [rotary[...].astype(F32), named, high, middle, low, rest], axis=0
    ).T.astype(BF16)
    chosen = ids[1] == 0
    mine[:, width:] = jnp.where(chosen, side[:half], side[half:])
    other[:, width:] = jnp.where(chosen, side[half:], side[:half])
    own = pl.multiple_of(ids[1] * half, half)
    far = pl.multiple_of((1 - ids[1]) * half, half)
    mine[:, :width] = norm_value(joint[pl.ds(own, half), :], joint_gain[...])
    stores[0].start()
    other[:, :width] = norm_value(joint[pl.ds(far, half), :], joint_gain[...])
    stores[1].start()
    stores[2].start()
    for load in loads[5:]:
        load.wait()
    row_mine[...] = norm_value(rows[pl.ds(own, half), :], rows_gain[...])
    stores[3].start()
    row_other[...] = norm_value(rows[pl.ds(far, half), :], rows_gain[...])
    stores[4].start()
    for store in stores:
        store.wait()


def prepare(ids, joint, joint_gain, rotary, routes, weights, rows, rows_gain):
    count, width = joint.shape
    half = count // 2
    inputs = (
        joint, joint_gain.reshape(1, width), rotary.T, routes.T, weights.T, rows,
        rows_gain.reshape(1, rows.shape[1]),
    )
    outputs = (
        jax.ShapeDtypeStruct((half, width + 128), BF16),
        jax.ShapeDtypeStruct((half, width + 128), BF16),
        jax.ShapeDtypeStruct((8, count), F32),
        jax.ShapeDtypeStruct((half, rows.shape[1]), BF16),
        jax.ShapeDtypeStruct((half, rows.shape[1]), BF16),
    )
    return pl.pallas_call(
        prepare_kernel,
        out_shape=outputs,
        in_specs=[SMEM_SPEC] + [HBM_SPEC] * len(inputs),
        out_specs=(HBM_SPEC,) * len(outputs),
        scratch_shapes=[pltpu.VMEM(v.shape, v.dtype) for v in inputs + outputs]
        + [pltpu.SemaphoreType.DMA((len(inputs) + len(outputs),))],
        compiler_params=params(60),
        cost_estimate=cost(4e12 * 3e-6, 4e6),
        name="prepare",
    )(ids, *inputs)


def turn_tables(cosine, sine, start, count, lanes):
    turned = pl.ds(start, count)
    half = cosine.shape[0]
    repeat = lanes // (2 * half)
    c, s = cosine[:, turned], sine[:, turned]
    return (
        jnp.concatenate([c, c] * repeat, axis=0).T,
        jnp.concatenate([-s, s] * repeat, axis=0).T,
    )


def pick_value(local_count, capacity, group_count, ids, routes, out):
    tokens = routes.shape[1]
    group = ids[2]
    total = group_count * local_count
    row = lax.broadcasted_iota(jnp.int32, (total, tokens), 0)
    expert = ((group ^ (row // local_count)) * local_count + row % local_count)
    first = routes[0:1, :] == expert
    second = routes[1:2, :] == expert
    before = (
        lax.broadcasted_iota(jnp.int32, (tokens, tokens), 0)
        < lax.broadcasted_iota(jnp.int32, (tokens, tokens), 1)
    ).astype(BF16)
    named = jnp.where(first | second, 1.0, 0.0).astype(BF16)
    slot = jnp.dot(named, before, preferred_element_type=F32) + (row * capacity).astype(F32)
    pair = jnp.concatenate(
        [
            jnp.sum(jnp.where(first, slot, 0.0), axis=0, keepdims=True),
            jnp.sum(jnp.where(second, slot, 0.0), axis=0, keepdims=True),
            jnp.zeros((126, tokens), F32),
        ],
        axis=0,
    ).T
    span = 128
    for start in range(0, total * capacity, span):
        place = (lax.broadcasted_iota(jnp.int32, (tokens, span), 1) + start).astype(F32)
        out[:, start : start + span] = jnp.where(
            (place == pair[:, 0:1]) | (place == pair[:, 1:2]), 1.0, 0.0
        ).astype(BF16)


def query_kernel(
    turn_width, local_count, capacity, group_count, ids, query_latent, gain, query_weight,
    query_rotary, cosine, sine, routes, plain, turned, pick
):
    rows = query_latent.shape[0]
    normed = norm_value(query_latent[...], gain[...])
    plain[...] = jnp.dot(normed, query_weight[...], preferred_element_type=F32).astype(BF16)
    start = pl.multiple_of(ids[2] * rows, rows)
    c, s = turn_tables(cosine, sine, start, rows, turned.shape[1])
    turned[...] = rotate_lanes(
        jnp.dot(normed, query_rotary[...], preferred_element_type=F32), c, s, turn_width // 2
    ).astype(BF16)
    pick_value(local_count, capacity, group_count, ids, routes, pick)


def queries(
    ids, query_latent, gain, query_weight, query_rotary, cosine, sine, routes, turn_width,
    local_count, capacity, group_count,
):
    rows, width = query_latent.shape
    tokens = routes.shape[0]
    return pl.pallas_call(
        functools.partial(query_kernel, turn_width, local_count, capacity, group_count),
        out_shape=(
            jax.ShapeDtypeStruct((rows, query_weight.shape[1]), BF16),
            jax.ShapeDtypeStruct((rows, query_rotary.shape[1]), BF16),
            jax.ShapeDtypeStruct((tokens, group_count * local_count * capacity), BF16),
        ),
        in_specs=[SMEM_SPEC] + [VMEM_SPEC] * 7,
        out_specs=(VMEM_SPEC,) * 3,
        compiler_params=params(60),
        cost_estimate=cost(4e12 * 4e-6, 12e6),
        name="queries",
    )(
        ids, query_latent, gain.reshape(1, width), query_weight, query_rotary, cosine, sine,
        routes.T,
    )


def attention_kernel(
    turn_width, piece_count, tp_bits, ids, plain, turned, cosine, sine, key_weight,
    value_weight, output_hbm, *rest
):
    pieces = rest[:piece_count]
    keep, send, meta, keys, values, mixed, output_weight, sem = rest[piece_count:]
    fetch = pltpu.make_async_copy(output_hbm, output_weight, sem)
    fetch.start()
    rows = plain.shape[0]
    latent = key_weight.shape[0]
    turn_lanes = turned.shape[1]
    pair_count = keys.shape[0]
    pair = 2 * NOPE
    scale = LOG2E * (NOPE + turn_width) ** (-0.5)
    half = pieces[0].shape[0]
    repeat = turn_lanes // turn_width

    for index, piece in enumerate(pieces):
        name, side = index // 2, index % 2
        place = ids[1] if side == 0 else 1 - ids[1]
        base = pl.multiple_of(place * half, half)
        block = piece[:, :latent]
        start = index * half
        key_block = jnp.dot(block, key_weight[...], preferred_element_type=F32).astype(BF16)
        value_block = jnp.dot(block, value_weight[...], preferred_element_type=F32).astype(BF16)
        beside = piece[:, latent:].astype(F32)
        if name > 0:
            meta[name - 1, :, pl.ds(base, half)] = beside.T[turn_width : turn_width + 8, :]
        key = beside[:, :turn_width]
        key = jnp.concatenate([key] * repeat, axis=1)
        c, s = turn_tables(
            cosine, sine, pl.multiple_of(ids[3 + name] * rows + place * half, half), half,
            turn_lanes,
        )
        key = rotate_lanes(key, c, s, turn_width // 2).astype(BF16)
        for p in range(pair_count):
            keys[p, start : start + half, :pair] = key_block[:, p * pair : (p + 1) * pair]
            keys[p, start : start + half, pair:] = key
            values[p, start : start + half, :] = value_block[:, p * pair : (p + 1) * pair]

    tile = min(rows, 256)
    plain_lane = lax.broadcasted_iota(jnp.int32, (tile, pair), 1)
    turn_lane = lax.broadcasted_iota(jnp.int32, (tile, turn_lanes), 1)
    zero = jnp.zeros((), BF16)

    def step(index, carry):
        row = pl.ds(pl.multiple_of(index * tile, tile), tile)
        for p in range(pair_count):
            outs = []
            for h in range(2):
                head = 2 * p + h
                left = jnp.where(
                    (plain_lane // NOPE) == h, plain[row, p * pair : (p + 1) * pair], zero
                )
                right = jnp.where((turn_lane // turn_width) == head, turned[row, :], zero)
                query = jnp.concatenate([left, right], axis=1)
                scores = lax.dot_general(
                    query, keys[p], (((1,), (1,)), ((), ())), preferred_element_type=F32
                )
                top = jnp.max(scores, axis=1, keepdims=True)
                expo = jnp.exp2((scores - top) * scale)
                total = jnp.sum(expo, axis=1, keepdims=True)
                mix = jnp.dot(expo.astype(BF16), values[p], preferred_element_type=F32)
                outs.append(mix / total)
            mixed[row, p * pair : (p + 1) * pair] = jnp.where(
                plain_lane < VDIM, outs[0], outs[1]
            ).astype(BF16)
        return carry

    lax.fori_loop(0, rows // tile, step, 0)

    fetch.wait()
    place_count = 1 << tp_bits
    block_rows = rows // place_count
    me = ids[0]
    middle = place_count // 2
    for target, low in ((send, middle), (keep, 0)):
        parts = [
            mixed[
                pl.ds(
                    pl.multiple_of((me ^ spread(low + i, tp_bits)) * block_rows, block_rows),
                    block_rows,
                ),
                :,
            ]
            for i in range(middle)
        ]
        target[...] = jnp.dot(
            jnp.concatenate(parts, axis=0), output_weight[...], preferred_element_type=F32
        ).astype(BF16)


def attention(
    ids, plain, turned, cosine, sine, key_weight, value_weight, output_weight, pieces,
    turn_width, tp_bits,
):
    rows = plain.shape[0]
    head_count = key_weight.shape[1] // NOPE
    key_rows = sum(p.shape[0] for p in pieces)
    turn_lanes = turned.shape[1]
    width = output_weight.shape[1]
    shape = jax.ShapeDtypeStruct((rows // 2, width), BF16)
    return pl.pallas_call(
        functools.partial(attention_kernel, turn_width, len(pieces), tp_bits),
        out_shape=(shape, shape, jax.ShapeDtypeStruct((len(pieces) // 2 - 1, 8, rows), F32)),
        in_specs=[SMEM_SPEC] + [VMEM_SPEC] * 6 + [HBM_SPEC] + [VMEM_SPEC] * len(pieces),
        out_specs=(VMEM_SPEC,) * 3,
        scratch_shapes=[
            pltpu.VMEM((head_count // 2, key_rows, 2 * NOPE + turn_lanes), BF16),
            pltpu.VMEM((head_count // 2, key_rows, 2 * VDIM), BF16),
            pltpu.VMEM((rows, head_count * VDIM), BF16),
            pltpu.VMEM(output_weight.shape, BF16),
            pltpu.SemaphoreType.DMA,
        ],
        compiler_params=params(26 if key_rows <= 2048 else 60),
        cost_estimate=cost(4e12 * 12e-6, 40e6),
        name="attention",
    )(
        ids, plain, turned, cosine, sine, key_weight, value_weight, output_weight, *pieces
    )


def experts_kernel(
    names, group_count, capacity, tp_bits, ids, gate, up, down, own_meta, metas, *rest
):
    blocks = len(names)
    pieces = rest[: 2 * blocks]
    keep, send, slots, loads, gathered = rest[2 * blocks :]
    local_count = gate.shape[0]
    tokens = own_meta.shape[1]
    half = tokens // 2
    me, core, group = ids[0], ids[1], ids[2]

    before = (
        lax.broadcasted_iota(jnp.int32, (tokens, tokens), 0)
        < lax.broadcasted_iota(jnp.int32, (tokens, tokens), 1)
    ).astype(BF16)
    row = lax.broadcasted_iota(jnp.int32, (8, tokens), 0)
    wanted = (row + group * local_count).astype(F32)
    for b in range(blocks):
        meta = own_meta[...] if names[b] == 0 else metas[names[b] - 1]
        first = meta[0:1, :] == wanted
        second = meta[1:2, :] == wanted
        named = (first | second) & (row < local_count)
        rank = jnp.dot(named.astype(BF16), before, preferred_element_type=F32)
        slots[b] = jnp.where(named, rank, -1.0)
        loads[b] = jnp.where(first, meta[2:3, :] + meta[4:5, :] + meta[6:7, :], 0.0) + jnp.where(
            second, meta[3:4, :] + meta[5:6, :] + meta[7:8, :], 0.0
        )

    own = pl.multiple_of(core * half, half)
    far = pl.multiple_of((1 - core) * half, half)
    place = lax.broadcasted_iota(jnp.int32, (capacity, half), 0).astype(F32)
    place_count = 1 << tp_bits
    part = down.shape[2] // place_count
    for j in range(local_count):
        scale = []
        for b in range(blocks):
            hits, weight = [], None
            for offset in (own, far):
                hit = place == slots[b, j : j + 1, pl.ds(offset, half)]
                load = jnp.where(hit, loads[b, j : j + 1, pl.ds(offset, half)], 0.0)
                load = jnp.sum(load, axis=1, keepdims=True)
                weight = load if weight is None else weight + load
                hits.append(jnp.where(hit, 1.0, 0.0).astype(BF16))
            block = jnp.concatenate([pieces[2 * b][...], pieces[2 * b + 1][...]], axis=0)
            gathered[b * capacity : (b + 1) * capacity, :] = jnp.dot(
                jnp.concatenate(hits, axis=1), block, preferred_element_type=F32
            ).astype(BF16)
            scale.append(weight)
        rows_in = gathered[...]
        gate_acts = jnp.dot(rows_in, gate[j], preferred_element_type=F32)
        up_acts = jnp.dot(rows_in, up[j], preferred_element_type=F32)
        hidden = (gate_acts * (1.0 / (1.0 + jnp.exp(-gate_acts))) * up_acts).astype(BF16)
        for target, low in ((send, place_count // 2), (keep, 0)):
            for i in range(place_count // 2):
                column = pl.multiple_of((me ^ spread(low + i, tp_bits)) * part, part)
                product = jnp.dot(
                    hidden, down[j, :, pl.ds(column, part)], preferred_element_type=F32
                )
                for b in range(blocks):
                    base = pl.multiple_of(
                        (ids[3 + group_count + names[b]] * local_count + j) * capacity, capacity
                    )
                    target[pl.ds(base, capacity), i * part : (i + 1) * part] = (
                        product[b * capacity : (b + 1) * capacity, :] * scale[b]
                    ).astype(BF16)


def run_experts(
    ids, names, own_meta, metas, pieces, gate_weight, up_weight, down_weight, capacity, tp_bits
):
    local_count, width, _ = gate_weight.shape
    count = len(names)
    tokens = own_meta.shape[1]
    rows = count * local_count * capacity
    shape = jax.ShapeDtypeStruct((rows, width // 2), BF16)
    return pl.pallas_call(
        functools.partial(
            experts_kernel, tuple(names), metas.shape[0] + 1, capacity, tp_bits
        ),
        out_shape=(shape, shape),
        in_specs=[SMEM_SPEC] + [VMEM_SPEC] * (5 + 2 * count),
        out_specs=(VMEM_SPEC, VMEM_SPEC),
        scratch_shapes=[
            pltpu.VMEM((count, 8, tokens), F32),
            pltpu.VMEM((count, 8, tokens), F32),
            pltpu.VMEM((count * capacity, width), BF16),
        ],
        compiler_params=params(min(60, 18 + 4 * count)),
        cost_estimate=cost(4e12 * 5e-6 * count, 14e6 * count),
        name="experts",
    )(ids, gate_weight, up_weight, down_weight, own_meta, metas, *pieces)


def combine_kernel(starts, pick, *rest):
    out = rest[-1]
    count = len(starts)
    total = None
    for start, part in zip(starts, rest[:count]):
        span = part.shape[0]
        found = jnp.dot(pick[:, start : start + span], part[...], preferred_element_type=F32)
        total = found if total is None else total + found
    for carry in rest[count:-1]:
        total = total + carry[...].astype(F32)
    out[...] = total.astype(BF16)


def combine(pick, parts, carries):
    tokens = pick.shape[0]
    names = sorted(parts)
    span, width = parts[names[0]].shape
    operands = [parts[r] for r in names] + list(carries)
    return pl.pallas_call(
        functools.partial(combine_kernel, tuple(r * span for r in names)),
        out_shape=jax.ShapeDtypeStruct((tokens, width), BF16),
        in_specs=[VMEM_SPEC] * (1 + len(operands)),
        out_specs=VMEM_SPEC,
        compiler_params=params(24),
        cost_estimate=cost(4e12 * 1e-6, 4e6),
        name="combine",
    )(pick, *operands)


def low_bit(value):
    return value & -value


def reverse_bits(value, bits):
    return sum(((value >> b) & 1) << (bits - 1 - b) for b in range(bits))


def step_over(value, bit, ep_bits):
    groups, parts = lax.axis_size("ep"), lax.axis_size("tp")
    pairs = []
    for e in range(groups):
        for t in range(parts):
            mask = 1 << (bit if t % 2 == 0 else ep_bits - 1 - bit)
            pairs.append((e * parts + t, (e ^ mask) * parts + t))
    return lax.ppermute(value, ("ep", "tp"), pairs)


def add_wide(left, right):
    return (left.astype(F32) + right.astype(F32)).astype(BF16)


def local(
    query_latent,
    joint_latent,
    rotary_key,
    query_gain,
    joint_gain,
    query_weight,
    query_rotary,
    key_weight,
    value_weight,
    output_weight,
    expert_input,
    expert_gain,
    routes,
    route_weight,
    gate_weight,
    up_weight,
    down_weight,
):
    group_count = lax.axis_size("ep")
    part_count = lax.axis_size("tp")
    ep_bits, tp_bits = bits_of(group_count), bits_of(part_count)
    ep, tp = lax.axis_index("ep"), lax.axis_index("tp")
    core = tp & 1
    names = range(group_count)
    groups = [ep ^ jnp.where(core == 0, n, reverse_bits(n, ep_bits)) for n in names]
    near = [n for n in names if bin(n).count("1") <= 1]
    far = [n for n in names if n not in near]
    classes = [near] + ([far] if far else [])
    place = {n: c.index(n) for c in classes for n in c}
    orders = [jnp.where(core == 0, place[n], place[reverse_bits(n, ep_bits)]) for n in names]
    ids = jnp.stack([tp, core, ep] + groups + orders).astype(jnp.int32)
    rows = query_latent.shape[0]
    turn_width = rotary_key.shape[1]
    local_count = gate_weight.shape[0]
    tokens = expert_input.shape[0]
    capacity = 3 * tokens // (2 * group_count)
    half_width = turn_width // 2

    latent_mine, latent_other, own_meta, row_mine, row_other = prepare(
        ids, joint_latent, joint_gain, rotary_key, routes, route_weight, expert_input,
        expert_gain,
    )
    latent_held = {0: latent_mine}
    for b in range(ep_bits):
        latent_held[1 << b] = step_over(latent_mine, b, ep_bits)
    row_held = {0: row_mine, 1: step_over(row_mine, 0, ep_bits)}

    positions = jnp.arange(rows * group_count, dtype=jnp.int32).astype(F32)
    frequencies = ROTARY_BASE ** (-jnp.arange(half_width, dtype=F32) / half_width)
    angles = frequencies[:, None] * positions[None, :]
    cosine, sine = jnp.cos(angles), jnp.sin(angles)
    plain, turned, pick = queries(
        ids, query_latent, query_gain, query_weight, query_rotary, cosine,
        sine, routes, turn_width, local_count, capacity, group_count,
    )
    for n in far:
        b = n.bit_length() - 1
        latent_held[n] = step_over(latent_held[n ^ (1 << b)], b, ep_bits)
    for b in range(1, ep_bits):
        row_held[1 << b] = step_over(row_mine, b, ep_bits)

    def with_other(values, own_other):
        swapped = {n: swap_over(values[n], "tp", 1) for n in names if n}
        return {
            n: [values[n], swapped[reverse_bits(n, ep_bits)] if n else own_other] for n in names
        }

    latents = with_other(latent_held, latent_other)
    keep, send, metas = attention(
        ids, plain, turned, cosine, sine, key_weight, value_weight, output_weight,
        [piece for n in names for piece in latents[n]], turn_width, tp_bits,
    )
    for n in far:
        b = n.bit_length() - 1
        row_held[n] = step_over(row_held[n ^ (1 << b)], b, ep_bits)
    arrived = swap_over(send, "tp", 1)
    for b in range(1, tp_bits):
        cut = keep.shape[0] // 2
        away = add_wide(keep[cut:], arrived[cut:])
        keep = add_wide(keep[:cut], arrived[:cut])
        arrived = swap_over(away, "tp", 1 << b)
    mixer_out = add_wide(keep, arrived)

    row_pairs = with_other(row_held, row_other)
    parts = {}
    span = local_count * capacity
    chunk_count = part_count // 2
    width = expert_input.shape[1] // part_count
    gathered = {}
    for chosen in classes:
        keep, send = run_experts(
            ids, chosen, own_meta, metas, [piece for n in chosen for piece in row_pairs[n]],
            gate_weight, up_weight, down_weight, capacity, tp_bits,
        )
        arrived = swap_over(send, "tp", 1)
        if chosen == near:
            both = add_wide(keep, arrived)
            for i, r in enumerate(chosen):
                for c in range(chunk_count):
                    parts[r, c] = both[i * span : (i + 1) * span, c * width : (c + 1) * width]
        else:
            for b in range(1, tp_bits):
                cut = keep.shape[1] // 2
                away = add_wide(keep[:, cut:], arrived[:, cut:])
                keep = add_wide(keep[:, :cut], arrived[:, :cut])
                arrived = swap_over(away, "tp", 1 << b)
            both = add_wide(keep, arrived)
            for i, r in enumerate(chosen):
                gathered[r] = swap_over(both[i * span : (i + 1) * span], "ep", r)

    carried = {}
    for c in sorted(range(chunk_count), key=lambda i: -spread(i, tp_bits)):
        mask = spread(c, tp_bits)
        found = {r: swap_over(parts[r, c], "ep", r) if r else parts[r, c] for r in near}
        if not mask:
            found.update(gathered)
        total = combine(pick, found, carried.pop(mask, []))
        if mask:
            arrived = swap_over(total, "tp", low_bit(mask))
            carried.setdefault(mask ^ low_bit(mask), []).append(arrived)
    expert_out = total
    return (mixer_out, expert_out)


def solution(mesh):
    return jax.shard_map(
        local,
        mesh=mesh,
        in_specs=(
            P("ep", None),
            P("ep", None),
            P("ep", None),
            P(),
            P(),
            P(None, "tp"),
            P(None, "tp"),
            P(None, "tp"),
            P(None, "tp"),
            P("tp", None),
            P("ep", None),
            P(),
            P("ep", None),
            P("ep", None),
            P("ep", None, "tp"),
            P("ep", None, "tp"),
            P("ep", "tp", None),
        ),
        out_specs=(P(("ep", "tp"), None), P("ep", "tp")),
        check_vma=False,
    )
```

profile of v0, /device:TPU:0, one launch (start us, length us, event | category | flops | bytes accessed | tf_op | source)
XLA Modules:
  0.0 172.8 jit_solution(2987413173988388024)
XLA Ops:
  1.2 4.7 %prepare.1 = (bf16[256,640]{1,0:T(8,128)(2,1)}, bf16[256,640]{1,0:T(8,128)(2,1)}, f32[8,512]{1,0:T(8,128)}, bf16[256,2048]{1,0:T(8,128)(2,1)}, bf16[256,2048]{1,0:T(8,128)(2,1)}) custom-call(s32[11]{0:T(128)} %stack.38.ids, bf16[512,512]{1,0:T(8,128)(2,1)} %joint_hbm.1, f32[1,512]{1,0:T(1,128)} %bitcast.20, bf16[32,512]{1,0:T(8,128)(2,1)} %bitcast.14, ...), custom_call_target="tpu_custom_call" | custom-call | flops 12000000 | bytes 4000000 | tf_op jit(solution)/shard_map/prepare/pallas_call | solution.py:137
  6.0 3.1 %collective-permute-start.10 = (bf16[256,2048]{1,0:T(8,128)(2,1)}, bf16[256,2048]{1,0:T(8,128)(2,1)}, u32[]{:S(2)}, u32[]{:S(2)}) collective-permute-start(bf16[256,2048]{1,0:T(8,128)(2,1)} %get-tuple-element.26.rest_0_), channel_id=1, source_target_pairs={{0,16},{1,9},{2,18},{3,11},{4,20},{5,13},{6,22},{7,15},{8,24},{9,1... | collective-permute-start | bytes 3145736 | tf_op jit(solution)/shard_map/ppermute | solution.py:489
  9.0 1.5 collective-permute-start.9
  11.1 21.7 %collective-permute-done.10.rest_4_ = bf16[256,2048]{1,0:T(8,128)(2,1)} collective-permute-done((bf16[256,2048]{1,0:T(8,128)(2,1)}, bf16[256,2048]{1,0:T(8,128)(2,1)}, u32[]{:S(2)}, u32[]{:S(2)}) %collective-permute-start.10) | collective-permute-done | bytes 1048608 | tf_op jit(solution)/shard_map/ppermute | solution.py:489
  32.8 2.6 %collective-permute-done.9.rest_2_ = bf16[256,2048]{1,0:T(8,128)(2,1)} collective-permute-done((bf16[256,2048]{1,0:T(8,128)(2,1)}, bf16[256,2048]{1,0:T(8,128)(2,1)}, u32[]{:S(2)}, u32[]{:S(2)}) %collective-permute-start.9) | collective-permute-done | bytes 1048608 | tf_op jit(solution)/shard_map/ppermute | solution.py:489
  35.4 4.5 %collective-permute-done.1.rest_4_ = bf16[256,640]{1,0:T(8,128)(2,1)S(1)} collective-permute-done((bf16[256,640]{1,0:T(8,128)(2,1)}, bf16[256,640]{1,0:T(8,128)(2,1)S(1)}, u32[]{:S(2)}, u32[]{:S(2)}) %collective-permute-start.1) | collective-permute-done | bytes 327712 | tf_op jit(solution)/shard_map/ppermute | solution.py:489
  39.8 2.4 %collective-permute-start.4 = (bf16[256,640]{1,0:T(8,128)(2,1)S(1)}, bf16[256,640]{1,0:T(8,128)(2,1)}, u32[]{:S(2)}, u32[]{:S(2)}) collective-permute-start(bf16[256,640]{1,0:T(8,128)(2,1)S(1)} %collective-permute-done.rest_2_), channel_id=1, source_target_pairs={{0,16},{1,9},{2,18},{3,11},{4,20},{5,13},{6,22},{7,15},{8,24},{9,1... | collective-permute-start | bytes 983048 | tf_op jit(solution)/shard_map/ppermute | solution.py:489
  42.4 5.0 %collective-permute-done.4.rest_6_ = bf16[256,640]{1,0:T(8,128)(2,1)} collective-permute-done((bf16[256,640]{1,0:T(8,128)(2,1)S(1)}, bf16[256,640]{1,0:T(8,128)(2,1)}, u32[]{:S(2)}, u32[]{:S(2)}) %collective-permute-start.4) | collective-permute-done | bytes 327712 | tf_op jit(solution)/shard_map/ppermute | solution.py:489
  47.4 1.2 multiply_sine_fusion
  48.6 4.3 %queries.1 = (bf16[512,256]{1,0:T(8,128)(2,1)}, bf16[512,128]{1,0:T(8,128)(2,1)}, bf16[512,1536]{1,0:T(8,128)(2,1)}) custom-call(s32[11]{0:T(128)} %stack.38.ids, bf16[512,1024]{1,0:T(8,128)(2,1)} %query_latent.1, f32[1,1024]{1,0:T(1,128)} %bitcast.19, bf16[1024,256]{1,0:T(8,128)(2,1)} %query_weight.1, bf16[1024,128]{1,0:T(8,128)(2,1)} %query_rotary.1, ...), custom_call_target="tpu_custom_call" | custom-call | flops 16000000 | bytes 12000000 | tf_op jit(solution)/shard_map/queries/pallas_call | solution.py:212
  53.0 0.9 copy-done.6
  53.9 0.9 copy-done.7
  54.8 1.0 copy-done.11
  55.7 1.0 copy-done.12
  56.7 0.9 copy-done.13
  57.7 0.9 copy-done.14
  58.6 0.9 copy-done.15
  59.6 0.9 copy-done.18
  61.1 11.1 %attention.1 = (bf16[256,2048]{1,0:T(8,128)(2,1)S(1)}, bf16[256,2048]{1,0:T(8,128)(2,1)S(1)}, f32[3,8,512]{2,1,0:T(8,128)S(1)}) custom-call(s32[11]{0:T(128)S(1)} %copy-done.20, bf16[512,256]{1,0:T(8,128)(2,1)S(1)} %copy-done.15, bf16[512,128]{1,0:T(8,128)(2,1)S(1)} %copy-done.18, f32[16,2048]{1,0:T(8,128)S(1)} %copy-done.7, f32[16,2048]{1,0:T(8,128)S(1)} %copy-done.6, ...), custom_call_target="tpu_custom_call" | custom-call | flops 48000000 | bytes 40000000 | tf_op jit(solution)/shard_map/attention/pallas_call | solution.py:332
  72.8 1.0 copy-done.22
  73.8 2.2 %copy-done.2 = bf16[2,2048,512]{2,1,0:T(8,128)(2,1)S(1)} copy-done((bf16[2,2048,512]{2,1,0:T(8,128)(2,1)S(1)}, bf16[2,2048,512]{2,1,0:T(8,128)(2,1)}, u32[]{:S(2)}) %copy-start.2) | copy-done | bytes 4194328
  75.9 2.2 %copy-done.4 = bf16[2,512,2048]{2,1,0:T(8,128)(2,1)S(1)} copy-done((bf16[2,512,2048]{2,1,0:T(8,128)(2,1)S(1)}, bf16[2,512,2048]{2,1,0:T(8,128)(2,1)}, u32[]{:S(2)}) %copy-start.4) | copy-done | bytes 4194328
  78.1 0.8 copy-done.17
  78.9 0.7 copy-done.19
  80.3 14.3 %experts.2 = (bf16[1152,1024]{1,0:T(8,128)(2,1)S(1)}, bf16[1152,1024]{1,0:T(8,128)(2,1)}) custom-call(s32[11]{0:T(128)S(1)} %copy-done.21, bf16[2,2048,512]{2,1,0:T(8,128)(2,1)S(1)} %copy-done.1, bf16[2,2048,512]{2,1,0:T(8,128)(2,1)S(1)} %copy-done.2, bf16[2,512,2048]{2,1,0:T(8,128)(2,1)S(1)} %copy-done.4, f32[8,512]{1,0:T(8,128)S(1)} %copy-done.19, ...), custom_call_target="tpu_custom_call" | custom-call | flops 60000000 | bytes 42000000 | tf_op jit(solution)/shard_map/experts/pallas_call | solution.py:427
  95.6 5.4 %collective-permute-done.17.rest_1_ = bf16[256,2048]{1,0:T(8,128)(2,1)S(1)} collective-permute-done((bf16[256,2048]{1,0:T(8,128)(2,1)}, bf16[256,2048]{1,0:T(8,128)(2,1)S(1)}, u32[]{:S(2)}, u32[]{:S(2)}) %collective-permute-start.17) | collective-permute-done | bytes 1048608 | tf_op jit(solution)/shard_map/ppermute | solution.py:37
  100.9 5.4 %experts.3 = (bf16[384,1024]{1,0:T(8,128)(2,1)S(1)}, bf16[384,1024]{1,0:T(8,128)(2,1)S(1)}) custom-call(s32[11]{0:T(128)S(1)} %copy-done.21, bf16[2,2048,512]{2,1,0:T(8,128)(2,1)S(1)} %copy-done.1, bf16[2,2048,512]{2,1,0:T(8,128)(2,1)S(1)} %copy-done.3, bf16[2,512,2048]{2,1,0:T(8,128)(2,1)S(1)} %copy-done.5, f32[8,512]{1,0:T(8,128)S(1)} %copy-done.19, ...), custom_call_target="tpu_custom_call" | custom-call | flops 20000000 | bytes 14000000 | tf_op jit(solution)/shard_map/experts/pallas_call | solution.py:427
  107.2 2.1 %collective-permute-start.7 = (bf16[128,2048]{1,0:T(8,128)(2,1)S(1)}, bf16[128,2048]{1,0:T(8,128)(2,1)S(1)}, u32[]{:S(2)}, u32[]{:S(2)}) collective-permute-start(bf16[128,2048]{1,0:T(8,128)(2,1)S(1)} %get-tuple-element.45), channel_id=1, source_target_pairs={{0,2},{1,3},{2,0},{3,1},{4,6},{5,7},{6,4},{7,5},{8,10},{9,11},{10,... | collective-permute-start | bytes 1572872 | tf_op jit(solution)/shard_map/ppermute | solution.py:37
  109.5 1.5 collective-permute-start.19
  111.1 1.1 add_convert_fusion
  112.4 0.7 collective-permute-start.24
  113.2 1.5 collective-permute-start.25
  114.7 15.2 %collective-permute-done.19 = bf16[384,512]{1,0:T(8,128)(2,1)S(1)} collective-permute-done((bf16[384,512]{1,0:T(8,128)(2,1)S(1)}, bf16[384,512]{1,0:T(8,128)(2,1)S(1)}, u32[]{:S(2)}, u32[]{:S(2)}) %collective-permute-start.19) | collective-permute-done | bytes 393248 | tf_op jit(solution)/shard_map/ppermute | solution.py:37
  130.0 2.8 %collective-permute-start.20 = (bf16[384,256]{1,0:T(8,128)(2,1)S(1)}, bf16[384,256]{1,0:T(8,128)(2,1)S(1)}, u32[]{:S(2)}, u32[]{:S(2)}) collective-permute-start(bf16[384,256]{1,0:T(8,128)(2,1)S(1)} %add_convert_fusion.9), channel_id=1, source_target_pairs={{0,4},{1,5},{2,6},{3,7},{4,0},{5,1},{6,2},{7,3},{8,12},{9,13},{10,... | collective-permute-start | bytes 589832 | tf_op jit(solution)/shard_map/ppermute | solution.py:37
  132.8 0.7 collective-permute-start.28
  134.1 1.6 collective-permute-start.26
  136.2 1.4 collective-permute-start.22
  137.6 5.4 %collective-permute-done.20 = bf16[384,256]{1,0:T(8,128)(2,1)S(1)} collective-permute-done((bf16[384,256]{1,0:T(8,128)(2,1)S(1)}, bf16[384,256]{1,0:T(8,128)(2,1)S(1)}, u32[]{:S(2)}, u32[]{:S(2)}) %collective-permute-start.20) | collective-permute-done | bytes 196640 | tf_op jit(solution)/shard_map/ppermute | solution.py:37
  142.9 1.5 collective-permute-start.23
  145.0 6.6 %collective-permute-done.29.rest_2_ = bf16[384,256]{1,0:T(8,128)(2,1)S(1)} collective-permute-done((bf16[384,256]{1,0:T(8,128)(2,1)S(1)}, bf16[384,256]{1,0:T(8,128)(2,1)S(1)}, u32[]{:S(2)}, u32[]{:S(2)}) %collective-permute-start.29) | collective-permute-done | bytes 196640 | tf_op jit(solution)/shard_map/ppermute | solution.py:37
  152.6 1.6 collective-permute-start.15
  154.2 1.6 collective-permute-start.21
  155.8 1.5 collective-permute-start.30
  157.9 3.7 %collective-permute-start.27 = (bf16[512,256]{1,0:T(8,128)(2,1)S(1)}, bf16[512,256]{1,0:T(8,128)(2,1)S(1)}, u32[]{:S(2)}, u32[]{:S(2)}) collective-permute-start(bf16[512,256]{1,0:T(8,128)(2,1)S(1)} %combine.5), channel_id=1, source_target_pairs={{0,4},{1,5},{2,6},{3,7},{4,0},{5,1},{6,2},{7,3},{8,12},{9,13},{10,... | collective-permute-start | bytes 786440 | tf_op jit(solution)/shard_map/ppermute | solution.py:37
  161.5 0.8 add_convert_fusion.5
  162.3 3.9 %collective-permute-done.30.rest_5_ = bf16[512,256]{1,0:T(8,128)(2,1)S(1)} collective-permute-done((bf16[512,256]{1,0:T(8,128)(2,1)S(1)}, bf16[512,256]{1,0:T(8,128)(2,1)S(1)}, u32[]{:S(2)}, u32[]{:S(2)}) %collective-permute-start.30) | collective-permute-done | bytes 262176 | tf_op jit(solution)/shard_map/ppermute | solution.py:37
  166.2 5.2 %collective-permute-done.27.rest_4_ = bf16[512,256]{1,0:T(8,128)(2,1)S(1)} collective-permute-done((bf16[512,256]{1,0:T(8,128)(2,1)S(1)}, bf16[512,256]{1,0:T(8,128)(2,1)S(1)}, u32[]{:S(2)}, u32[]{:S(2)}) %collective-permute-start.27) | collective-permute-done | bytes 262176 | tf_op jit(solution)/shard_map/ppermute | solution.py:37
  171.4 1.4 combine.7
  (83 shorter events, 8.7 us)
Async XLA Ops:
  1.2 51.7 %copy-start.8 = (bf16[256,2048]{1,0:T(8,128)(2,1)S(1)}, bf16[256,2048]{1,0:T(8,128)(2,1)}, u32[]{:S(2)}) copy-start(bf16[256,2048]{1,0:T(8,128)(2,1)} %output_hbm.1) | copy-start | bytes 3145732
  6.0 26.9 %collective-permute-start.10 = (bf16[256,2048]{1,0:T(8,128)(2,1)}, bf16[256,2048]{1,0:T(8,128)(2,1)}, u32[]{:S(2)}, u32[]{:S(2)}) collective-permute-start(bf16[256,2048]{1,0:T(8,128)(2,1)} %get-tuple-element.26.rest_0_), channel_id=1, source_target_pairs={{0,16},{1,9},{2,18},{3,11},{4,20},{5,13},{6,22},{7,15},{8,24},{9,1... | collective-permute-start | bytes 3145736 | tf_op jit(solution)/shard_map/ppermute | solution.py:489
  9.0 26.3 %collective-permute-start.9 = (bf16[256,2048]{1,0:T(8,128)(2,1)}, bf16[256,2048]{1,0:T(8,128)(2,1)}, u32[]{:S(2)}, u32[]{:S(2)}) collective-permute-start(bf16[256,2048]{1,0:T(8,128)(2,1)} %get-tuple-element.26.rest_0_), channel_id=1, source_target_pairs={{0,8},{1,17},{2,10},{3,19},{4,12},{5,21},{6,14},{7,23},{8,0},{9,25... | collective-permute-start | bytes 3145736 | tf_op jit(solution)/shard_map/ppermute | solution.py:489
  10.5 29.3 %collective-permute-start.1 = (bf16[256,640]{1,0:T(8,128)(2,1)}, bf16[256,640]{1,0:T(8,128)(2,1)S(1)}, u32[]{:S(2)}, u32[]{:S(2)}) collective-permute-start(bf16[256,640]{1,0:T(8,128)(2,1)} %get-tuple-element.19.rest_0_), channel_id=1, source_target_pairs={{0,16},{1,9},{2,18},{3,11},{4,20},{5,13},{6,22},{7,15},{8,24},{9,1... | collective-permute-start | bytes 983048 | tf_op jit(solution)/shard_map/ppermute | solution.py:489
  11.0 28.8 %collective-permute-start = (bf16[256,640]{1,0:T(8,128)(2,1)}, bf16[256,640]{1,0:T(8,128)(2,1)S(1)}, u32[]{:S(2)}, u32[]{:S(2)}) collective-permute-start(bf16[256,640]{1,0:T(8,128)(2,1)} %get-tuple-element.19.rest_0_), channel_id=1, source_target_pairs={{0,8},{1,17},{2,10},{3,19},{4,12},{5,21},{6,14},{7,23},{8,0},{9,25... | collective-permute-start | bytes 983048 | tf_op jit(solution)/shard_map/ppermute | solution.py:489
  32.8 40.9 %collective-permute-start.11 = (bf16[256,2048]{1,0:T(8,128)(2,1)}, bf16[256,2048]{1,0:T(8,128)(2,1)}, u32[]{:S(2)}, u32[]{:S(2)}) collective-permute-start(bf16[256,2048]{1,0:T(8,128)(2,1)} %collective-permute-done.10.rest_4_), channel_id=1, source_target_pairs={{0,1},{1,0},{2,3},{3,2},{4,5},{5,4},{6,7},{7,6},{8,9},{9,8},{10,11... | collective-permute-start | bytes 3145736 | tf_op jit(solution)/shard_map/ppermute | solution.py:37
  35.4 38.4 %collective-permute-start.12 = (bf16[256,2048]{1,0:T(8,128)(2,1)}, bf16[256,2048]{1,0:T(8,128)(2,1)}, u32[]{:S(2)}, u32[]{:S(2)}) collective-permute-start(bf16[256,2048]{1,0:T(8,128)(2,1)} %collective-permute-done.9.rest_2_), channel_id=1, source_target_pairs={{0,1},{1,0},{2,3},{3,2},{4,5},{5,4},{6,7},{7,6},{8,9},{9,8},{10,11... | collective-permute-start | bytes 3145736 | tf_op jit(solution)/shard_map/ppermute | solution.py:37
  39.8 2.5 %collective-permute-start.2 = (bf16[256,640]{1,0:T(8,128)(2,1)S(1)}, bf16[256,640]{1,0:T(8,128)(2,1)S(1)}, u32[]{:S(2)}, u32[]{:S(2)}) collective-permute-start(bf16[256,640]{1,0:T(8,128)(2,1)S(1)} %collective-permute-done.1.rest_4_), channel_id=1, source_target_pairs={{0,1},{1,0},{2,3},{3,2},{4,5},{5,4},{6,7},{7,6},{8,9},{9,8},{10,11... | collective-permute-start | bytes 983048 | tf_op jit(solution)/shard_map/ppermute | solution.py:37
  39.8 7.5 %collective-permute-start.4 = (bf16[256,640]{1,0:T(8,128)(2,1)S(1)}, bf16[256,640]{1,0:T(8,128)(2,1)}, u32[]{:S(2)}, u32[]{:S(2)}) collective-permute-start(bf16[256,640]{1,0:T(8,128)(2,1)S(1)} %collective-permute-done.rest_2_), channel_id=1, source_target_pairs={{0,16},{1,9},{2,18},{3,11},{4,20},{5,13},{6,22},{7,15},{8,24},{9,1... | collective-permute-start | bytes 983048 | tf_op jit(solution)/shard_map/ppermute | solution.py:489
  42.2 52.8 %collective-permute-start.16 = (bf16[256,2048]{1,0:T(8,128)(2,1)}, bf16[256,2048]{1,0:T(8,128)(2,1)}, u32[]{:S(2)}, u32[]{:S(2)}) collective-permute-start(bf16[256,2048]{1,0:T(8,128)(2,1)} %collective-permute-done.9.rest_2_), channel_id=1, source_target_pairs={{0,16},{1,9},{2,18},{3,11},{4,20},{5,13},{6,22},{7,15},{8,24},{9,1... | collective-permute-start | bytes 3145736 | tf_op jit(solution)/shard_map/ppermute | solution.py:489
  42.3 10.6 %collective-permute-start.3 = (bf16[256,640]{1,0:T(8,128)(2,1)S(1)}, bf16[256,640]{1,0:T(8,128)(2,1)}, u32[]{:S(2)}, u32[]{:S(2)}) collective-permute-start(bf16[256,640]{1,0:T(8,128)(2,1)S(1)} %collective-permute-done.rest_2_), channel_id=1, source_target_pairs={{0,1},{1,0},{2,3},{3,2},{4,5},{5,4},{6,7},{7,6},{8,9},{9,8},{10,11... | collective-permute-start | bytes 983048 | tf_op jit(solution)/shard_map/ppermute | solution.py:37
  47.4 5.6 %collective-permute-start.5 = (bf16[256,640]{1,0:T(8,128)(2,1)}, bf16[256,640]{1,0:T(8,128)(2,1)}, u32[]{:S(2)}, u32[]{:S(2)}) collective-permute-start(bf16[256,640]{1,0:T(8,128)(2,1)} %collective-permute-done.4.rest_6_), channel_id=1, source_target_pairs={{0,1},{1,0},{2,3},{3,2},{4,5},{5,4},{6,7},{7,6},{8,9},{9,8},{10,11... | collective-permute-start | bytes 983048 | tf_op jit(solution)/shard_map/ppermute | solution.py:37
  48.6 25.1 %copy-start.9 = (bf16[256,2048]{1,0:T(8,128)(2,1)S(1)}, bf16[256,2048]{1,0:T(8,128)(2,1)}, u32[]{:S(2)}) copy-start(bf16[256,2048]{1,0:T(8,128)(2,1)} %get-tuple-element.26.rest_0_) | copy-start | bytes 3145732
  48.6 25.1 %copy-start.10 = (bf16[256,2048]{1,0:T(8,128)(2,1)S(1)}, bf16[256,2048]{1,0:T(8,128)(2,1)}, u32[]{:S(2)}) copy-start(bf16[256,2048]{1,0:T(8,128)(2,1)} %get-tuple-element.27.rest_1_) | copy-start | bytes 3145732
  53.0 0.9 copy-start.6
  54.8 1.0 copy-start.11
  55.7 1.0 copy-start.12
  56.7 0.9 copy-start.13
  57.7 0.9 copy-start.14
  58.6 0.9 copy-start.15
  61.1 12.7 %copy-start.1 = (bf16[2,2048,512]{2,1,0:T(8,128)(2,1)S(1)}, bf16[2,2048,512]{2,1,0:T(8,128)(2,1)}, u32[]{:S(2)}) copy-start(bf16[2,2048,512]{2,1,0:T(8,128)(2,1)} %gate.3) | copy-start | bytes 12582916
  72.8 1.0 copy-start.22
  73.8 2.2 %copy-start.2 = (bf16[2,2048,512]{2,1,0:T(8,128)(2,1)S(1)}, bf16[2,2048,512]{2,1,0:T(8,128)(2,1)}, u32[]{:S(2)}) copy-start(bf16[2,2048,512]{2,1,0:T(8,128)(2,1)} %up.3) | copy-start | bytes 12582916
  75.9 2.2 %copy-start.4 = (bf16[2,512,2048]{2,1,0:T(8,128)(2,1)S(1)}, bf16[2,512,2048]{2,1,0:T(8,128)(2,1)}, u32[]{:S(2)}) copy-start(bf16[2,512,2048]{2,1,0:T(8,128)(2,1)} %down.3) | copy-start | bytes 12582916
  80.2 14.9 %copy-start.23 = (bf16[256,2048]{1,0:T(8,128)(2,1)S(1)}, bf16[256,2048]{1,0:T(8,128)(2,1)}, u32[]{:S(2)}) copy-start(bf16[256,2048]{1,0:T(8,128)(2,1)} %copy-done.22) | copy-start | bytes 3145732
  80.2 20.7 %copy-start.3 = (bf16[2,2048,512]{2,1,0:T(8,128)(2,1)S(1)}, bf16[2,2048,512]{2,1,0:T(8,128)(2,1)}, u32[]{:S(2)}) copy-start(bf16[2,2048,512]{2,1,0:T(8,128)(2,1)} %up.3) | copy-start | bytes 12582916
  80.2 20.7 %copy-start.5 = (bf16[2,512,2048]{2,1,0:T(8,128)(2,1)S(1)}, bf16[2,512,2048]{2,1,0:T(8,128)(2,1)}, u32[]{:S(2)}) copy-start(bf16[2,512,2048]{2,1,0:T(8,128)(2,1)} %down.3) | copy-start | bytes 12582916
  94.5 16.5 %collective-permute-start.13 = (bf16[1152,1024]{1,0:T(8,128)(2,1)}, bf16[1152,1024]{1,0:T(8,128)(2,1)S(1)}, u32[]{:S(2)}, u32[]{:S(2)}) collective-permute-start(bf16[1152,1024]{1,0:T(8,128)(2,1)} %get-tuple-element.29), channel_id=1, source_target_pairs={{0,1},{1,0},{2,3},{3,2},{4,5},{5,4},{6,7},{7,6},{8,9},{9,8},{10,11... | collective-permute-start | bytes 7077896 | tf_op jit(solution)/shard_map/ppermute | solution.py:37
  95.0 5.9 %collective-permute-start.17 = (bf16[256,2048]{1,0:T(8,128)(2,1)}, bf16[256,2048]{1,0:T(8,128)(2,1)S(1)}, u32[]{:S(2)}, u32[]{:S(2)}) collective-permute-start(bf16[256,2048]{1,0:T(8,128)(2,1)} %collective-permute-done.16.rest_0_), channel_id=1, source_target_pairs={{0,1},{1,0},{2,3},{3,2},{4,5},{5,4},{6,7},{7,6},{8,9},{9,8},{10,11... | collective-permute-start | bytes 3145736 | tf_op jit(solution)/shard_map/ppermute | solution.py:37
  95.1 11.7 %collective-permute-start.6 = (bf16[256,2048]{1,0:T(8,128)(2,1)S(1)}, bf16[256,2048]{1,0:T(8,128)(2,1)S(1)}, u32[]{:S(2)}, u32[]{:S(2)}) collective-permute-start(bf16[256,2048]{1,0:T(8,128)(2,1)S(1)} %copy-done.23), channel_id=1, source_target_pairs={{0,1},{1,0},{2,3},{3,2},{4,5},{5,4},{6,7},{7,6},{8,9},{9,8},{10,11... | collective-permute-start | bytes 3145736 | tf_op jit(solution)/shard_map/ppermute | solution.py:37
  106.3 3.0 %collective-permute-start.18 = (bf16[384,1024]{1,0:T(8,128)(2,1)S(1)}, bf16[384,1024]{1,0:T(8,128)(2,1)S(1)}, u32[]{:S(2)}, u32[]{:S(2)}) collective-permute-start(bf16[384,1024]{1,0:T(8,128)(2,1)S(1)} %get-tuple-element.31), channel_id=1, source_target_pairs={{0,1},{1,0},{2,3},{3,2},{4,5},{5,4},{6,7},{7,6},{8,9},{9,8},{10,11... | collective-permute-start | bytes 2359304 | tf_op jit(solution)/shard_map/ppermute | solution.py:37
  107.2 28.5 %collective-permute-start.7 = (bf16[128,2048]{1,0:T(8,128)(2,1)S(1)}, bf16[128,2048]{1,0:T(8,128)(2,1)S(1)}, u32[]{:S(2)}, u32[]{:S(2)}) collective-permute-start(bf16[128,2048]{1,0:T(8,128)(2,1)S(1)} %get-tuple-element.45), channel_id=1, source_target_pairs={{0,2},{1,3},{2,0},{3,1},{4,6},{5,7},{6,4},{7,5},{8,10},{9,11},{10,... | collective-permute-start | bytes 1572872 | tf_op jit(solution)/shard_map/ppermute | solution.py:37
  109.5 20.4 %collective-permute-start.19 = (bf16[384,512]{1,0:T(8,128)(2,1)S(1)}, bf16[384,512]{1,0:T(8,128)(2,1)S(1)}, u32[]{:S(2)}, u32[]{:S(2)}) collective-permute-start(bf16[384,512]{1,0:T(8,128)(2,1)S(1)} %get-tuple-element.47), channel_id=1, source_target_pairs={{0,2},{1,3},{2,0},{3,1},{4,6},{5,7},{6,4},{7,5},{8,10},{9,11},{10,... | collective-permute-start | bytes 1179656 | tf_op jit(solution)/shard_map/ppermute | solution.py:37
  112.2 21.3 %copy-start = (bf16[512,1536]{1,0:T(8,128)(2,1)S(1)}, bf16[512,1536]{1,0:T(8,128)(2,1)}, u32[]{:S(2)}) copy-start(bf16[512,1536]{1,0:T(8,128)(2,1)} %get-tuple-element.23.pick) | copy-start | bytes 4718596
  112.4 21.1 %collective-permute-start.24 = (bf16[384,256]{1,0:T(8,128)(2,1)S(1)}, bf16[384,256]{1,0:T(8,128)(2,1)S(1)}, u32[]{:S(2)}, u32[]{:S(2)}) collective-permute-start(bf16[384,256]{1,0:T(8,128)(2,1)S(1)} %get-tuple-element.36), channel_id=1, source_target_pairs={{0,8},{8,0},{16,24},{24,16},{1,9},{9,1},{17,25},{25,17},{2,10},{10... | collective-permute-start | bytes 589832 | tf_op jit(solution)/shard_map/ppermute | solution.py:37
  113.2 20.3 %collective-permute-start.25 = (bf16[384,256]{1,0:T(8,128)(2,1)S(1)}, bf16[384,256]{1,0:T(8,128)(2,1)S(1)}, u32[]{:S(2)}, u32[]{:S(2)}) collective-permute-start(bf16[384,256]{1,0:T(8,128)(2,1)S(1)} %get-tuple-element.35), channel_id=1, source_target_pairs={{0,16},{8,24},{16,0},{24,8},{1,17},{9,25},{17,1},{25,9},{2,18},{10... | collective-permute-start | bytes 589832 | tf_op jit(solution)/shard_map/ppermute | solution.py:37
  130.0 12.9 %collective-permute-start.20 = (bf16[384,256]{1,0:T(8,128)(2,1)S(1)}, bf16[384,256]{1,0:T(8,128)(2,1)S(1)}, u32[]{:S(2)}, u32[]{:S(2)}) collective-permute-start(bf16[384,256]{1,0:T(8,128)(2,1)S(1)} %add_convert_fusion.9), channel_id=1, source_target_pairs={{0,4},{1,5},{2,6},{3,7},{4,0},{5,1},{6,2},{7,3},{8,12},{9,13},{10,... | collective-permute-start | bytes 589832 | tf_op jit(solution)/shard_map/ppermute | solution.py:37
  132.8 11.6 %collective-permute-start.28 = (bf16[384,256]{1,0:T(8,128)(2,1)S(1)}, bf16[384,256]{1,0:T(8,128)(2,1)S(1)}, u32[]{:S(2)}, u32[]{:S(2)}) collective-permute-start(bf16[384,256]{1,0:T(8,128)(2,1)S(1)} %get-tuple-element.33), channel_id=1, source_target_pairs={{0,8},{8,0},{16,24},{24,16},{1,9},{9,1},{17,25},{25,17},{2,10},{10... | collective-permute-start | bytes 589832 | tf_op jit(solution)/shard_map/ppermute | solution.py:37
  134.1 21.7 %collective-permute-start.26 = (bf16[512,256]{1,0:T(8,128)(2,1)S(1)}, bf16[512,256]{1,0:T(8,128)(2,1)S(1)}, u32[]{:S(2)}, u32[]{:S(2)}) collective-permute-start(bf16[512,256]{1,0:T(8,128)(2,1)S(1)} %combine.4), channel_id=1, source_target_pairs={{0,2},{1,3},{2,0},{3,1},{4,6},{5,7},{6,4},{7,5},{8,10},{9,11},{10,... | collective-permute-start | bytes 786440 | tf_op jit(solution)/shard_map/ppermute | solution.py:37
  135.8 22.1 %collective-permute-start.8 = (bf16[64,2048]{1,0:T(8,128)(2,1)S(1)}, bf16[64,2048]{1,0:T(8,128)(2,1)S(1)}, u32[]{:S(2)}, u32[]{:S(2)}) collective-permute-start(bf16[64,2048]{1,0:T(8,128)(2,1)S(1)} %add_convert_fusion.6), channel_id=1, source_target_pairs={{0,4},{1,5},{2,6},{3,7},{4,0},{5,1},{6,2},{7,3},{8,12},{9,13},{10,... | collective-permute-start | bytes 786440 | tf_op jit(solution)/shard_map/ppermute | solution.py:37
  136.2 16.4 %collective-permute-start.22 = (bf16[384,256]{1,0:T(8,128)(2,1)S(1)}, bf16[384,256]{1,0:T(8,128)(2,1)S(1)}, u32[]{:S(2)}, u32[]{:S(2)}) collective-permute-start(bf16[384,256]{1,0:T(8,128)(2,1)S(1)} %get-tuple-element.39), channel_id=1, source_target_pairs={{0,8},{8,0},{16,24},{24,16},{1,9},{9,1},{17,25},{25,17},{2,10},{10... | collective-permute-start | bytes 589832 | tf_op jit(solution)/shard_map/ppermute | solution.py:37
  142.9 11.3 %collective-permute-start.23 = (bf16[384,256]{1,0:T(8,128)(2,1)S(1)}, bf16[384,256]{1,0:T(8,128)(2,1)S(1)}, u32[]{:S(2)}, u32[]{:S(2)}) collective-permute-start(bf16[384,256]{1,0:T(8,128)(2,1)S(1)} %get-tuple-element.38), channel_id=1, source_target_pairs={{0,16},{8,24},{16,0},{24,8},{1,17},{9,25},{17,1},{25,9},{2,18},{10... | collective-permute-start | bytes 589832 | tf_op jit(solution)/shard_map/ppermute | solution.py:37
  144.4 7.2 %collective-permute-start.29 = (bf16[384,256]{1,0:T(8,128)(2,1)S(1)}, bf16[384,256]{1,0:T(8,128)(2,1)S(1)}, u32[]{:S(2)}, u32[]{:S(2)}) collective-permute-start(bf16[384,256]{1,0:T(8,128)(2,1)S(1)} %get-tuple-element.32), channel_id=1, source_target_pairs={{0,16},{8,24},{16,0},{24,8},{1,17},{9,25},{17,1},{25,9},{2,18},{10... | collective-permute-start | bytes 589832 | tf_op jit(solution)/shard_map/ppermute | solution.py:37
  151.7 10.6 %collective-permute-start.14 = (bf16[384,256]{1,0:T(8,128)(2,1)S(1)}, bf16[384,256]{1,0:T(8,128)(2,1)S(1)}, u32[]{:S(2)}, u32[]{:S(2)}) collective-permute-start(bf16[384,256]{1,0:T(8,128)(2,1)S(1)} %get-tuple-element.42), channel_id=1, source_target_pairs={{0,8},{8,0},{16,24},{24,16},{1,9},{9,1},{17,25},{25,17},{2,10},{10... | collective-permute-start | bytes 589832 | tf_op jit(solution)/shard_map/ppermute | solution.py:37
  152.6 9.7 %collective-permute-start.15 = (bf16[384,256]{1,0:T(8,128)(2,1)S(1)}, bf16[384,256]{1,0:T(8,128)(2,1)S(1)}, u32[]{:S(2)}, u32[]{:S(2)}) collective-permute-start(bf16[384,256]{1,0:T(8,128)(2,1)S(1)} %get-tuple-element.41), channel_id=1, source_target_pairs={{0,16},{8,24},{16,0},{24,8},{1,17},{9,25},{17,1},{25,9},{2,18},{10... | collective-permute-start | bytes 589832 | tf_op jit(solution)/shard_map/ppermute | solution.py:37
  154.2 8.1 %collective-permute-start.21 = (bf16[384,256]{1,0:T(8,128)(2,1)S(1)}, bf16[384,256]{1,0:T(8,128)(2,1)S(1)}, u32[]{:S(2)}, u32[]{:S(2)}) collective-permute-start(bf16[384,256]{1,0:T(8,128)(2,1)S(1)} %add_convert_fusion.8), channel_id=1, source_target_pairs={{0,24},{8,16},{16,8},{24,0},{1,25},{9,17},{17,9},{25,1},{2,26},{10... | collective-permute-start | bytes 589832 | tf_op jit(solution)/shard_map/ppermute | solution.py:37
  155.8 10.4 %collective-permute-start.30 = (bf16[512,256]{1,0:T(8,128)(2,1)S(1)}, bf16[512,256]{1,0:T(8,128)(2,1)S(1)}, u32[]{:S(2)}, u32[]{:S(2)}) collective-permute-start(bf16[512,256]{1,0:T(8,128)(2,1)S(1)} %combine.6), channel_id=1, source_target_pairs={{0,2},{1,3},{2,0},{3,1},{4,6},{5,7},{6,4},{7,5},{8,10},{9,11},{10,... | collective-permute-start | bytes 786440 | tf_op jit(solution)/shard_map/ppermute | solution.py:37
  157.9 13.5 %collective-permute-start.27 = (bf16[512,256]{1,0:T(8,128)(2,1)S(1)}, bf16[512,256]{1,0:T(8,128)(2,1)S(1)}, u32[]{:S(2)}, u32[]{:S(2)}) collective-permute-start(bf16[512,256]{1,0:T(8,128)(2,1)S(1)} %combine.5), channel_id=1, source_target_pairs={{0,4},{1,5},{2,6},{3,7},{4,0},{5,1},{6,2},{7,3},{8,12},{9,13},{10,... | collective-permute-start | bytes 786440 | tf_op jit(solution)/shard_map/ppermute | solution.py:37
  (7 other events, 5.1 us)
where the time goes:
time: 173 us
  waiting for transfers between devices  75.4 us (44%)
  Pallas kernels  42.8 us (25%)
  starting transfers between devices  32.7 us (19%)
  local copies, waits for them, and re-layouts  17 us (10%)
  other arithmetic  3.97 us (2%)
    ppermute x25, waiting for transfers between devices, swap_over(): return lax.ppermute(value, axis, [(i, i ^ mask) for i in range(size)])  41.7 us
    ppermute x6, waiting for transfers between devices, step_over(): return lax.ppermute(value, ('ep', 'tp'), pairs)  33.7 us
    ppermute x25, starting transfers between devices, swap_over(): return lax.ppermute(value, axis, [(i, i ^ mask) for i in range(size)])  25.1 us
    pallas_call x2, Pallas kernels, run_experts(): pl.pallas_call(functools.partial(experts_kernel, tuple(names), metas.shap...  19.7 us
    unnamed x48, local copies, waits for them, and re-layouts  16.2 us
    pallas_call x1, Pallas kernels, attention(): pl.pallas_call(functools.partial(attention_kernel, turn_width, len(pieces...  11.1 us
    ppermute x6, starting transfers between devices, step_over(): return lax.ppermute(value, ('ep', 'tp'), pairs)  7.62 us
    pallas_call x1, Pallas kernels, prepare(): pl.pallas_call(prepare_kernel, out_shape=outputs, in_specs=[SMEM_SPEC] +...  4.72 us
  transfers between devices with their start and end apart: 31, of which 10 were waited for; matrix products, arithmetic and copies ran while one was open for 2% of the time, Pallas kernels for 21%

commit v1 on v0

--- a/solution.py
+++ b/solution.py
@@ -20,6 +20,10 @@
 SMEM_SPEC = pl.BlockSpec(memory_space=pltpu.SMEM)
 VMEM_SPEC = pl.BlockSpec(memory_space=pltpu.VMEM)
 HBM_SPEC = pl.BlockSpec(memory_space=pltpu.HBM)
+
+
+def in_hbm(value):
+    return pltpu.with_memory_space_constraint(value, pltpu.HBM)
 
 
 def params(mebibytes):
@@ -144,7 +148,7 @@
         compiler_params=params(60),
         cost_estimate=cost(4e12 * 3e-6, 4e6),
         name="prepare",
-    )(ids, *inputs)
+    )(ids, *[in_hbm(v) for v in inputs])
 
 
 def turn_tables(cosine, sine, start, count, lanes):
@@ -228,13 +232,22 @@
 
 
 def attention_kernel(
-    turn_width, piece_count, tp_bits, ids, plain, turned, cosine, sine, key_weight,
-    value_weight, output_hbm, *rest
+    turn_width, piece_count, tp_bits, ids, *rest
 ):
-    pieces = rest[:piece_count]
-    keep, send, meta, keys, values, mixed, output_weight, sem = rest[piece_count:]
-    fetch = pltpu.make_async_copy(output_hbm, output_weight, sem)
-    fetch.start()
+    sources = rest[:7]
+    pieces = rest[7 : 7 + piece_count]
+    keep, send, meta, keys, values, mixed = rest[7 + piece_count : 13 + piece_count]
+    targets = rest[13 + piece_count : 20 + piece_count]
+    sems = rest[-1]
+    key_weight, value_weight, cosine, sine, plain, turned, output_weight = targets
+    loads = [
+        pltpu.make_async_copy(source, target, sems.at[i])
+        for i, (source, target) in enumerate(zip(sources, targets))
+    ]
+    for load in loads:
+        load.start()
+    for load in loads[:4]:
+        load.wait()
     rows = plain.shape[0]
     latent = key_weight.shape[0]
     turn_lanes = turned.shape[1]
@@ -267,6 +280,8 @@
             keys[p, start : start + half, pair:] = key
             values[p, start : start + half, :] = value_block[:, p * pair : (p + 1) * pair]
 
+    loads[4].wait()
+    loads[5].wait()
     tile = min(rows, 256)
     plain_lane = lax.broadcasted_iota(jnp.int32, (tile, pair), 1)
     turn_lane = lax.broadcasted_iota(jnp.int32, (tile, turn_lanes), 1)
@@ -298,7 +313,7 @@
 
     lax.fori_loop(0, rows // tile, step, 0)
 
-    fetch.wait()
+    loads[6].wait()
     place_count = 1 << tp_bits
     block_rows = rows // place_count
     me = ids[0]
@@ -326,37 +341,50 @@
     rows = plain.shape[0]
     head_count = key_weight.shape[1] // NOPE
     key_rows = sum(p.shape[0] for p in pieces)
+    sources = (key_weight, value_weight, cosine, sine, plain, turned, output_weight)
     turn_lanes = turned.shape[1]
     width = output_weight.shape[1]
     shape = jax.ShapeDtypeStruct((rows // 2, width), BF16)
     return pl.pallas_call(
         functools.partial(attention_kernel, turn_width, len(pieces), tp_bits),
         out_shape=(shape, shape, jax.ShapeDtypeStruct((len(pieces) // 2 - 1, 8, rows), F32)),
-        in_specs=[SMEM_SPEC] + [VMEM_SPEC] * 6 + [HBM_SPEC] + [VMEM_SPEC] * len(pieces),
+        in_specs=[SMEM_SPEC] + [HBM_SPEC] * 7 + [VMEM_SPEC] * len(pieces),
         out_specs=(VMEM_SPEC,) * 3,
         scratch_shapes=[
             pltpu.VMEM((head_count // 2, key_rows, 2 * NOPE + turn_lanes), BF16),
             pltpu.VMEM((head_count // 2, key_rows, 2 * VDIM), BF16),
             pltpu.VMEM((rows, head_count * VDIM), BF16),
-            pltpu.VMEM(output_weight.shape, BF16),
-            pltpu.SemaphoreType.DMA,
+        ]
+        + [pltpu.VMEM(v.shape, v.dtype) for v in sources]
+        + [
+            pltpu.SemaphoreType.DMA((7,)),
         ],
         compiler_params=params(26 if key_rows <= 2048 else 60),
         cost_estimate=cost(4e12 * 12e-6, 40e6),
         name="attention",
-    )(
-        ids, plain, turned, cosine, sine, key_weight, value_weight, output_weight, *pieces
-    )
+    )(ids, *[in_hbm(v) for v in sources], *pieces)
 
 
 def experts_kernel(
-    names, group_count, capacity, tp_bits, ids, gate, up, down, own_meta, metas, *rest
+    names, fetch, group_count, capacity, tp_bits, ids, gate, up, down, *rest
 ):
     blocks = len(names)
-    pieces = rest[: 2 * blocks]
-    keep, send, slots, loads, gathered = rest[2 * blocks :]
+    tables = rest[:blocks]
+    pieces = rest[blocks : 3 * blocks]
+    if fetch:
+        sources = (gate, up, down)
+        keep, send, gate, up, down, slots, loads, gathered, sems = rest[3 * blocks :]
+        copies = [
+            pltpu.make_async_copy(source.at[j], target.at[j], sems.at[3 * j + k])
+            for j in range(gate.shape[0])
+            for k, (source, target) in enumerate(zip(sources, (gate, up, down)))
+        ]
+        for copy in copies:
+            copy.start()
+    else:
+        keep, send, slots, loads, gathered = rest[3 * blocks :]
     local_count = gate.shape[0]
-    tokens = own_meta.shape[1]
+    tokens = tables[0].shape[1]
     half = tokens // 2
     me, core, group = ids[0], ids[1], ids[2]
 
@@ -367,7 +395,7 @@
     row = lax.broadcasted_iota(jnp.int32, (8, tokens), 0)
     wanted = (row + group * local_count).astype(F32)
     for b in range(blocks):
-        meta = own_meta[...] if names[b] == 0 else metas[names[b] - 1]
+        meta = tables[b][...]
         first = meta[0:1, :] == wanted
         second = meta[1:2, :] == wanted
         named = (first | second) & (row < local_count)
@@ -398,8 +426,14 @@
             ).astype(BF16)
             scale.append(weight)
         rows_in = gathered[...]
+        if fetch:
+            copies[3 * j].wait()
         gate_acts = jnp.dot(rows_in, gate[j], preferred_element_type=F32)
+        if fetch:
+            copies[3 * j + 1].wait()
         up_acts = jnp.dot(rows_in, up[j], preferred_element_type=F32)
+        if fetch:
+            copies[3 * j + 2].wait()
         hidden = (gate_acts * (1.0 / (1.0 + jnp.exp(-gate_acts))) * up_acts).astype(BF16)
         for target, low in ((send, place_count // 2), (keep, 0)):
             for i in range(place_count // 2):
@@ -416,30 +450,34 @@
                     ).astype(BF16)
 
 
-def run_experts(
-    ids, names, own_meta, metas, pieces, gate_weight, up_weight, down_weight, capacity, tp_bits
-):
-    local_count, width, _ = gate_weight.shape
+def run_experts(ids, group_count, names, tables, pieces, weights, fetch, capacity, tp_bits):
+    local_count, width, _ = weights[0].shape
     count = len(names)
-    tokens = own_meta.shape[1]
+    tokens = tables[0].shape[1]
     rows = count * local_count * capacity
-    shape = jax.ShapeDtypeStruct((rows, width // 2), BF16)
+    shapes = [jax.ShapeDtypeStruct((rows, width // 2), BF16)] * 2
+    scratch = [
+        pltpu.VMEM((count, 8, tokens), F32),
+        pltpu.VMEM((count, 8, tokens), F32),
+        pltpu.VMEM((count * capacity, width), BF16),
+    ]
+    if fetch:
+        shapes += [pltpu.VMEM(w.shape, w.dtype) for w in weights]
+        scratch.append(pltpu.SemaphoreType.DMA((3 * local_count,)))
     return pl.pallas_call(
         functools.partial(
-            experts_kernel, tuple(names), metas.shape[0] + 1, capacity, tp_bits
+            experts_kernel, tuple(names), fetch, group_count, capacity, tp_bits
         ),
-        out_shape=(shape, shape),
-        in_specs=[SMEM_SPEC] + [VMEM_SPEC] * (5 + 2 * count),
-        out_specs=(VMEM_SPEC, VMEM_SPEC),
-        scratch_shapes=[
-            pltpu.VMEM((count, 8, tokens), F32),
-            pltpu.VMEM((count, 8, tokens), F32),
-            pltpu.VMEM((count * capacity, width), BF16),
-        ],
-        compiler_params=params(min(60, 18 + 4 * count)),
+        out_shape=tuple(shapes),
+        in_specs=[SMEM_SPEC]
+        + [HBM_SPEC if fetch else VMEM_SPEC] * 3
+        + [VMEM_SPEC] * (3 * count),
+        out_specs=(VMEM_SPEC,) * len(shapes),
+        scratch_shapes=scratch,
+        compiler_params=params(24 if fetch else min(60, 18 + 4 * count)),
         cost_estimate=cost(4e12 * 5e-6 * count, 14e6 * count),
         name="experts",
-    )(ids, gate_weight, up_weight, down_weight, own_meta, metas, *pieces)
+    )(ids, *([in_hbm(w) for w in weights] if fetch else weights), *tables, *pieces)
 
 
 def combine_kernel(starts, pick, *rest):
@@ -519,9 +557,10 @@
     core = tp & 1
     names = range(group_count)
     groups = [ep ^ jnp.where(core == 0, n, reverse_bits(n, ep_bits)) for n in names]
-    near = [n for n in names if bin(n).count("1") <= 1]
-    far = [n for n in names if n not in near]
-    classes = [near] + ([far] if far else [])
+    direct = [n for n in names if bin(n).count("1") == 1]
+    far = [n for n in names if bin(n).count("1") > 1]
+    near = [0] + direct
+    classes = [[0], direct] + ([far] if far else [])
     place = {n: c.index(n) for c in classes for n in c}
     orders = [jnp.where(core == 0, place[n], place[reverse_bits(n, ep_bits)]) for n in names]
     ids = jnp.stack([tp, core, ep] + groups + orders).astype(jnp.int32)
@@ -552,6 +591,11 @@
     for n in far:
         b = n.bit_length() - 1
         latent_held[n] = step_over(latent_held[n ^ (1 << b)], b, ep_bits)
+    own_keep, own_send, *weights = run_experts(
+        ids, group_count, [0], [own_meta], [row_mine, row_other],
+        (gate_weight, up_weight, down_weight), True, capacity, tp_bits,
+    )
+
     for b in range(1, ep_bits):
         row_held[1 << b] = step_over(row_mine, b, ep_bits)
 
@@ -584,12 +628,16 @@
     width = expert_input.shape[1] // part_count
     gathered = {}
     for chosen in classes:
-        keep, send = run_experts(
-            ids, chosen, own_meta, metas, [piece for n in chosen for piece in row_pairs[n]],
-            gate_weight, up_weight, down_weight, capacity, tp_bits,
-        )
+        if chosen == [0]:
+            keep, send = own_keep, own_send
+        else:
+            keep, send = run_experts(
+                ids, group_count, chosen, [metas[n - 1] for n in chosen],
+                [piece for n in chosen for piece in row_pairs[n]], weights, False,
+                capacity, tp_bits,
+            )
         arrived = swap_over(send, "tp", 1)
-        if chosen == near:
+        if chosen != far:
             both = add_wide(keep, arrived)
             for i, r in enumerate(chosen):
                 for c in range(chunk_count):

time: 173 us -> 162 us (0.936)
  local copies, waits for them, and re-layouts: 17 us -> 2.12 us
  waiting for transfers between devices: 75.4 us -> 78.5 us
    unnamed x48 -> x16, local copies, waits for them, and re-layouts: 16.2 us -> 1.34 us
    ppermute x6, waiting for transfers between devices: 33.7 us -> 41.2 us  [step_over(): return lax.ppermute(value, ('ep', 'tp'), pairs)]
    ppermute x25 -> x26, waiting for transfers between devices: 41.7 us -> 37.3 us  [swap_over(): return lax.ppermute(value, axis, [(i, i ^ mask) for i in range(size)])]
    pallas_call x2 -> x3, Pallas kernels: 19.7 us -> 20.6 us  [run_experts(): pl.pallas_call(functools.partial(experts_kernel, tuple(names), fetch, gro...]
    ppermute x25 -> x26, starting transfers between devices: 25.1 us -> 24.2 us  [swap_over(): return lax.ppermute(value, axis, [(i, i ^ mask) for i in range(size)])]
  transfers between devices with their start and end apart: 31 -> 32, of which waited for: 10 -> 12; matrix products, arithmetic and copies ran while one was open for 2% -> 2% of each run, Pallas kernels for 21% -> 24%
where the time goes in v1:
time: 162 us
  waiting for transfers between devices  78.5 us (48%)
  Pallas kernels  44.5 us (27%)
  starting transfers between devices  32.1 us (20%)
  other arithmetic  3.87 us (2%)
  local copies, waits for them, and re-layouts  2.12 us (1%)
    ppermute x6, waiting for transfers between devices, step_over(): return lax.ppermute(value, ('ep', 'tp'), pairs)  41.2 us
    ppermute x26, waiting for transfers between devices, swap_over(): return lax.ppermute(value, axis, [(i, i ^ mask) for i in range(size)])  37.3 us
    ppermute x26, starting transfers between devices, swap_over(): return lax.ppermute(value, axis, [(i, i ^ mask) for i in range(size)])  24.2 us
    pallas_call x3, Pallas kernels, run_experts(): pl.pallas_call(functools.partial(experts_kernel, tuple(names), fetch, gro...  20.6 us
    pallas_call x1, Pallas kernels, attention(): pl.pallas_call(functools.partial(attention_kernel, turn_width, len(pieces...  12 us
    ppermute x6, starting transfers between devices, step_over(): return lax.ppermute(value, ('ep', 'tp'), pairs)  7.88 us
    pallas_call x1, Pallas kernels, prepare(): pl.pallas_call(prepare_kernel, out_shape=outputs, in_specs=[SMEM_SPEC] +...  4.59 us
    pallas_call x1, Pallas kernels, queries(): pl.pallas_call(functools.partial(query_kernel, turn_width, local_count, c...  4.2 us
  transfers between devices with their start and end apart: 32, of which 12 were waited for; matrix products, arithmetic and copies ran while one was open for 2% of the time, Pallas kernels for 24%

profile of v1, /device:TPU:0, one launch (start us, length us, event | category | flops | bytes accessed | tf_op | source)
XLA Modules:
  0.0 162.0 jit_solution(2816130882393889247)
XLA Ops:
  0.6 0.6 stack.38.ids
  1.3 4.6 %prepare.1 = (bf16[256,640]{1,0:T(8,128)(2,1)}, bf16[256,640]{1,0:T(8,128)(2,1)}, f32[8,512]{1,0:T(8,128)}, bf16[256,2048]{1,0:T(8,128)(2,1)}, bf16[256,2048]{1,0:T(8,128)(2,1)}) custom-call(s32[11]{0:T(128)} %stack.38.ids, bf16[512,512]{1,0:T(8,128)(2,1)} %joint_hbm.1, f32[1,512]{1,0:T(1,128)} %bitcast.26, bf16[32,512]{1,0:T(8,128)(2,1)} %bitcast.20, ...), custom_call_target="tpu_custom_call" | custom-call | flops 12000000 | bytes 4000000 | tf_op jit(solution)/shard_map/prepare/pallas_call | solution.py:141
  5.9 3.1 %collective-permute-start.11 = (bf16[256,2048]{1,0:T(8,128)(2,1)}, bf16[256,2048]{1,0:T(8,128)(2,1)}, u32[]{:S(2)}, u32[]{:S(2)}) collective-permute-start(bf16[256,2048]{1,0:T(8,128)(2,1)} %get-tuple-element.30.rest_1_), channel_id=1, source_target_pairs={{0,16},{1,9},{2,18},{3,11},{4,20},{5,13},{6,22},{7,15},{8,24},{9,1... | collective-permute-start | bytes 3145736 | tf_op jit(solution)/shard_map/ppermute | solution.py:527
  8.9 1.5 collective-permute-start.10
  10.4 0.5 collective-permute-start.1
  11.0 21.7 %collective-permute-done.11.rest_4_ = bf16[256,2048]{1,0:T(8,128)(2,1)} collective-permute-done((bf16[256,2048]{1,0:T(8,128)(2,1)}, bf16[256,2048]{1,0:T(8,128)(2,1)}, u32[]{:S(2)}, u32[]{:S(2)}) %collective-permute-start.11) | collective-permute-done | bytes 1048608 | tf_op jit(solution)/shard_map/ppermute | solution.py:527
  32.7 2.6 %collective-permute-done.10.rest_2_ = bf16[256,2048]{1,0:T(8,128)(2,1)} collective-permute-done((bf16[256,2048]{1,0:T(8,128)(2,1)}, bf16[256,2048]{1,0:T(8,128)(2,1)}, u32[]{:S(2)}, u32[]{:S(2)}) %collective-permute-start.10) | collective-permute-done | bytes 1048608 | tf_op jit(solution)/shard_map/ppermute | solution.py:527
  35.3 0.4 collective-permute-start.17
  35.7 4.0 %collective-permute-done.1.rest_11_ = bf16[256,640]{1,0:T(8,128)(2,1)S(1)} collective-permute-done((bf16[256,640]{1,0:T(8,128)(2,1)}, bf16[256,640]{1,0:T(8,128)(2,1)S(1)}, u32[]{:S(2)}, u32[]{:S(2)}) %collective-permute-start.1) | collective-permute-done | bytes 327712 | tf_op jit(solution)/shard_map/ppermute | solution.py:527
  40.0 2.3 %collective-permute-start.4 = (bf16[256,640]{1,0:T(8,128)(2,1)S(1)}, bf16[256,640]{1,0:T(8,128)(2,1)}, u32[]{:S(2)}, u32[]{:S(2)}) collective-permute-start(bf16[256,640]{1,0:T(8,128)(2,1)S(1)} %collective-permute-done.rest_9_), channel_id=1, source_target_pairs={{0,16},{1,9},{2,18},{3,11},{4,20},{5,13},{6,22},{7,15},{8,24},{9,1... | collective-permute-start | bytes 983048 | tf_op jit(solution)/shard_map/ppermute | solution.py:527
  42.4 12.7 %collective-permute-done.4.rest_13_ = bf16[256,640]{1,0:T(8,128)(2,1)} collective-permute-done((bf16[256,640]{1,0:T(8,128)(2,1)S(1)}, bf16[256,640]{1,0:T(8,128)(2,1)}, u32[]{:S(2)}, u32[]{:S(2)}) %collective-permute-start.4) | collective-permute-done | bytes 327712 | tf_op jit(solution)/shard_map/ppermute | solution.py:527
  55.0 1.2 multiply_sine_fusion
  56.3 4.2 %queries.1 = (bf16[512,256]{1,0:T(8,128)(2,1)}, bf16[512,128]{1,0:T(8,128)(2,1)}, bf16[512,1536]{1,0:T(8,128)(2,1)}) custom-call(s32[11]{0:T(128)} %stack.38.ids, bf16[512,1024]{1,0:T(8,128)(2,1)} %query_latent.1, f32[1,1024]{1,0:T(1,128)} %bitcast.25, bf16[1024,256]{1,0:T(8,128)(2,1)} %query_weight.1, bf16[1024,128]{1,0:T(8,128)(2,1)} %query_rotary.1, ...), custom_call_target="tpu_custom_call" | custom-call | flops 16000000 | bytes 12000000 | tf_op jit(solution)/shard_map/queries/pallas_call | solution.py:216
  60.5 0.6 copy-done.5
  61.1 0.7 copy-done.7
  61.8 6.4 %experts.3 = (bf16[384,1024]{1,0:T(8,128)(2,1)S(1)}, bf16[384,1024]{1,0:T(8,128)(2,1)S(1)}, bf16[2,2048,512]{2,1,0:T(8,128)(2,1)S(1)}, bf16[2,2048,512]{2,1,0:T(8,128)(2,1)S(1)}, bf16[2,512,2048]{2,1,0:T(8,128)(2,1)S(1)}) custom-call(s32[11]{0:T(128)S(1)} %copy-done.5, bf16[2,2048,512]{2,1,0:T(8,128)(2,1)} %gate.1, bf16[2,2048,512]{2,1,0:T(8,128)(2,1)} %up.1, ...), custom_call_target="tpu_custom_call" | custom-call | flops 20000000 | bytes 14000000 | tf_op jit(solution)/shard_map/experts/pallas_call | solution.py:467
  68.2 0.6 collective-permute-start.9
  68.8 12.0 %attention.1 = (bf16[256,2048]{1,0:T(8,128)(2,1)S(1)}, bf16[256,2048]{1,0:T(8,128)(2,1)S(1)}, f32[3,8,512]{2,1,0:T(8,128)S(1)}) custom-call(s32[11]{0:T(128)S(1)} %copy-done.6, bf16[512,256]{1,0:T(8,128)(2,1)} %rest_0_.1, bf16[512,256]{1,0:T(8,128)(2,1)} %rest_1_.1, f32[16,2048]{1,0:T(8,128)} %get-tuple-element.62.cosine.rest_2_, ...), custom_call_target="tpu_custom_call" | custom-call | flops 48000000 | bytes 40000000 | tf_op jit(solution)/shard_map/attention/pallas_call | solution.py:348
  80.9 9.7 %experts.4 = (bf16[768,1024]{1,0:T(8,128)(2,1)S(1)}, bf16[768,1024]{1,0:T(8,128)(2,1)S(1)}) custom-call(s32[11]{0:T(128)S(1)} %copy-done.6, bf16[2,2048,512]{2,1,0:T(8,128)(2,1)S(1)} %get-tuple-element.34.gate, bf16[2,2048,512]{2,1,0:T(8,128)(2,1)S(1)} %get-tuple-element.35.up, bf16[2,512,2048]{2,1,0:T(8,128)(2,1)S(1)} %get-tuple-element.36.down, ...), custom_call_target="tpu_custom_call" | custom-call | flops 40000000 | bytes 28000000 | tf_op jit(solution)/shard_map/experts/pallas_call | solution.py:467
  90.7 0.5 collective-permute-start.18
  91.6 4.0 %collective-permute-done.18.rest_2_ = bf16[256,2048]{1,0:T(8,128)(2,1)S(1)} collective-permute-done((bf16[256,2048]{1,0:T(8,128)(2,1)S(1)}, bf16[256,2048]{1,0:T(8,128)(2,1)S(1)}, u32[]{:S(2)}, u32[]{:S(2)}) %collective-permute-start.18) | collective-permute-done | bytes 1048608 | tf_op jit(solution)/shard_map/ppermute | solution.py:41
  95.6 4.5 %experts.5 = (bf16[384,1024]{1,0:T(8,128)(2,1)S(1)}, bf16[384,1024]{1,0:T(8,128)(2,1)S(1)}) custom-call(s32[11]{0:T(128)S(1)} %copy-done.6, bf16[2,2048,512]{2,1,0:T(8,128)(2,1)S(1)} %get-tuple-element.34.gate, bf16[2,2048,512]{2,1,0:T(8,128)(2,1)S(1)} %get-tuple-element.35.up, bf16[2,512,2048]{2,1,0:T(8,128)(2,1)S(1)} %get-tuple-element.36.down, ...), custom_call_target="tpu_custom_call" | custom-call | flops 20000000 | bytes 14000000 | tf_op jit(solution)/shard_map/experts/pallas_call | solution.py:467
  100.7 2.1 %collective-permute-start.7 = (bf16[128,2048]{1,0:T(8,128)(2,1)S(1)}, bf16[128,2048]{1,0:T(8,128)(2,1)S(1)}, u32[]{:S(2)}, u32[]{:S(2)}) collective-permute-start(bf16[128,2048]{1,0:T(8,128)(2,1)S(1)} %get-tuple-element.43), channel_id=1, source_target_pairs={{0,2},{1,3},{2,0},{3,1},{4,6},{5,7},{6,4},{7,5},{8,10},{9,11},{10,... | collective-permute-start | bytes 1572872 | tf_op jit(solution)/shard_map/ppermute | solution.py:41
  102.8 0.7 add_convert_fusion
  103.8 1.0 collective-permute-start.20
  104.9 0.7 collective-permute-start.25
  105.6 1.5 collective-permute-start.26
  107.1 1.7 %collective-permute-start.23 = (bf16[384,256]{1,0:T(8,128)(2,1)S(1)}, bf16[384,256]{1,0:T(8,128)(2,1)S(1)}, u32[]{:S(2)}, u32[]{:S(2)}) collective-permute-start(bf16[384,256]{1,0:T(8,128)(2,1)S(1)} %get-tuple-element.49), channel_id=1, source_target_pairs={{0,8},{8,0},{16,24},{24,16},{1,9},{9,1},{17,25},{25,17},{2,10},{10... | collective-permute-start | bytes 589832 | tf_op jit(solution)/shard_map/ppermute | solution.py:41
  108.8 3.9 %collective-permute-done.25.rest_1_ = bf16[384,256]{1,0:T(8,128)(2,1)S(1)} collective-permute-done((bf16[384,256]{1,0:T(8,128)(2,1)S(1)}, bf16[384,256]{1,0:T(8,128)(2,1)S(1)}, u32[]{:S(2)}, u32[]{:S(2)}) %collective-permute-start.25) | collective-permute-done | bytes 196640 | tf_op jit(solution)/shard_map/ppermute | solution.py:41
  112.8 1.5 collective-permute-start.24
  114.3 0.6 collective-permute-start.29
  114.9 0.6 combine.4
  115.4 8.3 %collective-permute-done.20 = bf16[384,512]{1,0:T(8,128)(2,1)S(1)} collective-permute-done((bf16[384,512]{1,0:T(8,128)(2,1)S(1)}, bf16[384,512]{1,0:T(8,128)(2,1)S(1)}, u32[]{:S(2)}, u32[]{:S(2)}) %collective-permute-start.20) | collective-permute-done | bytes 393248 | tf_op jit(solution)/shard_map/ppermute | solution.py:41
  123.7 1.7 %collective-permute-start.30 = (bf16[384,256]{1,0:T(8,128)(2,1)S(1)}, bf16[384,256]{1,0:T(8,128)(2,1)S(1)}, u32[]{:S(2)}, u32[]{:S(2)}) collective-permute-start(bf16[384,256]{1,0:T(8,128)(2,1)S(1)} %get-tuple-element.44), channel_id=1, source_target_pairs={{0,16},{8,24},{16,0},{24,8},{1,17},{9,25},{17,1},{25,9},{2,18},{10... | collective-permute-start | bytes 589832 | tf_op jit(solution)/shard_map/ppermute | solution.py:41
  125.5 1.6 collective-permute-start.27
  127.1 2.6 %collective-permute-start.21 = (bf16[384,256]{1,0:T(8,128)(2,1)S(1)}, bf16[384,256]{1,0:T(8,128)(2,1)S(1)}, u32[]{:S(2)}, u32[]{:S(2)}) collective-permute-start(bf16[384,256]{1,0:T(8,128)(2,1)S(1)} %add_convert_fusion.10), channel_id=1, source_target_pairs={{0,4},{1,5},{2,6},{3,7},{4,0},{5,1},{6,2},{7,3},{8,12},{9,13},{10,... | collective-permute-start | bytes 589832 | tf_op jit(solution)/shard_map/ppermute | solution.py:41
  129.8 0.6 collective-permute-done.30.rest_2_
  130.3 2.5 %collective-permute-start.8 = (bf16[64,2048]{1,0:T(8,128)(2,1)S(1)}, bf16[64,2048]{1,0:T(8,128)(2,1)S(1)}, u32[]{:S(2)}, u32[]{:S(2)}) collective-permute-start(bf16[64,2048]{1,0:T(8,128)(2,1)S(1)} %add_convert_fusion.7), channel_id=1, source_target_pairs={{0,4},{1,5},{2,6},{3,7},{4,0},{5,1},{6,2},{7,3},{8,12},{9,13},{10,... | collective-permute-start | bytes 786440 | tf_op jit(solution)/shard_map/ppermute | solution.py:41
  132.9 0.6 combine.6
  133.4 0.7 collective-permute-start.15
  134.1 1.5 collective-permute-start.16
  135.6 3.0 %collective-permute-done.27.rest_3_ = bf16[512,256]{1,0:T(8,128)(2,1)S(1)} collective-permute-done((bf16[512,256]{1,0:T(8,128)(2,1)S(1)}, bf16[512,256]{1,0:T(8,128)(2,1)S(1)}, u32[]{:S(2)}, u32[]{:S(2)}) %collective-permute-start.27) | collective-permute-done | bytes 262176 | tf_op jit(solution)/shard_map/ppermute | solution.py:41
  138.6 0.6 combine.5
  139.2 2.9 %collective-permute-start.28 = (bf16[512,256]{1,0:T(8,128)(2,1)S(1)}, bf16[512,256]{1,0:T(8,128)(2,1)S(1)}, u32[]{:S(2)}, u32[]{:S(2)}) collective-permute-start(bf16[512,256]{1,0:T(8,128)(2,1)S(1)} %combine.5), channel_id=1, source_target_pairs={{0,4},{1,5},{2,6},{3,7},{4,0},{5,1},{6,2},{7,3},{8,12},{9,13},{10,... | collective-permute-start | bytes 786440 | tf_op jit(solution)/shard_map/ppermute | solution.py:41
  142.2 9.7 %collective-permute-done.8 = bf16[64,2048]{1,0:T(8,128)(2,1)S(1)} collective-permute-done((bf16[64,2048]{1,0:T(8,128)(2,1)S(1)}, bf16[64,2048]{1,0:T(8,128)(2,1)S(1)}, u32[]{:S(2)}, u32[]{:S(2)}) %collective-permute-start.8) | collective-permute-done | bytes 262176 | tf_op jit(solution)/shard_map/ppermute | solution.py:41
  151.8 0.8 add_convert_fusion.6
  152.7 7.9 %collective-permute-done.28.rest_4_ = bf16[512,256]{1,0:T(8,128)(2,1)S(1)} collective-permute-done((bf16[512,256]{1,0:T(8,128)(2,1)S(1)}, bf16[512,256]{1,0:T(8,128)(2,1)S(1)}, u32[]{:S(2)}, u32[]{:S(2)}) %collective-permute-start.28) | collective-permute-done | bytes 262176 | tf_op jit(solution)/shard_map/ppermute | solution.py:41
  160.6 1.4 combine.7
  (57 shorter events, 2.2 us)
Async XLA Ops:
  5.9 54.6 %copy-start.1 = (bf16[256,2048]{1,0:T(8,128)(2,1)S(1)}, bf16[256,2048]{1,0:T(8,128)(2,1)}, u32[]{:S(2)}) copy-start(bf16[256,2048]{1,0:T(8,128)(2,1)} %get-tuple-element.30.rest_1_) | copy-start | bytes 3145732
  5.9 54.6 %copy-start.2 = (bf16[256,2048]{1,0:T(8,128)(2,1)S(1)}, bf16[256,2048]{1,0:T(8,128)(2,1)}, u32[]{:S(2)}) copy-start(bf16[256,2048]{1,0:T(8,128)(2,1)} %get-tuple-element.31.rest_2_) | copy-start | bytes 3145732
  5.9 26.9 %collective-permute-start.11 = (bf16[256,2048]{1,0:T(8,128)(2,1)}, bf16[256,2048]{1,0:T(8,128)(2,1)}, u32[]{:S(2)}, u32[]{:S(2)}) collective-permute-start(bf16[256,2048]{1,0:T(8,128)(2,1)} %get-tuple-element.30.rest_1_), channel_id=1, source_target_pairs={{0,16},{1,9},{2,18},{3,11},{4,20},{5,13},{6,22},{7,15},{8,24},{9,1... | collective-permute-start | bytes 3145736 | tf_op jit(solution)/shard_map/ppermute | solution.py:527
  8.9 26.3 %collective-permute-start.10 = (bf16[256,2048]{1,0:T(8,128)(2,1)}, bf16[256,2048]{1,0:T(8,128)(2,1)}, u32[]{:S(2)}, u32[]{:S(2)}) collective-permute-start(bf16[256,2048]{1,0:T(8,128)(2,1)} %get-tuple-element.30.rest_1_), channel_id=1, source_target_pairs={{0,8},{1,17},{2,10},{3,19},{4,12},{5,21},{6,14},{7,23},{8,0},{9,25... | collective-permute-start | bytes 3145736 | tf_op jit(solution)/shard_map/ppermute | solution.py:527
  10.4 29.3 %collective-permute-start.1 = (bf16[256,640]{1,0:T(8,128)(2,1)}, bf16[256,640]{1,0:T(8,128)(2,1)S(1)}, u32[]{:S(2)}, u32[]{:S(2)}) collective-permute-start(bf16[256,640]{1,0:T(8,128)(2,1)} %get-tuple-element.24.rest_7_), channel_id=1, source_target_pairs={{0,16},{1,9},{2,18},{3,11},{4,20},{5,13},{6,22},{7,15},{8,24},{9,1... | collective-permute-start | bytes 983048 | tf_op jit(solution)/shard_map/ppermute | solution.py:527
  10.9 29.1 %collective-permute-start = (bf16[256,640]{1,0:T(8,128)(2,1)}, bf16[256,640]{1,0:T(8,128)(2,1)S(1)}, u32[]{:S(2)}, u32[]{:S(2)}) collective-permute-start(bf16[256,640]{1,0:T(8,128)(2,1)} %get-tuple-element.24.rest_7_), channel_id=1, source_target_pairs={{0,8},{1,17},{2,10},{3,19},{4,12},{5,21},{6,14},{7,23},{8,0},{9,25... | collective-permute-start | bytes 983048 | tf_op jit(solution)/shard_map/ppermute | solution.py:527
  32.7 48.1 %collective-permute-start.12 = (bf16[256,2048]{1,0:T(8,128)(2,1)}, bf16[256,2048]{1,0:T(8,128)(2,1)}, u32[]{:S(2)}, u32[]{:S(2)}) collective-permute-start(bf16[256,2048]{1,0:T(8,128)(2,1)} %collective-permute-done.11.rest_4_), channel_id=1, source_target_pairs={{0,1},{1,0},{2,3},{3,2},{4,5},{5,4},{6,7},{7,6},{8,9},{9,8},{10,11... | collective-permute-start | bytes 3145736 | tf_op jit(solution)/shard_map/ppermute | solution.py:41
  35.3 45.6 %collective-permute-start.13 = (bf16[256,2048]{1,0:T(8,128)(2,1)}, bf16[256,2048]{1,0:T(8,128)(2,1)}, u32[]{:S(2)}, u32[]{:S(2)}) collective-permute-start(bf16[256,2048]{1,0:T(8,128)(2,1)} %collective-permute-done.10.rest_2_), channel_id=1, source_target_pairs={{0,1},{1,0},{2,3},{3,2},{4,5},{5,4},{6,7},{7,6},{8,9},{9,8},{10,11... | collective-permute-start | bytes 3145736 | tf_op jit(solution)/shard_map/ppermute | solution.py:41
  35.3 55.4 %collective-permute-start.17 = (bf16[256,2048]{1,0:T(8,128)(2,1)}, bf16[256,2048]{1,0:T(8,128)(2,1)S(1)}, u32[]{:S(2)}, u32[]{:S(2)}) collective-permute-start(bf16[256,2048]{1,0:T(8,128)(2,1)} %collective-permute-done.10.rest_2_), channel_id=1, source_target_pairs={{0,16},{1,9},{2,18},{3,11},{4,20},{5,13},{6,22},{7,15},{8,24},{9,1... | collective-permute-start | bytes 3145736 | tf_op jit(solution)/shard_map/ppermute | solution.py:527
  39.8 2.5 %collective-permute-start.2 = (bf16[256,640]{1,0:T(8,128)(2,1)S(1)}, bf16[256,640]{1,0:T(8,128)(2,1)S(1)}, u32[]{:S(2)}, u32[]{:S(2)}) collective-permute-start(bf16[256,640]{1,0:T(8,128)(2,1)S(1)} %collective-permute-done.1.rest_11_), channel_id=1, source_target_pairs={{0,1},{1,0},{2,3},{3,2},{4,5},{5,4},{6,7},{7,6},{8,9},{9,8},{10,11... | collective-permute-start | bytes 983048 | tf_op jit(solution)/shard_map/ppermute | solution.py:41
  40.0 15.0 %collective-permute-start.4 = (bf16[256,640]{1,0:T(8,128)(2,1)S(1)}, bf16[256,640]{1,0:T(8,128)(2,1)}, u32[]{:S(2)}, u32[]{:S(2)}) collective-permute-start(bf16[256,640]{1,0:T(8,128)(2,1)S(1)} %collective-permute-done.rest_9_), channel_id=1, source_target_pairs={{0,16},{1,9},{2,18},{3,11},{4,20},{5,13},{6,22},{7,15},{8,24},{9,1... | collective-permute-start | bytes 983048 | tf_op jit(solution)/shard_map/ppermute | solution.py:527
  42.3 25.9 %collective-permute-start.3 = (bf16[256,640]{1,0:T(8,128)(2,1)S(1)}, bf16[256,640]{1,0:T(8,128)(2,1)}, u32[]{:S(2)}, u32[]{:S(2)}) collective-permute-start(bf16[256,640]{1,0:T(8,128)(2,1)S(1)} %collective-permute-done.rest_9_), channel_id=1, source_target_pairs={{0,1},{1,0},{2,3},{3,2},{4,5},{5,4},{6,7},{7,6},{8,9},{9,8},{10,11... | collective-permute-start | bytes 983048 | tf_op jit(solution)/shard_map/ppermute | solution.py:41
  55.0 13.8 %collective-permute-start.5 = (bf16[256,640]{1,0:T(8,128)(2,1)}, bf16[256,640]{1,0:T(8,128)(2,1)}, u32[]{:S(2)}, u32[]{:S(2)}) collective-permute-start(bf16[256,640]{1,0:T(8,128)(2,1)} %collective-permute-done.4.rest_13_), channel_id=1, source_target_pairs={{0,1},{1,0},{2,3},{3,2},{4,5},{5,4},{6,7},{7,6},{8,9},{9,8},{10,11... | collective-permute-start | bytes 983048 | tf_op jit(solution)/shard_map/ppermute | solution.py:41
  60.5 0.6 copy-start.5
  61.1 0.7 copy-start.7
  61.8 7.0 %copy-start.3 = (bf16[256,640]{1,0:T(8,128)(2,1)S(1)}, bf16[256,640]{1,0:T(8,128)(2,1)}, u32[]{:S(2)}) copy-start(bf16[256,640]{1,0:T(8,128)(2,1)} %get-tuple-element.24.rest_7_) | copy-start | bytes 983044
  61.8 7.0 %copy-start.4 = (bf16[256,640]{1,0:T(8,128)(2,1)S(1)}, bf16[256,640]{1,0:T(8,128)(2,1)}, u32[]{:S(2)}) copy-start(bf16[256,640]{1,0:T(8,128)(2,1)} %get-tuple-element.25.rest_8_) | copy-start | bytes 983044
  61.8 7.0 %copy-start.6 = (s32[11]{0:T(128)S(1)}, s32[11]{0:T(128)}, u32[]{:S(2)}) copy-start(s32[11]{0:T(128)} %stack.38.ids) | copy-start | bytes 136
  68.2 23.0 %collective-permute-start.9 = (bf16[384,1024]{1,0:T(8,128)(2,1)S(1)}, bf16[384,1024]{1,0:T(8,128)(2,1)S(1)}, u32[]{:S(2)}, u32[]{:S(2)}) collective-permute-start(bf16[384,1024]{1,0:T(8,128)(2,1)S(1)} %get-tuple-element.33), channel_id=1, source_target_pairs={{0,1},{1,0},{2,3},{3,2},{4,5},{5,4},{6,7},{7,6},{8,9},{9,8},{10,11... | collective-permute-start | bytes 2359304 | tf_op jit(solution)/shard_map/ppermute | solution.py:41
  90.6 12.2 %collective-permute-start.14 = (bf16[768,1024]{1,0:T(8,128)(2,1)S(1)}, bf16[768,1024]{1,0:T(8,128)(2,1)S(1)}, u32[]{:S(2)}, u32[]{:S(2)}) collective-permute-start(bf16[768,1024]{1,0:T(8,128)(2,1)S(1)} %get-tuple-element.39), channel_id=1, source_target_pairs={{0,1},{1,0},{2,3},{3,2},{4,5},{5,4},{6,7},{7,6},{8,9},{9,8},{10,11... | collective-permute-start | bytes 4718600 | tf_op jit(solution)/shard_map/ppermute | solution.py:41
  90.7 4.9 %collective-permute-start.18 = (bf16[256,2048]{1,0:T(8,128)(2,1)S(1)}, bf16[256,2048]{1,0:T(8,128)(2,1)S(1)}, u32[]{:S(2)}, u32[]{:S(2)}) collective-permute-start(bf16[256,2048]{1,0:T(8,128)(2,1)S(1)} %collective-permute-done.17.rest_1_), channel_id=1, source_target_pairs={{0,1},{1,0},{2,3},{3,2},{4,5},{5,4},{6,7},{7,6},{8,9},{9,8},{10,11... | collective-permute-start | bytes 3145736 | tf_op jit(solution)/shard_map/ppermute | solution.py:41
  91.2 9.1 %collective-permute-start.6 = (bf16[256,2048]{1,0:T(8,128)(2,1)S(1)}, bf16[256,2048]{1,0:T(8,128)(2,1)S(1)}, u32[]{:S(2)}, u32[]{:S(2)}) collective-permute-start(bf16[256,2048]{1,0:T(8,128)(2,1)S(1)} %get-tuple-element.27), channel_id=1, source_target_pairs={{0,1},{1,0},{2,3},{3,2},{4,5},{5,4},{6,7},{7,6},{8,9},{9,8},{10,11... | collective-permute-start | bytes 3145736 | tf_op jit(solution)/shard_map/ppermute | solution.py:41
  100.1 3.4 %collective-permute-start.19 = (bf16[384,1024]{1,0:T(8,128)(2,1)S(1)}, bf16[384,1024]{1,0:T(8,128)(2,1)S(1)}, u32[]{:S(2)}, u32[]{:S(2)}) collective-permute-start(bf16[384,1024]{1,0:T(8,128)(2,1)S(1)} %get-tuple-element.41), channel_id=1, source_target_pairs={{0,1},{1,0},{2,3},{3,2},{4,5},{5,4},{6,7},{7,6},{8,9},{9,8},{10,11... | collective-permute-start | bytes 2359304 | tf_op jit(solution)/shard_map/ppermute | solution.py:41
  100.7 24.8 %collective-permute-start.7 = (bf16[128,2048]{1,0:T(8,128)(2,1)S(1)}, bf16[128,2048]{1,0:T(8,128)(2,1)S(1)}, u32[]{:S(2)}, u32[]{:S(2)}) collective-permute-start(bf16[128,2048]{1,0:T(8,128)(2,1)S(1)} %get-tuple-element.43), channel_id=1, source_target_pairs={{0,2},{1,3},{2,0},{3,1},{4,6},{5,7},{6,4},{7,5},{8,10},{9,11},{10,... | collective-permute-start | bytes 1572872 | tf_op jit(solution)/shard_map/ppermute | solution.py:41
  103.8 20.0 %collective-permute-start.20 = (bf16[384,512]{1,0:T(8,128)(2,1)S(1)}, bf16[384,512]{1,0:T(8,128)(2,1)S(1)}, u32[]{:S(2)}, u32[]{:S(2)}) collective-permute-start(bf16[384,512]{1,0:T(8,128)(2,1)S(1)} %get-tuple-element.53), channel_id=1, source_target_pairs={{0,2},{1,3},{2,0},{3,1},{4,6},{5,7},{6,4},{7,5},{8,10},{9,11},{10,... | collective-permute-start | bytes 1179656 | tf_op jit(solution)/shard_map/ppermute | solution.py:41
  104.9 10.0 %copy-start = (bf16[512,1536]{1,0:T(8,128)(2,1)S(1)}, bf16[512,1536]{1,0:T(8,128)(2,1)}, u32[]{:S(2)}) copy-start(bf16[512,1536]{1,0:T(8,128)(2,1)} %get-tuple-element.28.pick) | copy-start | bytes 4718596
  104.9 7.8 %collective-permute-start.25 = (bf16[384,256]{1,0:T(8,128)(2,1)S(1)}, bf16[384,256]{1,0:T(8,128)(2,1)S(1)}, u32[]{:S(2)}, u32[]{:S(2)}) collective-permute-start(bf16[384,256]{1,0:T(8,128)(2,1)S(1)} %get-tuple-element.47), channel_id=1, source_target_pairs={{0,8},{8,0},{16,24},{24,16},{1,9},{9,1},{17,25},{25,17},{2,10},{10... | collective-permute-start | bytes 589832 | tf_op jit(solution)/shard_map/ppermute | solution.py:41
  105.6 8.7 %collective-permute-start.26 = (bf16[384,256]{1,0:T(8,128)(2,1)S(1)}, bf16[384,256]{1,0:T(8,128)(2,1)S(1)}, u32[]{:S(2)}, u32[]{:S(2)}) collective-permute-start(bf16[384,256]{1,0:T(8,128)(2,1)S(1)} %get-tuple-element.46), channel_id=1, source_target_pairs={{0,16},{8,24},{16,0},{24,8},{1,17},{9,25},{17,1},{25,9},{2,18},{10... | collective-permute-start | bytes 589832 | tf_op jit(solution)/shard_map/ppermute | solution.py:41
  107.1 26.3 %collective-permute-start.23 = (bf16[384,256]{1,0:T(8,128)(2,1)S(1)}, bf16[384,256]{1,0:T(8,128)(2,1)S(1)}, u32[]{:S(2)}, u32[]{:S(2)}) collective-permute-start(bf16[384,256]{1,0:T(8,128)(2,1)S(1)} %get-tuple-element.49), channel_id=1, source_target_pairs={{0,8},{8,0},{16,24},{24,16},{1,9},{9,1},{17,25},{25,17},{2,10},{10... | collective-permute-start | bytes 589832 | tf_op jit(solution)/shard_map/ppermute | solution.py:41
  112.8 21.4 %collective-permute-start.24 = (bf16[384,256]{1,0:T(8,128)(2,1)S(1)}, bf16[384,256]{1,0:T(8,128)(2,1)S(1)}, u32[]{:S(2)}, u32[]{:S(2)}) collective-permute-start(bf16[384,256]{1,0:T(8,128)(2,1)S(1)} %get-tuple-element.48), channel_id=1, source_target_pairs={{0,16},{8,24},{16,0},{24,8},{1,17},{9,25},{17,1},{25,9},{2,18},{10... | collective-permute-start | bytes 589832 | tf_op jit(solution)/shard_map/ppermute | solution.py:41
  114.3 12.8 %collective-permute-start.29 = (bf16[384,256]{1,0:T(8,128)(2,1)S(1)}, bf16[384,256]{1,0:T(8,128)(2,1)S(1)}, u32[]{:S(2)}, u32[]{:S(2)}) collective-permute-start(bf16[384,256]{1,0:T(8,128)(2,1)S(1)} %get-tuple-element.45), channel_id=1, source_target_pairs={{0,8},{8,0},{16,24},{24,16},{1,9},{9,1},{17,25},{25,17},{2,10},{10... | collective-permute-start | bytes 589832 | tf_op jit(solution)/shard_map/ppermute | solution.py:41
  123.7 6.6 %collective-permute-start.30 = (bf16[384,256]{1,0:T(8,128)(2,1)S(1)}, bf16[384,256]{1,0:T(8,128)(2,1)S(1)}, u32[]{:S(2)}, u32[]{:S(2)}) collective-permute-start(bf16[384,256]{1,0:T(8,128)(2,1)S(1)} %get-tuple-element.44), channel_id=1, source_target_pairs={{0,16},{8,24},{16,0},{24,8},{1,17},{9,25},{17,1},{25,9},{2,18},{10... | collective-permute-start | bytes 589832 | tf_op jit(solution)/shard_map/ppermute | solution.py:41
  125.5 13.1 %collective-permute-start.27 = (bf16[512,256]{1,0:T(8,128)(2,1)S(1)}, bf16[512,256]{1,0:T(8,128)(2,1)S(1)}, u32[]{:S(2)}, u32[]{:S(2)}) collective-permute-start(bf16[512,256]{1,0:T(8,128)(2,1)S(1)} %combine.4), channel_id=1, source_target_pairs={{0,2},{1,3},{2,0},{3,1},{4,6},{5,7},{6,4},{7,5},{8,10},{9,11},{10,... | collective-permute-start | bytes 786440 | tf_op jit(solution)/shard_map/ppermute | solution.py:41
  127.1 12.1 %collective-permute-start.21 = (bf16[384,256]{1,0:T(8,128)(2,1)S(1)}, bf16[384,256]{1,0:T(8,128)(2,1)S(1)}, u32[]{:S(2)}, u32[]{:S(2)}) collective-permute-start(bf16[384,256]{1,0:T(8,128)(2,1)S(1)} %add_convert_fusion.10), channel_id=1, source_target_pairs={{0,4},{1,5},{2,6},{3,7},{4,0},{5,1},{6,2},{7,3},{8,12},{9,13},{10,... | collective-permute-start | bytes 589832 | tf_op jit(solution)/shard_map/ppermute | solution.py:41
  130.3 21.5 %collective-permute-start.8 = (bf16[64,2048]{1,0:T(8,128)(2,1)S(1)}, bf16[64,2048]{1,0:T(8,128)(2,1)S(1)}, u32[]{:S(2)}, u32[]{:S(2)}) collective-permute-start(bf16[64,2048]{1,0:T(8,128)(2,1)S(1)} %add_convert_fusion.7), channel_id=1, source_target_pairs={{0,4},{1,5},{2,6},{3,7},{4,0},{5,1},{6,2},{7,3},{8,12},{9,13},{10,... | collective-permute-start | bytes 786440 | tf_op jit(solution)/shard_map/ppermute | solution.py:41
  133.4 19.2 %collective-permute-start.15 = (bf16[384,256]{1,0:T(8,128)(2,1)S(1)}, bf16[384,256]{1,0:T(8,128)(2,1)S(1)}, u32[]{:S(2)}, u32[]{:S(2)}) collective-permute-start(bf16[384,256]{1,0:T(8,128)(2,1)S(1)} %get-tuple-element.51), channel_id=1, source_target_pairs={{0,8},{8,0},{16,24},{24,16},{1,9},{9,1},{17,25},{25,17},{2,10},{10... | collective-permute-start | bytes 589832 | tf_op jit(solution)/shard_map/ppermute | solution.py:41
  134.1 18.5 %collective-permute-start.16 = (bf16[384,256]{1,0:T(8,128)(2,1)S(1)}, bf16[384,256]{1,0:T(8,128)(2,1)S(1)}, u32[]{:S(2)}, u32[]{:S(2)}) collective-permute-start(bf16[384,256]{1,0:T(8,128)(2,1)S(1)} %get-tuple-element.50), channel_id=1, source_target_pairs={{0,16},{8,24},{16,0},{24,8},{1,17},{9,25},{17,1},{25,9},{2,18},{10... | collective-permute-start | bytes 589832 | tf_op jit(solution)/shard_map/ppermute | solution.py:41
  138.6 14.0 %collective-permute-start.31 = (bf16[512,256]{1,0:T(8,128)(2,1)S(1)}, bf16[512,256]{1,0:T(8,128)(2,1)S(1)}, u32[]{:S(2)}, u32[]{:S(2)}) collective-permute-start(bf16[512,256]{1,0:T(8,128)(2,1)S(1)} %combine.6), channel_id=1, source_target_pairs={{0,2},{1,3},{2,0},{3,1},{4,6},{5,7},{6,4},{7,5},{8,10},{9,11},{10,... | collective-permute-start | bytes 786440 | tf_op jit(solution)/shard_map/ppermute | solution.py:41
  139.2 21.4 %collective-permute-start.28 = (bf16[512,256]{1,0:T(8,128)(2,1)S(1)}, bf16[512,256]{1,0:T(8,128)(2,1)S(1)}, u32[]{:S(2)}, u32[]{:S(2)}) collective-permute-start(bf16[512,256]{1,0:T(8,128)(2,1)S(1)} %combine.5), channel_id=1, source_target_pairs={{0,4},{1,5},{2,6},{3,7},{4,0},{5,1},{6,2},{7,3},{8,12},{9,13},{10,... | collective-permute-start | bytes 786440 | tf_op jit(solution)/shard_map/ppermute | solution.py:41
  151.8 8.7 %collective-permute-start.22 = (bf16[384,256]{1,0:T(8,128)(2,1)S(1)}, bf16[384,256]{1,0:T(8,128)(2,1)S(1)}, u32[]{:S(2)}, u32[]{:S(2)}) collective-permute-start(bf16[384,256]{1,0:T(8,128)(2,1)S(1)} %add_convert_fusion.9), channel_id=1, source_target_pairs={{0,24},{8,16},{16,8},{24,0},{1,25},{9,17},{17,9},{25,1},{2,26},{10... | collective-permute-start | bytes 589832 | tf_op jit(solution)/shard_map/ppermute | solution.py:41

commit v2 on v1

--- a/solution.py
+++ b/solution.py
@@ -282,7 +282,7 @@
 
     loads[4].wait()
     loads[5].wait()
-    tile = min(rows, 256)
+    tile = min(rows, 512)
     plain_lane = lax.broadcasted_iota(jnp.int32, (tile, pair), 1)
     turn_lane = lax.broadcasted_iota(jnp.int32, (tile, turn_lanes), 1)
     zero = jnp.zeros((), BF16)
@@ -490,17 +490,17 @@
         total = found if total is None else total + found
     for carry in rest[count:-1]:
         total = total + carry[...].astype(F32)
-    out[...] = total.astype(BF16)
-
-
-def combine(pick, parts, carries):
+    out[...] = total.astype(out.dtype)
+
+
+def combine(pick, parts, carries, dtype):
     tokens = pick.shape[0]
     names = sorted(parts)
     span, width = parts[names[0]].shape
     operands = [parts[r] for r in names] + list(carries)
     return pl.pallas_call(
         functools.partial(combine_kernel, tuple(r * span for r in names)),
-        out_shape=jax.ShapeDtypeStruct((tokens, width), BF16),
+        out_shape=jax.ShapeDtypeStruct((tokens, width), dtype),
         in_specs=[VMEM_SPEC] * (1 + len(operands)),
         out_specs=VMEM_SPEC,
         compiler_params=params(24),
@@ -658,11 +658,17 @@
         found = {r: swap_over(parts[r, c], "ep", r) if r else parts[r, c] for r in near}
         if not mask:
             found.update(gathered)
-        total = combine(pick, found, carried.pop(mask, []))
+        carries = carried.pop(mask, [])
+        if mask:
+            total = combine(pick, found, carries, BF16)
+        else:
+            total = combine(pick, found, [], F32)
         if mask:
             arrived = swap_over(total, "tp", low_bit(mask))
             carried.setdefault(mask ^ low_bit(mask), []).append(arrived)
-    expert_out = total
+    for carry in carries:
+        total = total + carry.astype(F32)
+    expert_out = total.astype(BF16)
     return (mixer_out, expert_out)
 
 

time: 162 us -> 165 us (1.019)
  waiting for transfers between devices: 78.5 us -> 87 us
  starting transfers between devices: 32.1 us -> 26.3 us
    ppermute x26, waiting for transfers between devices: 37.3 us -> 45.8 us  [swap_over(): return lax.ppermute(value, axis, [(i, i ^ mask) for i in range(size)])]
    ppermute x26, starting transfers between devices: 24.2 us -> 18.4 us  [swap_over(): return lax.ppermute(value, axis, [(i, i ^ mask) for i in range(size)])]
where the time goes in v2:
time: 165 us
  waiting for transfers between devices  87 us (53%)
  Pallas kernels  43.6 us (26%)
  starting transfers between devices  26.3 us (16%)
  other arithmetic  4.64 us (3%)
  local copies, waits for them, and re-layouts  2.12 us (1%)
    ppermute x26, waiting for transfers between devices, swap_over(): return lax.ppermute(value, axis, [(i, i ^ mask) for i in range(size)])  45.8 us
    ppermute x6, waiting for transfers between devices, step_over(): return lax.ppermute(value, ('ep', 'tp'), pairs)  41.2 us
    pallas_call x3, Pallas kernels, run_experts(): pl.pallas_call(functools.partial(experts_kernel, tuple(names), fetch, gro...  20.8 us
    ppermute x26, starting transfers between devices, swap_over(): return lax.ppermute(value, axis, [(i, i ^ mask) for i in range(size)])  18.4 us
    pallas_call x1, Pallas kernels, attention(): pl.pallas_call(functools.partial(attention_kernel, turn_width, len(pieces...  11.6 us
    ppermute x6, starting transfers between devices, step_over(): return lax.ppermute(value, ('ep', 'tp'), pairs)  7.88 us
    pallas_call x1, Pallas kernels, prepare(): pl.pallas_call(prepare_kernel, out_shape=outputs, in_specs=[SMEM_SPEC] +...  4.59 us
    pallas_call x1, Pallas kernels, queries(): pl.pallas_call(functools.partial(query_kernel, turn_width, local_count, c...  4.2 us
  transfers between devices with their start and end apart: 32, of which 12 were waited for; matrix products, arithmetic and copies ran while one was open for 2% of the time, Pallas kernels for 24%

profile of v2, /device:TPU:0, one launch (start us, length us, event | category | flops | bytes accessed | tf_op | source)
XLA Modules:
  0.0 164.6 jit_solution(2014756702867342959)
XLA Ops:
  0.6 0.6 stack.38.ids
  1.3 4.6 %prepare.1 = (bf16[256,640]{1,0:T(8,128)(2,1)}, bf16[256,640]{1,0:T(8,128)(2,1)}, f32[8,512]{1,0:T(8,128)}, bf16[256,2048]{1,0:T(8,128)(2,1)}, bf16[256,2048]{1,0:T(8,128)(2,1)}) custom-call(s32[11]{0:T(128)} %stack.38.ids, bf16[512,512]{1,0:T(8,128)(2,1)} %joint_hbm.1, f32[1,512]{1,0:T(1,128)} %bitcast.26, bf16[32,512]{1,0:T(8,128)(2,1)} %bitcast.20, ...), custom_call_target="tpu_custom_call" | custom-call | flops 12000000 | bytes 4000000 | tf_op jit(solution)/shard_map/prepare/pallas_call | solution.py:141
  5.9 3.1 %collective-permute-start.11 = (bf16[256,2048]{1,0:T(8,128)(2,1)}, bf16[256,2048]{1,0:T(8,128)(2,1)}, u32[]{:S(2)}, u32[]{:S(2)}) collective-permute-start(bf16[256,2048]{1,0:T(8,128)(2,1)} %get-tuple-element.30.rest_1_), channel_id=1, source_target_pairs={{0,16},{1,9},{2,18},{3,11},{4,20},{5,13},{6,22},{7,15},{8,24},{9,1... | collective-permute-start | bytes 3145736 | tf_op jit(solution)/shard_map/ppermute | solution.py:527
  8.9 1.5 collective-permute-start.10
  10.4 0.5 collective-permute-start.1
  11.0 21.7 %collective-permute-done.11.rest_4_ = bf16[256,2048]{1,0:T(8,128)(2,1)} collective-permute-done((bf16[256,2048]{1,0:T(8,128)(2,1)}, bf16[256,2048]{1,0:T(8,128)(2,1)}, u32[]{:S(2)}, u32[]{:S(2)}) %collective-permute-start.11) | collective-permute-done | bytes 1048608 | tf_op jit(solution)/shard_map/ppermute | solution.py:527
  32.7 2.6 %collective-permute-done.10.rest_2_ = bf16[256,2048]{1,0:T(8,128)(2,1)} collective-permute-done((bf16[256,2048]{1,0:T(8,128)(2,1)}, bf16[256,2048]{1,0:T(8,128)(2,1)}, u32[]{:S(2)}, u32[]{:S(2)}) %collective-permute-start.10) | collective-permute-done | bytes 1048608 | tf_op jit(solution)/shard_map/ppermute | solution.py:527
  35.3 0.4 collective-permute-start.17
  35.7 4.0 %collective-permute-done.1.rest_11_ = bf16[256,640]{1,0:T(8,128)(2,1)S(1)} collective-permute-done((bf16[256,640]{1,0:T(8,128)(2,1)}, bf16[256,640]{1,0:T(8,128)(2,1)S(1)}, u32[]{:S(2)}, u32[]{:S(2)}) %collective-permute-start.1) | collective-permute-done | bytes 327712 | tf_op jit(solution)/shard_map/ppermute | solution.py:527
  40.0 2.3 %collective-permute-start.4 = (bf16[256,640]{1,0:T(8,128)(2,1)S(1)}, bf16[256,640]{1,0:T(8,128)(2,1)}, u32[]{:S(2)}, u32[]{:S(2)}) collective-permute-start(bf16[256,640]{1,0:T(8,128)(2,1)S(1)} %collective-permute-done.rest_9_), channel_id=1, source_target_pairs={{0,16},{1,9},{2,18},{3,11},{4,20},{5,13},{6,22},{7,15},{8,24},{9,1... | collective-permute-start | bytes 983048 | tf_op jit(solution)/shard_map/ppermute | solution.py:527
  42.4 12.7 %collective-permute-done.4.rest_13_ = bf16[256,640]{1,0:T(8,128)(2,1)} collective-permute-done((bf16[256,640]{1,0:T(8,128)(2,1)S(1)}, bf16[256,640]{1,0:T(8,128)(2,1)}, u32[]{:S(2)}, u32[]{:S(2)}) %collective-permute-start.4) | collective-permute-done | bytes 327712 | tf_op jit(solution)/shard_map/ppermute | solution.py:527
  55.0 1.2 multiply_sine_fusion
  56.3 4.2 %queries.1 = (bf16[512,256]{1,0:T(8,128)(2,1)}, bf16[512,128]{1,0:T(8,128)(2,1)}, bf16[512,1536]{1,0:T(8,128)(2,1)}) custom-call(s32[11]{0:T(128)} %stack.38.ids, bf16[512,1024]{1,0:T(8,128)(2,1)} %query_latent.1, f32[1,1024]{1,0:T(1,128)} %bitcast.25, bf16[1024,256]{1,0:T(8,128)(2,1)} %query_weight.1, bf16[1024,128]{1,0:T(8,128)(2,1)} %query_rotary.1, ...), custom_call_target="tpu_custom_call" | custom-call | flops 16000000 | bytes 12000000 | tf_op jit(solution)/shard_map/queries/pallas_call | solution.py:216
  60.5 0.6 copy-done.5
  61.1 0.7 copy-done.7
  61.8 6.4 %experts.3 = (bf16[384,1024]{1,0:T(8,128)(2,1)S(1)}, bf16[384,1024]{1,0:T(8,128)(2,1)S(1)}, bf16[2,2048,512]{2,1,0:T(8,128)(2,1)S(1)}, bf16[2,2048,512]{2,1,0:T(8,128)(2,1)S(1)}, bf16[2,512,2048]{2,1,0:T(8,128)(2,1)S(1)}) custom-call(s32[11]{0:T(128)S(1)} %copy-done.5, bf16[2,2048,512]{2,1,0:T(8,128)(2,1)} %gate.1, bf16[2,2048,512]{2,1,0:T(8,128)(2,1)} %up.1, ...), custom_call_target="tpu_custom_call" | custom-call | flops 20000000 | bytes 14000000 | tf_op jit(solution)/shard_map/experts/pallas_call | solution.py:467
  68.2 0.6 collective-permute-start.9
  68.8 11.6 %attention.1 = (bf16[256,2048]{1,0:T(8,128)(2,1)S(1)}, bf16[256,2048]{1,0:T(8,128)(2,1)S(1)}, f32[3,8,512]{2,1,0:T(8,128)S(1)}) custom-call(s32[11]{0:T(128)S(1)} %copy-done.6, bf16[512,256]{1,0:T(8,128)(2,1)} %rest_0_.1, bf16[512,256]{1,0:T(8,128)(2,1)} %rest_1_.1, f32[16,2048]{1,0:T(8,128)} %get-tuple-element.62.cosine.rest_2_, ...), custom_call_target="tpu_custom_call" | custom-call | flops 48000000 | bytes 40000000 | tf_op jit(solution)/shard_map/attention/pallas_call | solution.py:348
  80.5 9.7 %experts.4 = (bf16[768,1024]{1,0:T(8,128)(2,1)S(1)}, bf16[768,1024]{1,0:T(8,128)(2,1)S(1)}) custom-call(s32[11]{0:T(128)S(1)} %copy-done.6, bf16[2,2048,512]{2,1,0:T(8,128)(2,1)S(1)} %get-tuple-element.34.gate, bf16[2,2048,512]{2,1,0:T(8,128)(2,1)S(1)} %get-tuple-element.35.up, bf16[2,512,2048]{2,1,0:T(8,128)(2,1)S(1)} %get-tuple-element.36.down, ...), custom_call_target="tpu_custom_call" | custom-call | flops 40000000 | bytes 28000000 | tf_op jit(solution)/shard_map/experts/pallas_call | solution.py:467
  90.3 0.5 collective-permute-start.18
  91.2 4.0 %collective-permute-done.18.rest_2_ = bf16[256,2048]{1,0:T(8,128)(2,1)S(1)} collective-permute-done((bf16[256,2048]{1,0:T(8,128)(2,1)S(1)}, bf16[256,2048]{1,0:T(8,128)(2,1)S(1)}, u32[]{:S(2)}, u32[]{:S(2)}) %collective-permute-start.18) | collective-permute-done | bytes 1048608 | tf_op jit(solution)/shard_map/ppermute | solution.py:41
  95.2 4.8 %experts.5 = (bf16[384,1024]{1,0:T(8,128)(2,1)S(1)}, bf16[384,1024]{1,0:T(8,128)(2,1)S(1)}) custom-call(s32[11]{0:T(128)S(1)} %copy-done.6, bf16[2,2048,512]{2,1,0:T(8,128)(2,1)S(1)} %get-tuple-element.34.gate, bf16[2,2048,512]{2,1,0:T(8,128)(2,1)S(1)} %get-tuple-element.35.up, bf16[2,512,2048]{2,1,0:T(8,128)(2,1)S(1)} %get-tuple-element.36.down, ...), custom_call_target="tpu_custom_call" | custom-call | flops 20000000 | bytes 14000000 | tf_op jit(solution)/shard_map/experts/pallas_call | solution.py:467
  100.5 2.1 %collective-permute-start.7 = (bf16[128,2048]{1,0:T(8,128)(2,1)S(1)}, bf16[128,2048]{1,0:T(8,128)(2,1)S(1)}, u32[]{:S(2)}, u32[]{:S(2)}) collective-permute-start(bf16[128,2048]{1,0:T(8,128)(2,1)S(1)} %get-tuple-element.43), channel_id=1, source_target_pairs={{0,2},{1,3},{2,0},{3,1},{4,6},{5,7},{6,4},{7,5},{8,10},{9,11},{10,... | collective-permute-start | bytes 1572872 | tf_op jit(solution)/shard_map/ppermute | solution.py:41
  102.7 0.7 add_convert_fusion
  103.6 1.0 collective-permute-start.20
  104.7 0.7 collective-permute-start.25
  105.4 1.5 collective-permute-start.26
  107.0 1.5 collective-permute-start.29
  108.4 4.1 %collective-permute-done.25.rest_1_ = bf16[384,256]{1,0:T(8,128)(2,1)S(1)} collective-permute-done((bf16[384,256]{1,0:T(8,128)(2,1)S(1)}, bf16[384,256]{1,0:T(8,128)(2,1)S(1)}, u32[]{:S(2)}, u32[]{:S(2)}) %collective-permute-start.25) | collective-permute-done | bytes 196640 | tf_op jit(solution)/shard_map/ppermute | solution.py:41
  112.6 1.5 collective-permute-start.30
  114.1 0.6 collective-permute-start.23
  114.7 0.6 combine.5
  115.3 8.3 %collective-permute-done.20 = bf16[384,512]{1,0:T(8,128)(2,1)S(1)} collective-permute-done((bf16[384,512]{1,0:T(8,128)(2,1)S(1)}, bf16[384,512]{1,0:T(8,128)(2,1)S(1)}, u32[]{:S(2)}, u32[]{:S(2)}) %collective-permute-start.20) | collective-permute-done | bytes 393248 | tf_op jit(solution)/shard_map/ppermute | solution.py:41
  123.5 1.7 %collective-permute-start.24 = (bf16[384,256]{1,0:T(8,128)(2,1)S(1)}, bf16[384,256]{1,0:T(8,128)(2,1)S(1)}, u32[]{:S(2)}, u32[]{:S(2)}) collective-permute-start(bf16[384,256]{1,0:T(8,128)(2,1)S(1)} %get-tuple-element.48), channel_id=1, source_target_pairs={{0,16},{8,24},{16,0},{24,8},{1,17},{9,25},{17,1},{25,9},{2,18},{10... | collective-permute-start | bytes 589832 | tf_op jit(solution)/shard_map/ppermute | solution.py:41
  125.3 1.6 collective-permute-start.27
  126.9 2.6 %collective-permute-start.21 = (bf16[384,256]{1,0:T(8,128)(2,1)S(1)}, bf16[384,256]{1,0:T(8,128)(2,1)S(1)}, u32[]{:S(2)}, u32[]{:S(2)}) collective-permute-start(bf16[384,256]{1,0:T(8,128)(2,1)S(1)} %add_convert_fusion.11), channel_id=1, source_target_pairs={{0,4},{1,5},{2,6},{3,7},{4,0},{5,1},{6,2},{7,3},{8,12},{9,13},{10,... | collective-permute-start | bytes 589832 | tf_op jit(solution)/shard_map/ppermute | solution.py:41
  130.0 0.6 combine.7
  130.6 0.7 collective-permute-start.15
  131.2 0.5 collective-permute-start.16
  131.7 6.7 %collective-permute-done.27.rest_3_ = bf16[512,256]{1,0:T(8,128)(2,1)S(1)} collective-permute-done((bf16[512,256]{1,0:T(8,128)(2,1)S(1)}, bf16[512,256]{1,0:T(8,128)(2,1)S(1)}, u32[]{:S(2)}, u32[]{:S(2)}) %collective-permute-start.27) | collective-permute-done | bytes 262176 | tf_op jit(solution)/shard_map/ppermute | solution.py:41
  138.5 0.6 combine.6
  139.0 5.0 %collective-permute-done.21 = bf16[384,256]{1,0:T(8,128)(2,1)S(1)} collective-permute-done((bf16[384,256]{1,0:T(8,128)(2,1)S(1)}, bf16[384,256]{1,0:T(8,128)(2,1)S(1)}, u32[]{:S(2)}, u32[]{:S(2)}) %collective-permute-start.21) | collective-permute-done | bytes 196640 | tf_op jit(solution)/shard_map/ppermute | solution.py:41
  144.1 12.4 %collective-permute-done.8 = bf16[64,2048]{1,0:T(8,128)(2,1)S(1)} collective-permute-done((bf16[64,2048]{1,0:T(8,128)(2,1)S(1)}, bf16[64,2048]{1,0:T(8,128)(2,1)S(1)}, u32[]{:S(2)}, u32[]{:S(2)}) %collective-permute-start.8) | collective-permute-done | bytes 262176 | tf_op jit(solution)/shard_map/ppermute | solution.py:41
  156.5 0.5 collective-permute-start.22
  157.0 0.8 add_convert_fusion.7
  157.8 5.3 %collective-permute-done.22.rest_3_ = bf16[384,256]{1,0:T(8,128)(2,1)S(1)} collective-permute-done((bf16[384,256]{1,0:T(8,128)(2,1)S(1)}, bf16[384,256]{1,0:T(8,128)(2,1)S(1)}, u32[]{:S(2)}, u32[]{:S(2)}) %collective-permute-start.22) | collective-permute-done | bytes 196640 | tf_op jit(solution)/shard_map/ppermute | solution.py:41
  163.1 0.7 combine.4
  163.8 0.8 add_convert_fusion.6
  (58 shorter events, 2.5 us)
Async XLA Ops:
  5.9 54.6 %copy-start.1 = (bf16[256,2048]{1,0:T(8,128)(2,1)S(1)}, bf16[256,2048]{1,0:T(8,128)(2,1)}, u32[]{:S(2)}) copy-start(bf16[256,2048]{1,0:T(8,128)(2,1)} %get-tuple-element.30.rest_1_) | copy-start | bytes 3145732
  5.9 54.6 %copy-start.2 = (bf16[256,2048]{1,0:T(8,128)(2,1)S(1)}, bf16[256,2048]{1,0:T(8,128)(2,1)}, u32[]{:S(2)}) copy-start(bf16[256,2048]{1,0:T(8,128)(2,1)} %get-tuple-element.31.rest_2_) | copy-start | bytes 3145732
  5.9 26.9 %collective-permute-start.11 = (bf16[256,2048]{1,0:T(8,128)(2,1)}, bf16[256,2048]{1,0:T(8,128)(2,1)}, u32[]{:S(2)}, u32[]{:S(2)}) collective-permute-start(bf16[256,2048]{1,0:T(8,128)(2,1)} %get-tuple-element.30.rest_1_), channel_id=1, source_target_pairs={{0,16},{1,9},{2,18},{3,11},{4,20},{5,13},{6,22},{7,15},{8,24},{9,1... | collective-permute-start | bytes 3145736 | tf_op jit(solution)/shard_map/ppermute | solution.py:527
  8.9 26.3 %collective-permute-start.10 = (bf16[256,2048]{1,0:T(8,128)(2,1)}, bf16[256,2048]{1,0:T(8,128)(2,1)}, u32[]{:S(2)}, u32[]{:S(2)}) collective-permute-start(bf16[256,2048]{1,0:T(8,128)(2,1)} %get-tuple-element.30.rest_1_), channel_id=1, source_target_pairs={{0,8},{1,17},{2,10},{3,19},{4,12},{5,21},{6,14},{7,23},{8,0},{9,25... | collective-permute-start | bytes 3145736 | tf_op jit(solution)/shard_map/ppermute | solution.py:527
  10.4 29.3 %collective-permute-start.1 = (bf16[256,640]{1,0:T(8,128)(2,1)}, bf16[256,640]{1,0:T(8,128)(2,1)S(1)}, u32[]{:S(2)}, u32[]{:S(2)}) collective-permute-start(bf16[256,640]{1,0:T(8,128)(2,1)} %get-tuple-element.24.rest_7_), channel_id=1, source_target_pairs={{0,16},{1,9},{2,18},{3,11},{4,20},{5,13},{6,22},{7,15},{8,24},{9,1... | collective-permute-start | bytes 983048 | tf_op jit(solution)/shard_map/ppermute | solution.py:527
  10.9 29.1 %collective-permute-start = (bf16[256,640]{1,0:T(8,128)(2,1)}, bf16[256,640]{1,0:T(8,128)(2,1)S(1)}, u32[]{:S(2)}, u32[]{:S(2)}) collective-permute-start(bf16[256,640]{1,0:T(8,128)(2,1)} %get-tuple-element.24.rest_7_), channel_id=1, source_target_pairs={{0,8},{1,17},{2,10},{3,19},{4,12},{5,21},{6,14},{7,23},{8,0},{9,25... | collective-permute-start | bytes 983048 | tf_op jit(solution)/shard_map/ppermute | solution.py:527
  32.7 47.7 %collective-permute-start.12 = (bf16[256,2048]{1,0:T(8,128)(2,1)}, bf16[256,2048]{1,0:T(8,128)(2,1)}, u32[]{:S(2)}, u32[]{:S(2)}) collective-permute-start(bf16[256,2048]{1,0:T(8,128)(2,1)} %collective-permute-done.11.rest_4_), channel_id=1, source_target_pairs={{0,1},{1,0},{2,3},{3,2},{4,5},{5,4},{6,7},{7,6},{8,9},{9,8},{10,11... | collective-permute-start | bytes 3145736 | tf_op jit(solution)/shard_map/ppermute | solution.py:41
  35.3 45.2 %collective-permute-start.13 = (bf16[256,2048]{1,0:T(8,128)(2,1)}, bf16[256,2048]{1,0:T(8,128)(2,1)}, u32[]{:S(2)}, u32[]{:S(2)}) collective-permute-start(bf16[256,2048]{1,0:T(8,128)(2,1)} %collective-permute-done.10.rest_2_), channel_id=1, source_target_pairs={{0,1},{1,0},{2,3},{3,2},{4,5},{5,4},{6,7},{7,6},{8,9},{9,8},{10,11... | collective-permute-start | bytes 3145736 | tf_op jit(solution)/shard_map/ppermute | solution.py:41
  35.3 55.0 %collective-permute-start.17 = (bf16[256,2048]{1,0:T(8,128)(2,1)}, bf16[256,2048]{1,0:T(8,128)(2,1)S(1)}, u32[]{:S(2)}, u32[]{:S(2)}) collective-permute-start(bf16[256,2048]{1,0:T(8,128)(2,1)} %collective-permute-done.10.rest_2_), channel_id=1, source_target_pairs={{0,16},{1,9},{2,18},{3,11},{4,20},{5,13},{6,22},{7,15},{8,24},{9,1... | collective-permute-start | bytes 3145736 | tf_op jit(solution)/shard_map/ppermute | solution.py:527
  39.8 2.5 %collective-permute-start.2 = (bf16[256,640]{1,0:T(8,128)(2,1)S(1)}, bf16[256,640]{1,0:T(8,128)(2,1)S(1)}, u32[]{:S(2)}, u32[]{:S(2)}) collective-permute-start(bf16[256,640]{1,0:T(8,128)(2,1)S(1)} %collective-permute-done.1.rest_11_), channel_id=1, source_target_pairs={{0,1},{1,0},{2,3},{3,2},{4,5},{5,4},{6,7},{7,6},{8,9},{9,8},{10,11... | collective-permute-start | bytes 983048 | tf_op jit(solution)/shard_map/ppermute | solution.py:41
  40.0 15.0 %collective-permute-start.4 = (bf16[256,640]{1,0:T(8,128)(2,1)S(1)}, bf16[256,640]{1,0:T(8,128)(2,1)}, u32[]{:S(2)}, u32[]{:S(2)}) collective-permute-start(bf16[256,640]{1,0:T(8,128)(2,1)S(1)} %collective-permute-done.rest_9_), channel_id=1, source_target_pairs={{0,16},{1,9},{2,18},{3,11},{4,20},{5,13},{6,22},{7,15},{8,24},{9,1... | collective-permute-start | bytes 983048 | tf_op jit(solution)/shard_map/ppermute | solution.py:527
  42.3 25.9 %collective-permute-start.3 = (bf16[256,640]{1,0:T(8,128)(2,1)S(1)}, bf16[256,640]{1,0:T(8,128)(2,1)}, u32[]{:S(2)}, u32[]{:S(2)}) collective-permute-start(bf16[256,640]{1,0:T(8,128)(2,1)S(1)} %collective-permute-done.rest_9_), channel_id=1, source_target_pairs={{0,1},{1,0},{2,3},{3,2},{4,5},{5,4},{6,7},{7,6},{8,9},{9,8},{10,11... | collective-permute-start | bytes 983048 | tf_op jit(solution)/shard_map/ppermute | solution.py:41
  55.0 13.8 %collective-permute-start.5 = (bf16[256,640]{1,0:T(8,128)(2,1)}, bf16[256,640]{1,0:T(8,128)(2,1)}, u32[]{:S(2)}, u32[]{:S(2)}) collective-permute-start(bf16[256,640]{1,0:T(8,128)(2,1)} %collective-permute-done.4.rest_13_), channel_id=1, source_target_pairs={{0,1},{1,0},{2,3},{3,2},{4,5},{5,4},{6,7},{7,6},{8,9},{9,8},{10,11... | collective-permute-start | bytes 983048 | tf_op jit(solution)/shard_map/ppermute | solution.py:41
  60.5 0.6 copy-start.5
  61.1 0.7 copy-start.7
  61.8 7.0 %copy-start.3 = (bf16[256,640]{1,0:T(8,128)(2,1)S(1)}, bf16[256,640]{1,0:T(8,128)(2,1)}, u32[]{:S(2)}) copy-start(bf16[256,640]{1,0:T(8,128)(2,1)} %get-tuple-element.24.rest_7_) | copy-start | bytes 983044
  61.8 7.0 %copy-start.4 = (bf16[256,640]{1,0:T(8,128)(2,1)S(1)}, bf16[256,640]{1,0:T(8,128)(2,1)}, u32[]{:S(2)}) copy-start(bf16[256,640]{1,0:T(8,128)(2,1)} %get-tuple-element.25.rest_8_) | copy-start | bytes 983044
  61.8 7.0 %copy-start.6 = (s32[11]{0:T(128)S(1)}, s32[11]{0:T(128)}, u32[]{:S(2)}) copy-start(s32[11]{0:T(128)} %stack.38.ids) | copy-start | bytes 136
  68.2 22.6 %collective-permute-start.9 = (bf16[384,1024]{1,0:T(8,128)(2,1)S(1)}, bf16[384,1024]{1,0:T(8,128)(2,1)S(1)}, u32[]{:S(2)}, u32[]{:S(2)}) collective-permute-start(bf16[384,1024]{1,0:T(8,128)(2,1)S(1)} %get-tuple-element.33), channel_id=1, source_target_pairs={{0,1},{1,0},{2,3},{3,2},{4,5},{5,4},{6,7},{7,6},{8,9},{9,8},{10,11... | collective-permute-start | bytes 2359304 | tf_op jit(solution)/shard_map/ppermute | solution.py:41
  90.2 12.5 %collective-permute-start.14 = (bf16[768,1024]{1,0:T(8,128)(2,1)S(1)}, bf16[768,1024]{1,0:T(8,128)(2,1)S(1)}, u32[]{:S(2)}, u32[]{:S(2)}) collective-permute-start(bf16[768,1024]{1,0:T(8,128)(2,1)S(1)} %get-tuple-element.39), channel_id=1, source_target_pairs={{0,1},{1,0},{2,3},{3,2},{4,5},{5,4},{6,7},{7,6},{8,9},{9,8},{10,11... | collective-permute-start | bytes 4718600 | tf_op jit(solution)/shard_map/ppermute | solution.py:41
  90.3 4.9 %collective-permute-start.18 = (bf16[256,2048]{1,0:T(8,128)(2,1)S(1)}, bf16[256,2048]{1,0:T(8,128)(2,1)S(1)}, u32[]{:S(2)}, u32[]{:S(2)}) collective-permute-start(bf16[256,2048]{1,0:T(8,128)(2,1)S(1)} %collective-permute-done.17.rest_1_), channel_id=1, source_target_pairs={{0,1},{1,0},{2,3},{3,2},{4,5},{5,4},{6,7},{7,6},{8,9},{9,8},{10,11... | collective-permute-start | bytes 3145736 | tf_op jit(solution)/shard_map/ppermute | solution.py:41
  90.8 9.4 %collective-permute-start.6 = (bf16[256,2048]{1,0:T(8,128)(2,1)S(1)}, bf16[256,2048]{1,0:T(8,128)(2,1)S(1)}, u32[]{:S(2)}, u32[]{:S(2)}) collective-permute-start(bf16[256,2048]{1,0:T(8,128)(2,1)S(1)} %get-tuple-element.27), channel_id=1, source_target_pairs={{0,1},{1,0},{2,3},{3,2},{4,5},{5,4},{6,7},{7,6},{8,9},{9,8},{10,11... | collective-permute-start | bytes 3145736 | tf_op jit(solution)/shard_map/ppermute | solution.py:41
  99.9 3.4 %collective-permute-start.19 = (bf16[384,1024]{1,0:T(8,128)(2,1)S(1)}, bf16[384,1024]{1,0:T(8,128)(2,1)S(1)}, u32[]{:S(2)}, u32[]{:S(2)}) collective-permute-start(bf16[384,1024]{1,0:T(8,128)(2,1)S(1)} %get-tuple-element.41), channel_id=1, source_target_pairs={{0,1},{1,0},{2,3},{3,2},{4,5},{5,4},{6,7},{7,6},{8,9},{9,8},{10,11... | collective-permute-start | bytes 2359304 | tf_op jit(solution)/shard_map/ppermute | solution.py:41
  100.5 24.8 %collective-permute-start.7 = (bf16[128,2048]{1,0:T(8,128)(2,1)S(1)}, bf16[128,2048]{1,0:T(8,128)(2,1)S(1)}, u32[]{:S(2)}, u32[]{:S(2)}) collective-permute-start(bf16[128,2048]{1,0:T(8,128)(2,1)S(1)} %get-tuple-element.43), channel_id=1, source_target_pairs={{0,2},{1,3},{2,0},{3,1},{4,6},{5,7},{6,4},{7,5},{8,10},{9,11},{10,... | collective-permute-start | bytes 1572872 | tf_op jit(solution)/shard_map/ppermute | solution.py:41
  103.6 19.9 %collective-permute-start.20 = (bf16[384,512]{1,0:T(8,128)(2,1)S(1)}, bf16[384,512]{1,0:T(8,128)(2,1)S(1)}, u32[]{:S(2)}, u32[]{:S(2)}) collective-permute-start(bf16[384,512]{1,0:T(8,128)(2,1)S(1)} %get-tuple-element.53), channel_id=1, source_target_pairs={{0,2},{1,3},{2,0},{3,1},{4,6},{5,7},{6,4},{7,5},{8,10},{9,11},{10,... | collective-permute-start | bytes 1179656 | tf_op jit(solution)/shard_map/ppermute | solution.py:41
  104.7 10.0 %copy-start = (bf16[512,1536]{1,0:T(8,128)(2,1)S(1)}, bf16[512,1536]{1,0:T(8,128)(2,1)}, u32[]{:S(2)}) copy-start(bf16[512,1536]{1,0:T(8,128)(2,1)} %get-tuple-element.28.pick) | copy-start | bytes 4718596
  104.7 7.8 %collective-permute-start.25 = (bf16[384,256]{1,0:T(8,128)(2,1)S(1)}, bf16[384,256]{1,0:T(8,128)(2,1)S(1)}, u32[]{:S(2)}, u32[]{:S(2)}) collective-permute-start(bf16[384,256]{1,0:T(8,128)(2,1)S(1)} %get-tuple-element.47), channel_id=1, source_target_pairs={{0,8},{8,0},{16,24},{24,16},{1,9},{9,1},{17,25},{25,17},{2,10},{10... | collective-permute-start | bytes 589832 | tf_op jit(solution)/shard_map/ppermute | solution.py:41
  105.4 8.7 %collective-permute-start.26 = (bf16[384,256]{1,0:T(8,128)(2,1)S(1)}, bf16[384,256]{1,0:T(8,128)(2,1)S(1)}, u32[]{:S(2)}, u32[]{:S(2)}) collective-permute-start(bf16[384,256]{1,0:T(8,128)(2,1)S(1)} %get-tuple-element.44), channel_id=1, source_target_pairs={{0,16},{8,24},{16,0},{24,8},{1,17},{9,25},{17,1},{25,9},{2,18},{10... | collective-permute-start | bytes 589832 | tf_op jit(solution)/shard_map/ppermute | solution.py:41
  107.0 19.9 %collective-permute-start.29 = (bf16[384,256]{1,0:T(8,128)(2,1)S(1)}, bf16[384,256]{1,0:T(8,128)(2,1)S(1)}, u32[]{:S(2)}, u32[]{:S(2)}) collective-permute-start(bf16[384,256]{1,0:T(8,128)(2,1)S(1)} %get-tuple-element.46), channel_id=1, source_target_pairs={{0,8},{8,0},{16,24},{24,16},{1,9},{9,1},{17,25},{25,17},{2,10},{10... | collective-permute-start | bytes 589832 | tf_op jit(solution)/shard_map/ppermute | solution.py:41
  112.6 17.0 %collective-permute-start.30 = (bf16[384,256]{1,0:T(8,128)(2,1)S(1)}, bf16[384,256]{1,0:T(8,128)(2,1)S(1)}, u32[]{:S(2)}, u32[]{:S(2)}) collective-permute-start(bf16[384,256]{1,0:T(8,128)(2,1)S(1)} %get-tuple-element.45), channel_id=1, source_target_pairs={{0,16},{8,24},{16,0},{24,8},{1,17},{9,25},{17,1},{25,9},{2,18},{10... | collective-permute-start | bytes 589832 | tf_op jit(solution)/shard_map/ppermute | solution.py:41
  114.1 16.5 %collective-permute-start.23 = (bf16[384,256]{1,0:T(8,128)(2,1)S(1)}, bf16[384,256]{1,0:T(8,128)(2,1)S(1)}, u32[]{:S(2)}, u32[]{:S(2)}) collective-permute-start(bf16[384,256]{1,0:T(8,128)(2,1)S(1)} %get-tuple-element.49), channel_id=1, source_target_pairs={{0,8},{8,0},{16,24},{24,16},{1,9},{9,1},{17,25},{25,17},{2,10},{10... | collective-permute-start | bytes 589832 | tf_op jit(solution)/shard_map/ppermute | solution.py:41
  123.5 7.7 %collective-permute-start.24 = (bf16[384,256]{1,0:T(8,128)(2,1)S(1)}, bf16[384,256]{1,0:T(8,128)(2,1)S(1)}, u32[]{:S(2)}, u32[]{:S(2)}) collective-permute-start(bf16[384,256]{1,0:T(8,128)(2,1)S(1)} %get-tuple-element.48), channel_id=1, source_target_pairs={{0,16},{8,24},{16,0},{24,8},{1,17},{9,25},{17,1},{25,9},{2,18},{10... | collective-permute-start | bytes 589832 | tf_op jit(solution)/shard_map/ppermute | solution.py:41
  125.3 13.1 %collective-permute-start.27 = (bf16[512,256]{1,0:T(8,128)(2,1)S(1)}, bf16[512,256]{1,0:T(8,128)(2,1)S(1)}, u32[]{:S(2)}, u32[]{:S(2)}) collective-permute-start(bf16[512,256]{1,0:T(8,128)(2,1)S(1)} %combine.5), channel_id=1, source_target_pairs={{0,2},{1,3},{2,0},{3,1},{4,6},{5,7},{6,4},{7,5},{8,10},{9,11},{10,... | collective-permute-start | bytes 786440 | tf_op jit(solution)/shard_map/ppermute | solution.py:41
  126.9 17.1 %collective-permute-start.21 = (bf16[384,256]{1,0:T(8,128)(2,1)S(1)}, bf16[384,256]{1,0:T(8,128)(2,1)S(1)}, u32[]{:S(2)}, u32[]{:S(2)}) collective-permute-start(bf16[384,256]{1,0:T(8,128)(2,1)S(1)} %add_convert_fusion.11), channel_id=1, source_target_pairs={{0,4},{1,5},{2,6},{3,7},{4,0},{5,1},{6,2},{7,3},{8,12},{9,13},{10,... | collective-permute-start | bytes 589832 | tf_op jit(solution)/shard_map/ppermute | solution.py:41
  129.6 26.9 %collective-permute-start.8 = (bf16[64,2048]{1,0:T(8,128)(2,1)S(1)}, bf16[64,2048]{1,0:T(8,128)(2,1)S(1)}, u32[]{:S(2)}, u32[]{:S(2)}) collective-permute-start(bf16[64,2048]{1,0:T(8,128)(2,1)S(1)} %add_convert_fusion.8), channel_id=1, source_target_pairs={{0,4},{1,5},{2,6},{3,7},{4,0},{5,1},{6,2},{7,3},{8,12},{9,13},{10,... | collective-permute-start | bytes 786440 | tf_op jit(solution)/shard_map/ppermute | solution.py:41
  130.6 27.3 %collective-permute-start.15 = (bf16[384,256]{1,0:T(8,128)(2,1)S(1)}, bf16[384,256]{1,0:T(8,128)(2,1)S(1)}, u32[]{:S(2)}, u32[]{:S(2)}) collective-permute-start(bf16[384,256]{1,0:T(8,128)(2,1)S(1)} %get-tuple-element.51), channel_id=1, source_target_pairs={{0,8},{8,0},{16,24},{24,16},{1,9},{9,1},{17,25},{25,17},{2,10},{10... | collective-permute-start | bytes 589832 | tf_op jit(solution)/shard_map/ppermute | solution.py:41
  131.2 26.6 %collective-permute-start.16 = (bf16[384,256]{1,0:T(8,128)(2,1)S(1)}, bf16[384,256]{1,0:T(8,128)(2,1)S(1)}, u32[]{:S(2)}, u32[]{:S(2)}) collective-permute-start(bf16[384,256]{1,0:T(8,128)(2,1)S(1)} %get-tuple-element.50), channel_id=1, source_target_pairs={{0,16},{8,24},{16,0},{24,8},{1,17},{9,25},{17,1},{25,9},{2,18},{10... | collective-permute-start | bytes 589832 | tf_op jit(solution)/shard_map/ppermute | solution.py:41
  138.5 25.3 %collective-permute-start.31 = (bf16[512,256]{1,0:T(8,128)(2,1)S(1)}, bf16[512,256]{1,0:T(8,128)(2,1)S(1)}, u32[]{:S(2)}, u32[]{:S(2)}) collective-permute-start(bf16[512,256]{1,0:T(8,128)(2,1)S(1)} %combine.7), channel_id=1, source_target_pairs={{0,2},{1,3},{2,0},{3,1},{4,6},{5,7},{6,4},{7,5},{8,10},{9,11},{10,... | collective-permute-start | bytes 786440 | tf_op jit(solution)/shard_map/ppermute | solution.py:41
  144.0 19.8 %collective-permute-start.28 = (bf16[512,256]{1,0:T(8,128)(2,1)S(1)}, bf16[512,256]{1,0:T(8,128)(2,1)S(1)}, u32[]{:S(2)}, u32[]{:S(2)}) collective-permute-start(bf16[512,256]{1,0:T(8,128)(2,1)S(1)} %combine.6), channel_id=1, source_target_pairs={{0,4},{1,5},{2,6},{3,7},{4,0},{5,1},{6,2},{7,3},{8,12},{9,13},{10,... | collective-permute-start | bytes 786440 | tf_op jit(solution)/shard_map/ppermute | solution.py:41
  156.5 6.6 %collective-permute-start.22 = (bf16[384,256]{1,0:T(8,128)(2,1)S(1)}, bf16[384,256]{1,0:T(8,128)(2,1)S(1)}, u32[]{:S(2)}, u32[]{:S(2)}) collective-permute-start(bf16[384,256]{1,0:T(8,128)(2,1)S(1)} %add_convert_fusion.10), channel_id=1, source_target_pairs={{0,24},{8,16},{16,8},{24,0},{1,25},{9,17},{17,9},{25,1},{2,26},{10... | collective-permute-start | bytes 589832 | tf_op jit(solution)/shard_map/ppermute | solution.py:41

commit v3 on v2

--- a/solution.py
+++ b/solution.py
@@ -75,13 +75,23 @@
         (joint_hbm, joint), (joint_gain_hbm, joint_gain), (rotary_hbm, rotary),
         (routes_hbm, routes), (weights_hbm, weights), (rows_gain_hbm, rows_gain), (rows_hbm, rows),
     )
+    half, full = mine.shape
+    own = pl.multiple_of(ids[1] * half, half)
+    far = pl.multiple_of((1 - ids[1]) * half, half)
+    cut = half // 2
+    spans = [(own, 0), (own, cut), (far, 0), (far, cut)]
+    inputs = inputs[:-1] + tuple(
+        (rows_hbm.at[pl.ds(base + at, cut)], rows.at[pl.ds(base + at, cut)]) for base, at in spans
+    )
     loads = [
         pltpu.make_async_copy(source, target, sems.at[i])
         for i, (source, target) in enumerate(inputs)
     ]
-    outputs = (
-        (mine, mine_hbm), (other, other_hbm), (meta, meta_hbm), (row_mine, row_mine_hbm),
-        (row_other, row_other_hbm),
+    outputs = ((mine, mine_hbm), (other, other_hbm), (meta, meta_hbm)) + tuple(
+        (source.at[pl.ds(at, cut)], target.at[pl.ds(at, cut)])
+        for (source, target), (_, at) in zip(
+            [(row_mine, row_mine_hbm)] * 2 + [(row_other, row_other_hbm)] * 2, spans
+        )
     )
     stores = [
         pltpu.make_async_copy(source, target, sems.at[len(loads) + i])
@@ -91,7 +101,6 @@
         load.start()
     for load in loads[:5]:
         load.wait()
-    half, full = mine.shape
     count, width = joint.shape
     turn, top = rotary.shape[0], routes.shape[0]
     weight = weights[...]
@@ -107,19 +116,17 @@
     chosen = ids[1] == 0
     mine[:, width:] = jnp.where(chosen, side[:half], side[half:])
     other[:, width:] = jnp.where(chosen, side[half:], side[:half])
-    own = pl.multiple_of(ids[1] * half, half)
-    far = pl.multiple_of((1 - ids[1]) * half, half)
     mine[:, :width] = norm_value(joint[pl.ds(own, half), :], joint_gain[...])
     stores[0].start()
     other[:, :width] = norm_value(joint[pl.ds(far, half), :], joint_gain[...])
     stores[1].start()
     stores[2].start()
-    for load in loads[5:]:
-        load.wait()
-    row_mine[...] = norm_value(rows[pl.ds(own, half), :], rows_gain[...])
-    stores[3].start()
-    row_other[...] = norm_value(rows[pl.ds(far, half), :], rows_gain[...])
-    stores[4].start()
+    loads[5].wait()
+    for i, (base, at) in enumerate(spans):
+        loads[6 + i].wait()
+        target = row_mine if i < 2 else row_other
+        target[at : at + cut, :] = norm_value(rows[pl.ds(base + at, cut), :], rows_gain[...])
+        stores[3 + i].start()
     for store in stores:
         store.wait()
 
@@ -144,7 +151,7 @@
         in_specs=[SMEM_SPEC] + [HBM_SPEC] * len(inputs),
         out_specs=(HBM_SPEC,) * len(outputs),
         scratch_shapes=[pltpu.VMEM(v.shape, v.dtype) for v in inputs + outputs]
-        + [pltpu.SemaphoreType.DMA((len(inputs) + len(outputs),))],
+        + [pltpu.SemaphoreType.DMA((len(inputs) + len(outputs) + 5,))],
         compiler_params=params(60),
         cost_estimate=cost(4e12 * 3e-6, 4e6),
         name="prepare",

time: 165 us -> 164 us (level)
  no operation moved by 1% of the time
where the time goes in v3:
time: 164 us
  waiting for transfers between devices  86.9 us (53%)
  Pallas kernels  42.9 us (26%)
  starting transfers between devices  26.4 us (16%)
  other arithmetic  4.65 us (3%)
  local copies, waits for them, and re-layouts  2.12 us (1%)
    ppermute x26, waiting for transfers between devices, swap_over(): return lax.ppermute(value, axis, [(i, i ^ mask) for i in range(size)])  45.8 us
    ppermute x6, waiting for transfers between devices, step_over(): return lax.ppermute(value, ('ep', 'tp'), pairs)  41.2 us
    pallas_call x3, Pallas kernels, run_experts(): pl.pallas_call(functools.partial(experts_kernel, tuple(names), fetch, gro...  20.8 us
    ppermute x26, starting transfers between devices, swap_over(): return lax.ppermute(value, axis, [(i, i ^ mask) for i in range(size)])  18.5 us
    pallas_call x1, Pallas kernels, attention(): pl.pallas_call(functools.partial(attention_kernel, turn_width, len(pieces...  11.6 us
    ppermute x6, starting transfers between devices, step_over(): return lax.ppermute(value, ('ep', 'tp'), pairs)  7.88 us
    pallas_call x1, Pallas kernels, queries(): pl.pallas_call(functools.partial(query_kernel, turn_width, local_count, c...  4.2 us
    pallas_call x1, Pallas kernels, prepare(): pl.pallas_call(prepare_kernel, out_shape=outputs, in_specs=[SMEM_SPEC] +...  3.87 us
  transfers between devices with their start and end apart: 32, of which 12 were waited for; matrix products, arithmetic and copies ran while one was open for 2% of the time, Pallas kernels for 24%

profile of v3, /device:TPU:0, one launch (start us, length us, event | category | flops | bytes accessed | tf_op | source)
XLA Modules:
  0.0 163.9 jit_solution(10636345868087056515)
XLA Ops:
  0.6 0.6 stack.38.ids
  1.3 3.9 %prepare.1 = (bf16[256,640]{1,0:T(8,128)(2,1)}, bf16[256,640]{1,0:T(8,128)(2,1)}, f32[8,512]{1,0:T(8,128)}, bf16[256,2048]{1,0:T(8,128)(2,1)}, bf16[256,2048]{1,0:T(8,128)(2,1)}) custom-call(s32[11]{0:T(128)} %stack.38.ids, bf16[512,512]{1,0:T(8,128)(2,1)} %joint_hbm.1, f32[1,512]{1,0:T(1,128)} %bitcast.26, bf16[32,512]{1,0:T(8,128)(2,1)} %bitcast.20, ...), custom_call_target="tpu_custom_call" | custom-call | flops 12000000 | bytes 4000000 | tf_op jit(solution)/shard_map/prepare/pallas_call | solution.py:148
  5.2 3.1 %collective-permute-start.11 = (bf16[256,2048]{1,0:T(8,128)(2,1)}, bf16[256,2048]{1,0:T(8,128)(2,1)}, u32[]{:S(2)}, u32[]{:S(2)}) collective-permute-start(bf16[256,2048]{1,0:T(8,128)(2,1)} %get-tuple-element.30.rest_1_), channel_id=1, source_target_pairs={{0,16},{1,9},{2,18},{3,11},{4,20},{5,13},{6,22},{7,15},{8,24},{9,1... | collective-permute-start | bytes 3145736 | tf_op jit(solution)/shard_map/ppermute | solution.py:534
  8.2 1.5 collective-permute-start.10
  9.7 0.5 collective-permute-start.1
  10.3 21.7 %collective-permute-done.11.rest_4_ = bf16[256,2048]{1,0:T(8,128)(2,1)} collective-permute-done((bf16[256,2048]{1,0:T(8,128)(2,1)}, bf16[256,2048]{1,0:T(8,128)(2,1)}, u32[]{:S(2)}, u32[]{:S(2)}) %collective-permute-start.11) | collective-permute-done | bytes 1048608 | tf_op jit(solution)/shard_map/ppermute | solution.py:534
  32.0 2.6 %collective-permute-done.10.rest_2_ = bf16[256,2048]{1,0:T(8,128)(2,1)} collective-permute-done((bf16[256,2048]{1,0:T(8,128)(2,1)}, bf16[256,2048]{1,0:T(8,128)(2,1)}, u32[]{:S(2)}, u32[]{:S(2)}) %collective-permute-start.10) | collective-permute-done | bytes 1048608 | tf_op jit(solution)/shard_map/ppermute | solution.py:534
  34.6 0.4 collective-permute-start.17
  35.0 4.0 %collective-permute-done.1.rest_11_ = bf16[256,640]{1,0:T(8,128)(2,1)S(1)} collective-permute-done((bf16[256,640]{1,0:T(8,128)(2,1)}, bf16[256,640]{1,0:T(8,128)(2,1)S(1)}, u32[]{:S(2)}, u32[]{:S(2)}) %collective-permute-start.1) | collective-permute-done | bytes 327712 | tf_op jit(solution)/shard_map/ppermute | solution.py:534
  39.3 2.3 %collective-permute-start.4 = (bf16[256,640]{1,0:T(8,128)(2,1)S(1)}, bf16[256,640]{1,0:T(8,128)(2,1)}, u32[]{:S(2)}, u32[]{:S(2)}) collective-permute-start(bf16[256,640]{1,0:T(8,128)(2,1)S(1)} %collective-permute-done.rest_9_), channel_id=1, source_target_pairs={{0,16},{1,9},{2,18},{3,11},{4,20},{5,13},{6,22},{7,15},{8,24},{9,1... | collective-permute-start | bytes 983048 | tf_op jit(solution)/shard_map/ppermute | solution.py:534
  41.7 12.7 %collective-permute-done.4.rest_13_ = bf16[256,640]{1,0:T(8,128)(2,1)} collective-permute-done((bf16[256,640]{1,0:T(8,128)(2,1)S(1)}, bf16[256,640]{1,0:T(8,128)(2,1)}, u32[]{:S(2)}, u32[]{:S(2)}) %collective-permute-start.4) | collective-permute-done | bytes 327712 | tf_op jit(solution)/shard_map/ppermute | solution.py:534
  54.3 1.2 multiply_sine_fusion
  55.6 4.2 %queries.1 = (bf16[512,256]{1,0:T(8,128)(2,1)}, bf16[512,128]{1,0:T(8,128)(2,1)}, bf16[512,1536]{1,0:T(8,128)(2,1)}) custom-call(s32[11]{0:T(128)} %stack.38.ids, bf16[512,1024]{1,0:T(8,128)(2,1)} %query_latent.1, f32[1,1024]{1,0:T(1,128)} %bitcast.25, bf16[1024,256]{1,0:T(8,128)(2,1)} %query_weight.1, bf16[1024,128]{1,0:T(8,128)(2,1)} %query_rotary.1, ...), custom_call_target="tpu_custom_call" | custom-call | flops 16000000 | bytes 12000000 | tf_op jit(solution)/shard_map/queries/pallas_call | solution.py:223
  59.8 0.6 copy-done.5
  60.4 0.7 copy-done.7
  61.1 6.4 %experts.3 = (bf16[384,1024]{1,0:T(8,128)(2,1)S(1)}, bf16[384,1024]{1,0:T(8,128)(2,1)S(1)}, bf16[2,2048,512]{2,1,0:T(8,128)(2,1)S(1)}, bf16[2,2048,512]{2,1,0:T(8,128)(2,1)S(1)}, bf16[2,512,2048]{2,1,0:T(8,128)(2,1)S(1)}) custom-call(s32[11]{0:T(128)S(1)} %copy-done.5, bf16[2,2048,512]{2,1,0:T(8,128)(2,1)} %gate.1, bf16[2,2048,512]{2,1,0:T(8,128)(2,1)} %up.1, ...), custom_call_target="tpu_custom_call" | custom-call | flops 20000000 | bytes 14000000 | tf_op jit(solution)/shard_map/experts/pallas_call | solution.py:474
  67.5 0.6 collective-permute-start.9
  68.1 11.6 %attention.1 = (bf16[256,2048]{1,0:T(8,128)(2,1)S(1)}, bf16[256,2048]{1,0:T(8,128)(2,1)S(1)}, f32[3,8,512]{2,1,0:T(8,128)S(1)}) custom-call(s32[11]{0:T(128)S(1)} %copy-done.6, bf16[512,256]{1,0:T(8,128)(2,1)} %rest_0_.1, bf16[512,256]{1,0:T(8,128)(2,1)} %rest_1_.1, f32[16,2048]{1,0:T(8,128)} %get-tuple-element.62.cosine.rest_2_, ...), custom_call_target="tpu_custom_call" | custom-call | flops 48000000 | bytes 40000000 | tf_op jit(solution)/shard_map/attention/pallas_call | solution.py:355
  79.8 9.7 %experts.4 = (bf16[768,1024]{1,0:T(8,128)(2,1)S(1)}, bf16[768,1024]{1,0:T(8,128)(2,1)S(1)}) custom-call(s32[11]{0:T(128)S(1)} %copy-done.6, bf16[2,2048,512]{2,1,0:T(8,128)(2,1)S(1)} %get-tuple-element.34.gate, bf16[2,2048,512]{2,1,0:T(8,128)(2,1)S(1)} %get-tuple-element.35.up, bf16[2,512,2048]{2,1,0:T(8,128)(2,1)S(1)} %get-tuple-element.36.down, ...), custom_call_target="tpu_custom_call" | custom-call | flops 40000000 | bytes 28000000 | tf_op jit(solution)/shard_map/experts/pallas_call | solution.py:474
  89.6 0.5 collective-permute-start.18
  90.4 4.0 %collective-permute-done.18.rest_2_ = bf16[256,2048]{1,0:T(8,128)(2,1)S(1)} collective-permute-done((bf16[256,2048]{1,0:T(8,128)(2,1)S(1)}, bf16[256,2048]{1,0:T(8,128)(2,1)S(1)}, u32[]{:S(2)}, u32[]{:S(2)}) %collective-permute-start.18) | collective-permute-done | bytes 1048608 | tf_op jit(solution)/shard_map/ppermute | solution.py:41
  94.4 4.8 %experts.5 = (bf16[384,1024]{1,0:T(8,128)(2,1)S(1)}, bf16[384,1024]{1,0:T(8,128)(2,1)S(1)}) custom-call(s32[11]{0:T(128)S(1)} %copy-done.6, bf16[2,2048,512]{2,1,0:T(8,128)(2,1)S(1)} %get-tuple-element.34.gate, bf16[2,2048,512]{2,1,0:T(8,128)(2,1)S(1)} %get-tuple-element.35.up, bf16[2,512,2048]{2,1,0:T(8,128)(2,1)S(1)} %get-tuple-element.36.down, ...), custom_call_target="tpu_custom_call" | custom-call | flops 20000000 | bytes 14000000 | tf_op jit(solution)/shard_map/experts/pallas_call | solution.py:474
  99.8 2.1 %collective-permute-start.7 = (bf16[128,2048]{1,0:T(8,128)(2,1)S(1)}, bf16[128,2048]{1,0:T(8,128)(2,1)S(1)}, u32[]{:S(2)}, u32[]{:S(2)}) collective-permute-start(bf16[128,2048]{1,0:T(8,128)(2,1)S(1)} %get-tuple-element.43), channel_id=1, source_target_pairs={{0,2},{1,3},{2,0},{3,1},{4,6},{5,7},{6,4},{7,5},{8,10},{9,11},{10,... | collective-permute-start | bytes 1572872 | tf_op jit(solution)/shard_map/ppermute | solution.py:41
  101.9 0.7 add_convert_fusion
  102.9 1.0 collective-permute-start.20
  104.0 0.7 collective-permute-start.25
  104.7 1.5 collective-permute-start.26
  106.2 1.5 collective-permute-start.29
  107.7 4.1 %collective-permute-done.25.rest_1_ = bf16[384,256]{1,0:T(8,128)(2,1)S(1)} collective-permute-done((bf16[384,256]{1,0:T(8,128)(2,1)S(1)}, bf16[384,256]{1,0:T(8,128)(2,1)S(1)}, u32[]{:S(2)}, u32[]{:S(2)}) %collective-permute-start.25) | collective-permute-done | bytes 196640 | tf_op jit(solution)/shard_map/ppermute | solution.py:41
  111.8 1.5 collective-permute-start.30
  113.3 0.6 collective-permute-start.23
  114.0 0.6 combine.5
  114.5 8.3 %collective-permute-done.20 = bf16[384,512]{1,0:T(8,128)(2,1)S(1)} collective-permute-done((bf16[384,512]{1,0:T(8,128)(2,1)S(1)}, bf16[384,512]{1,0:T(8,128)(2,1)S(1)}, u32[]{:S(2)}, u32[]{:S(2)}) %collective-permute-start.20) | collective-permute-done | bytes 393248 | tf_op jit(solution)/shard_map/ppermute | solution.py:41
  122.8 1.7 %collective-permute-start.24 = (bf16[384,256]{1,0:T(8,128)(2,1)S(1)}, bf16[384,256]{1,0:T(8,128)(2,1)S(1)}, u32[]{:S(2)}, u32[]{:S(2)}) collective-permute-start(bf16[384,256]{1,0:T(8,128)(2,1)S(1)} %get-tuple-element.48), channel_id=1, source_target_pairs={{0,16},{8,24},{16,0},{24,8},{1,17},{9,25},{17,1},{25,9},{2,18},{10... | collective-permute-start | bytes 589832 | tf_op jit(solution)/shard_map/ppermute | solution.py:41
  124.6 1.6 collective-permute-start.27
  126.2 2.6 %collective-permute-start.21 = (bf16[384,256]{1,0:T(8,128)(2,1)S(1)}, bf16[384,256]{1,0:T(8,128)(2,1)S(1)}, u32[]{:S(2)}, u32[]{:S(2)}) collective-permute-start(bf16[384,256]{1,0:T(8,128)(2,1)S(1)} %add_convert_fusion.11), channel_id=1, source_target_pairs={{0,4},{1,5},{2,6},{3,7},{4,0},{5,1},{6,2},{7,3},{8,12},{9,13},{10,... | collective-permute-start | bytes 589832 | tf_op jit(solution)/shard_map/ppermute | solution.py:41
  129.3 0.6 combine.7
  129.8 0.7 collective-permute-start.15
  130.5 0.5 collective-permute-start.16
  131.0 6.7 %collective-permute-done.27.rest_3_ = bf16[512,256]{1,0:T(8,128)(2,1)S(1)} collective-permute-done((bf16[512,256]{1,0:T(8,128)(2,1)S(1)}, bf16[512,256]{1,0:T(8,128)(2,1)S(1)}, u32[]{:S(2)}, u32[]{:S(2)}) %collective-permute-start.27) | collective-permute-done | bytes 262176 | tf_op jit(solution)/shard_map/ppermute | solution.py:41
  137.7 0.6 combine.6
  138.3 5.0 %collective-permute-done.21 = bf16[384,256]{1,0:T(8,128)(2,1)S(1)} collective-permute-done((bf16[384,256]{1,0:T(8,128)(2,1)S(1)}, bf16[384,256]{1,0:T(8,128)(2,1)S(1)}, u32[]{:S(2)}, u32[]{:S(2)}) %collective-permute-start.21) | collective-permute-done | bytes 196640 | tf_op jit(solution)/shard_map/ppermute | solution.py:41
  143.4 12.4 %collective-permute-done.8 = bf16[64,2048]{1,0:T(8,128)(2,1)S(1)} collective-permute-done((bf16[64,2048]{1,0:T(8,128)(2,1)S(1)}, bf16[64,2048]{1,0:T(8,128)(2,1)S(1)}, u32[]{:S(2)}, u32[]{:S(2)}) %collective-permute-start.8) | collective-permute-done | bytes 262176 | tf_op jit(solution)/shard_map/ppermute | solution.py:41
  155.8 0.5 collective-permute-start.22
  156.3 0.8 add_convert_fusion.7
  157.1 5.2 %collective-permute-done.22.rest_3_ = bf16[384,256]{1,0:T(8,128)(2,1)S(1)} collective-permute-done((bf16[384,256]{1,0:T(8,128)(2,1)S(1)}, bf16[384,256]{1,0:T(8,128)(2,1)S(1)}, u32[]{:S(2)}, u32[]{:S(2)}) %collective-permute-start.22) | collective-permute-done | bytes 196640 | tf_op jit(solution)/shard_map/ppermute | solution.py:41
  162.4 0.7 combine.4
  163.1 0.8 add_convert_fusion.6
  (58 shorter events, 2.5 us)
Async XLA Ops:
  5.1 54.6 %copy-start.1 = (bf16[256,2048]{1,0:T(8,128)(2,1)S(1)}, bf16[256,2048]{1,0:T(8,128)(2,1)}, u32[]{:S(2)}) copy-start(bf16[256,2048]{1,0:T(8,128)(2,1)} %get-tuple-element.30.rest_1_) | copy-start | bytes 3145732
  5.2 54.6 %copy-start.2 = (bf16[256,2048]{1,0:T(8,128)(2,1)S(1)}, bf16[256,2048]{1,0:T(8,128)(2,1)}, u32[]{:S(2)}) copy-start(bf16[256,2048]{1,0:T(8,128)(2,1)} %get-tuple-element.31.rest_2_) | copy-start | bytes 3145732
  5.2 26.9 %collective-permute-start.11 = (bf16[256,2048]{1,0:T(8,128)(2,1)}, bf16[256,2048]{1,0:T(8,128)(2,1)}, u32[]{:S(2)}, u32[]{:S(2)}) collective-permute-start(bf16[256,2048]{1,0:T(8,128)(2,1)} %get-tuple-element.30.rest_1_), channel_id=1, source_target_pairs={{0,16},{1,9},{2,18},{3,11},{4,20},{5,13},{6,22},{7,15},{8,24},{9,1... | collective-permute-start | bytes 3145736 | tf_op jit(solution)/shard_map/ppermute | solution.py:534
  8.2 26.3 %collective-permute-start.10 = (bf16[256,2048]{1,0:T(8,128)(2,1)}, bf16[256,2048]{1,0:T(8,128)(2,1)}, u32[]{:S(2)}, u32[]{:S(2)}) collective-permute-start(bf16[256,2048]{1,0:T(8,128)(2,1)} %get-tuple-element.30.rest_1_), channel_id=1, source_target_pairs={{0,8},{1,17},{2,10},{3,19},{4,12},{5,21},{6,14},{7,23},{8,0},{9,25... | collective-permute-start | bytes 3145736 | tf_op jit(solution)/shard_map/ppermute | solution.py:534
  9.7 29.3 %collective-permute-start.1 = (bf16[256,640]{1,0:T(8,128)(2,1)}, bf16[256,640]{1,0:T(8,128)(2,1)S(1)}, u32[]{:S(2)}, u32[]{:S(2)}) collective-permute-start(bf16[256,640]{1,0:T(8,128)(2,1)} %get-tuple-element.24.rest_7_), channel_id=1, source_target_pairs={{0,16},{1,9},{2,18},{3,11},{4,20},{5,13},{6,22},{7,15},{8,24},{9,1... | collective-permute-start | bytes 983048 | tf_op jit(solution)/shard_map/ppermute | solution.py:534
  10.2 29.1 %collective-permute-start = (bf16[256,640]{1,0:T(8,128)(2,1)}, bf16[256,640]{1,0:T(8,128)(2,1)S(1)}, u32[]{:S(2)}, u32[]{:S(2)}) collective-permute-start(bf16[256,640]{1,0:T(8,128)(2,1)} %get-tuple-element.24.rest_7_), channel_id=1, source_target_pairs={{0,8},{1,17},{2,10},{3,19},{4,12},{5,21},{6,14},{7,23},{8,0},{9,25... | collective-permute-start | bytes 983048 | tf_op jit(solution)/shard_map/ppermute | solution.py:534
  32.0 47.7 %collective-permute-start.12 = (bf16[256,2048]{1,0:T(8,128)(2,1)}, bf16[256,2048]{1,0:T(8,128)(2,1)}, u32[]{:S(2)}, u32[]{:S(2)}) collective-permute-start(bf16[256,2048]{1,0:T(8,128)(2,1)} %collective-permute-done.11.rest_4_), channel_id=1, source_target_pairs={{0,1},{1,0},{2,3},{3,2},{4,5},{5,4},{6,7},{7,6},{8,9},{9,8},{10,11... | collective-permute-start | bytes 3145736 | tf_op jit(solution)/shard_map/ppermute | solution.py:41
  34.6 45.2 %collective-permute-start.13 = (bf16[256,2048]{1,0:T(8,128)(2,1)}, bf16[256,2048]{1,0:T(8,128)(2,1)}, u32[]{:S(2)}, u32[]{:S(2)}) collective-permute-start(bf16[256,2048]{1,0:T(8,128)(2,1)} %collective-permute-done.10.rest_2_), channel_id=1, source_target_pairs={{0,1},{1,0},{2,3},{3,2},{4,5},{5,4},{6,7},{7,6},{8,9},{9,8},{10,11... | collective-permute-start | bytes 3145736 | tf_op jit(solution)/shard_map/ppermute | solution.py:41
  34.6 55.0 %collective-permute-start.17 = (bf16[256,2048]{1,0:T(8,128)(2,1)}, bf16[256,2048]{1,0:T(8,128)(2,1)S(1)}, u32[]{:S(2)}, u32[]{:S(2)}) collective-permute-start(bf16[256,2048]{1,0:T(8,128)(2,1)} %collective-permute-done.10.rest_2_), channel_id=1, source_target_pairs={{0,16},{1,9},{2,18},{3,11},{4,20},{5,13},{6,22},{7,15},{8,24},{9,1... | collective-permute-start | bytes 3145736 | tf_op jit(solution)/shard_map/ppermute | solution.py:534
  39.0 2.5 %collective-permute-start.2 = (bf16[256,640]{1,0:T(8,128)(2,1)S(1)}, bf16[256,640]{1,0:T(8,128)(2,1)S(1)}, u32[]{:S(2)}, u32[]{:S(2)}) collective-permute-start(bf16[256,640]{1,0:T(8,128)(2,1)S(1)} %collective-permute-done.1.rest_11_), channel_id=1, source_target_pairs={{0,1},{1,0},{2,3},{3,2},{4,5},{5,4},{6,7},{7,6},{8,9},{9,8},{10,11... | collective-permute-start | bytes 983048 | tf_op jit(solution)/shard_map/ppermute | solution.py:41
  39.3 15.0 %collective-permute-start.4 = (bf16[256,640]{1,0:T(8,128)(2,1)S(1)}, bf16[256,640]{1,0:T(8,128)(2,1)}, u32[]{:S(2)}, u32[]{:S(2)}) collective-permute-start(bf16[256,640]{1,0:T(8,128)(2,1)S(1)} %collective-permute-done.rest_9_), channel_id=1, source_target_pairs={{0,16},{1,9},{2,18},{3,11},{4,20},{5,13},{6,22},{7,15},{8,24},{9,1... | collective-permute-start | bytes 983048 | tf_op jit(solution)/shard_map/ppermute | solution.py:534
  41.6 25.9 %collective-permute-start.3 = (bf16[256,640]{1,0:T(8,128)(2,1)S(1)}, bf16[256,640]{1,0:T(8,128)(2,1)}, u32[]{:S(2)}, u32[]{:S(2)}) collective-permute-start(bf16[256,640]{1,0:T(8,128)(2,1)S(1)} %collective-permute-done.rest_9_), channel_id=1, source_target_pairs={{0,1},{1,0},{2,3},{3,2},{4,5},{5,4},{6,7},{7,6},{8,9},{9,8},{10,11... | collective-permute-start | bytes 983048 | tf_op jit(solution)/shard_map/ppermute | solution.py:41
  54.3 13.8 %collective-permute-start.5 = (bf16[256,640]{1,0:T(8,128)(2,1)}, bf16[256,640]{1,0:T(8,128)(2,1)}, u32[]{:S(2)}, u32[]{:S(2)}) collective-permute-start(bf16[256,640]{1,0:T(8,128)(2,1)} %collective-permute-done.4.rest_13_), channel_id=1, source_target_pairs={{0,1},{1,0},{2,3},{3,2},{4,5},{5,4},{6,7},{7,6},{8,9},{9,8},{10,11... | collective-permute-start | bytes 983048 | tf_op jit(solution)/shard_map/ppermute | solution.py:41
  59.8 0.6 copy-start.5
  60.4 0.7 copy-start.7
  61.1 7.0 %copy-start.3 = (bf16[256,640]{1,0:T(8,128)(2,1)S(1)}, bf16[256,640]{1,0:T(8,128)(2,1)}, u32[]{:S(2)}) copy-start(bf16[256,640]{1,0:T(8,128)(2,1)} %get-tuple-element.24.rest_7_) | copy-start | bytes 983044
  61.1 7.0 %copy-start.4 = (bf16[256,640]{1,0:T(8,128)(2,1)S(1)}, bf16[256,640]{1,0:T(8,128)(2,1)}, u32[]{:S(2)}) copy-start(bf16[256,640]{1,0:T(8,128)(2,1)} %get-tuple-element.25.rest_8_) | copy-start | bytes 983044
  61.1 7.0 %copy-start.6 = (s32[11]{0:T(128)S(1)}, s32[11]{0:T(128)}, u32[]{:S(2)}) copy-start(s32[11]{0:T(128)} %stack.38.ids) | copy-start | bytes 136
  67.5 22.6 %collective-permute-start.9 = (bf16[384,1024]{1,0:T(8,128)(2,1)S(1)}, bf16[384,1024]{1,0:T(8,128)(2,1)S(1)}, u32[]{:S(2)}, u32[]{:S(2)}) collective-permute-start(bf16[384,1024]{1,0:T(8,128)(2,1)S(1)} %get-tuple-element.33), channel_id=1, source_target_pairs={{0,1},{1,0},{2,3},{3,2},{4,5},{5,4},{6,7},{7,6},{8,9},{9,8},{10,11... | collective-permute-start | bytes 2359304 | tf_op jit(solution)/shard_map/ppermute | solution.py:41
  89.5 12.5 %collective-permute-start.14 = (bf16[768,1024]{1,0:T(8,128)(2,1)S(1)}, bf16[768,1024]{1,0:T(8,128)(2,1)S(1)}, u32[]{:S(2)}, u32[]{:S(2)}) collective-permute-start(bf16[768,1024]{1,0:T(8,128)(2,1)S(1)} %get-tuple-element.39), channel_id=1, source_target_pairs={{0,1},{1,0},{2,3},{3,2},{4,5},{5,4},{6,7},{7,6},{8,9},{9,8},{10,11... | collective-permute-start | bytes 4718600 | tf_op jit(solution)/shard_map/ppermute | solution.py:41
  89.6 4.9 %collective-permute-start.18 = (bf16[256,2048]{1,0:T(8,128)(2,1)S(1)}, bf16[256,2048]{1,0:T(8,128)(2,1)S(1)}, u32[]{:S(2)}, u32[]{:S(2)}) collective-permute-start(bf16[256,2048]{1,0:T(8,128)(2,1)S(1)} %collective-permute-done.17.rest_1_), channel_id=1, source_target_pairs={{0,1},{1,0},{2,3},{3,2},{4,5},{5,4},{6,7},{7,6},{8,9},{9,8},{10,11... | collective-permute-start | bytes 3145736 | tf_op jit(solution)/shard_map/ppermute | solution.py:41
  90.0 9.3 %collective-permute-start.6 = (bf16[256,2048]{1,0:T(8,128)(2,1)S(1)}, bf16[256,2048]{1,0:T(8,128)(2,1)S(1)}, u32[]{:S(2)}, u32[]{:S(2)}) collective-permute-start(bf16[256,2048]{1,0:T(8,128)(2,1)S(1)} %get-tuple-element.27), channel_id=1, source_target_pairs={{0,1},{1,0},{2,3},{3,2},{4,5},{5,4},{6,7},{7,6},{8,9},{9,8},{10,11... | collective-permute-start | bytes 3145736 | tf_op jit(solution)/shard_map/ppermute | solution.py:41
  99.2 3.4 %collective-permute-start.19 = (bf16[384,1024]{1,0:T(8,128)(2,1)S(1)}, bf16[384,1024]{1,0:T(8,128)(2,1)S(1)}, u32[]{:S(2)}, u32[]{:S(2)}) collective-permute-start(bf16[384,1024]{1,0:T(8,128)(2,1)S(1)} %get-tuple-element.41), channel_id=1, source_target_pairs={{0,1},{1,0},{2,3},{3,2},{4,5},{5,4},{6,7},{7,6},{8,9},{9,8},{10,11... | collective-permute-start | bytes 2359304 | tf_op jit(solution)/shard_map/ppermute | solution.py:41
  99.8 24.8 %collective-permute-start.7 = (bf16[128,2048]{1,0:T(8,128)(2,1)S(1)}, bf16[128,2048]{1,0:T(8,128)(2,1)S(1)}, u32[]{:S(2)}, u32[]{:S(2)}) collective-permute-start(bf16[128,2048]{1,0:T(8,128)(2,1)S(1)} %get-tuple-element.43), channel_id=1, source_target_pairs={{0,2},{1,3},{2,0},{3,1},{4,6},{5,7},{6,4},{7,5},{8,10},{9,11},{10,... | collective-permute-start | bytes 1572872 | tf_op jit(solution)/shard_map/ppermute | solution.py:41
  102.9 19.9 %collective-permute-start.20 = (bf16[384,512]{1,0:T(8,128)(2,1)S(1)}, bf16[384,512]{1,0:T(8,128)(2,1)S(1)}, u32[]{:S(2)}, u32[]{:S(2)}) collective-permute-start(bf16[384,512]{1,0:T(8,128)(2,1)S(1)} %get-tuple-element.53), channel_id=1, source_target_pairs={{0,2},{1,3},{2,0},{3,1},{4,6},{5,7},{6,4},{7,5},{8,10},{9,11},{10,... | collective-permute-start | bytes 1179656 | tf_op jit(solution)/shard_map/ppermute | solution.py:41
  104.0 10.0 %copy-start = (bf16[512,1536]{1,0:T(8,128)(2,1)S(1)}, bf16[512,1536]{1,0:T(8,128)(2,1)}, u32[]{:S(2)}) copy-start(bf16[512,1536]{1,0:T(8,128)(2,1)} %get-tuple-element.28.pick) | copy-start | bytes 4718596
  104.0 7.8 %collective-permute-start.25 = (bf16[384,256]{1,0:T(8,128)(2,1)S(1)}, bf16[384,256]{1,0:T(8,128)(2,1)S(1)}, u32[]{:S(2)}, u32[]{:S(2)}) collective-permute-start(bf16[384,256]{1,0:T(8,128)(2,1)S(1)} %get-tuple-element.47), channel_id=1, source_target_pairs={{0,8},{8,0},{16,24},{24,16},{1,9},{9,1},{17,25},{25,17},{2,10},{10... | collective-permute-start | bytes 589832 | tf_op jit(solution)/shard_map/ppermute | solution.py:41
  104.7 8.7 %collective-permute-start.26 = (bf16[384,256]{1,0:T(8,128)(2,1)S(1)}, bf16[384,256]{1,0:T(8,128)(2,1)S(1)}, u32[]{:S(2)}, u32[]{:S(2)}) collective-permute-start(bf16[384,256]{1,0:T(8,128)(2,1)S(1)} %get-tuple-element.44), channel_id=1, source_target_pairs={{0,16},{8,24},{16,0},{24,8},{1,17},{9,25},{17,1},{25,9},{2,18},{10... | collective-permute-start | bytes 589832 | tf_op jit(solution)/shard_map/ppermute | solution.py:41
  106.2 19.9 %collective-permute-start.29 = (bf16[384,256]{1,0:T(8,128)(2,1)S(1)}, bf16[384,256]{1,0:T(8,128)(2,1)S(1)}, u32[]{:S(2)}, u32[]{:S(2)}) collective-permute-start(bf16[384,256]{1,0:T(8,128)(2,1)S(1)} %get-tuple-element.46), channel_id=1, source_target_pairs={{0,8},{8,0},{16,24},{24,16},{1,9},{9,1},{17,25},{25,17},{2,10},{10... | collective-permute-start | bytes 589832 | tf_op jit(solution)/shard_map/ppermute | solution.py:41
  111.8 17.0 %collective-permute-start.30 = (bf16[384,256]{1,0:T(8,128)(2,1)S(1)}, bf16[384,256]{1,0:T(8,128)(2,1)S(1)}, u32[]{:S(2)}, u32[]{:S(2)}) collective-permute-start(bf16[384,256]{1,0:T(8,128)(2,1)S(1)} %get-tuple-element.45), channel_id=1, source_target_pairs={{0,16},{8,24},{16,0},{24,8},{1,17},{9,25},{17,1},{25,9},{2,18},{10... | collective-permute-start | bytes 589832 | tf_op jit(solution)/shard_map/ppermute | solution.py:41
  113.3 16.5 %collective-permute-start.23 = (bf16[384,256]{1,0:T(8,128)(2,1)S(1)}, bf16[384,256]{1,0:T(8,128)(2,1)S(1)}, u32[]{:S(2)}, u32[]{:S(2)}) collective-permute-start(bf16[384,256]{1,0:T(8,128)(2,1)S(1)} %get-tuple-element.49), channel_id=1, source_target_pairs={{0,8},{8,0},{16,24},{24,16},{1,9},{9,1},{17,25},{25,17},{2,10},{10... | collective-permute-start | bytes 589832 | tf_op jit(solution)/shard_map/ppermute | solution.py:41
  122.8 7.7 %collective-permute-start.24 = (bf16[384,256]{1,0:T(8,128)(2,1)S(1)}, bf16[384,256]{1,0:T(8,128)(2,1)S(1)}, u32[]{:S(2)}, u32[]{:S(2)}) collective-permute-start(bf16[384,256]{1,0:T(8,128)(2,1)S(1)} %get-tuple-element.48), channel_id=1, source_target_pairs={{0,16},{8,24},{16,0},{24,8},{1,17},{9,25},{17,1},{25,9},{2,18},{10... | collective-permute-start | bytes 589832 | tf_op jit(solution)/shard_map/ppermute | solution.py:41
  124.6 13.1 %collective-permute-start.27 = (bf16[512,256]{1,0:T(8,128)(2,1)S(1)}, bf16[512,256]{1,0:T(8,128)(2,1)S(1)}, u32[]{:S(2)}, u32[]{:S(2)}) collective-permute-start(bf16[512,256]{1,0:T(8,128)(2,1)S(1)} %combine.5), channel_id=1, source_target_pairs={{0,2},{1,3},{2,0},{3,1},{4,6},{5,7},{6,4},{7,5},{8,10},{9,11},{10,... | collective-permute-start | bytes 786440 | tf_op jit(solution)/shard_map/ppermute | solution.py:41
  126.2 17.1 %collective-permute-start.21 = (bf16[384,256]{1,0:T(8,128)(2,1)S(1)}, bf16[384,256]{1,0:T(8,128)(2,1)S(1)}, u32[]{:S(2)}, u32[]{:S(2)}) collective-permute-start(bf16[384,256]{1,0:T(8,128)(2,1)S(1)} %add_convert_fusion.11), channel_id=1, source_target_pairs={{0,4},{1,5},{2,6},{3,7},{4,0},{5,1},{6,2},{7,3},{8,12},{9,13},{10,... | collective-permute-start | bytes 589832 | tf_op jit(solution)/shard_map/ppermute | solution.py:41
  128.9 26.9 %collective-permute-start.8 = (bf16[64,2048]{1,0:T(8,128)(2,1)S(1)}, bf16[64,2048]{1,0:T(8,128)(2,1)S(1)}, u32[]{:S(2)}, u32[]{:S(2)}) collective-permute-start(bf16[64,2048]{1,0:T(8,128)(2,1)S(1)} %add_convert_fusion.8), channel_id=1, source_target_pairs={{0,4},{1,5},{2,6},{3,7},{4,0},{5,1},{6,2},{7,3},{8,12},{9,13},{10,... | collective-permute-start | bytes 786440 | tf_op jit(solution)/shard_map/ppermute | solution.py:41
  129.8 27.3 %collective-permute-start.15 = (bf16[384,256]{1,0:T(8,128)(2,1)S(1)}, bf16[384,256]{1,0:T(8,128)(2,1)S(1)}, u32[]{:S(2)}, u32[]{:S(2)}) collective-permute-start(bf16[384,256]{1,0:T(8,128)(2,1)S(1)} %get-tuple-element.51), channel_id=1, source_target_pairs={{0,8},{8,0},{16,24},{24,16},{1,9},{9,1},{17,25},{25,17},{2,10},{10... | collective-permute-start | bytes 589832 | tf_op jit(solution)/shard_map/ppermute | solution.py:41
  130.5 26.6 %collective-permute-start.16 = (bf16[384,256]{1,0:T(8,128)(2,1)S(1)}, bf16[384,256]{1,0:T(8,128)(2,1)S(1)}, u32[]{:S(2)}, u32[]{:S(2)}) collective-permute-start(bf16[384,256]{1,0:T(8,128)(2,1)S(1)} %get-tuple-element.50), channel_id=1, source_target_pairs={{0,16},{8,24},{16,0},{24,8},{1,17},{9,25},{17,1},{25,9},{2,18},{10... | collective-permute-start | bytes 589832 | tf_op jit(solution)/shard_map/ppermute | solution.py:41
  137.7 25.4 %collective-permute-start.31 = (bf16[512,256]{1,0:T(8,128)(2,1)S(1)}, bf16[512,256]{1,0:T(8,128)(2,1)S(1)}, u32[]{:S(2)}, u32[]{:S(2)}) collective-permute-start(bf16[512,256]{1,0:T(8,128)(2,1)S(1)} %combine.7), channel_id=1, source_target_pairs={{0,2},{1,3},{2,0},{3,1},{4,6},{5,7},{6,4},{7,5},{8,10},{9,11},{10,... | collective-permute-start | bytes 786440 | tf_op jit(solution)/shard_map/ppermute | solution.py:41
  143.3 19.8 %collective-permute-start.28 = (bf16[512,256]{1,0:T(8,128)(2,1)S(1)}, bf16[512,256]{1,0:T(8,128)(2,1)S(1)}, u32[]{:S(2)}, u32[]{:S(2)}) collective-permute-start(bf16[512,256]{1,0:T(8,128)(2,1)S(1)} %combine.6), channel_id=1, source_target_pairs={{0,4},{1,5},{2,6},{3,7},{4,0},{5,1},{6,2},{7,3},{8,12},{9,13},{10,... | collective-permute-start | bytes 786440 | tf_op jit(solution)/shard_map/ppermute | solution.py:41
  155.8 6.6 %collective-permute-start.22 = (bf16[384,256]{1,0:T(8,128)(2,1)S(1)}, bf16[384,256]{1,0:T(8,128)(2,1)S(1)}, u32[]{:S(2)}, u32[]{:S(2)}) collective-permute-start(bf16[384,256]{1,0:T(8,128)(2,1)S(1)} %add_convert_fusion.10), channel_id=1, source_target_pairs={{0,24},{8,16},{16,8},{24,0},{1,25},{9,17},{17,9},{25,1},{2,26},{10... | collective-permute-start | bytes 589832 | tf_op jit(solution)/shard_map/ppermute | solution.py:41
